TPU v7x, 1024 devices: a whole 8x8x8 slice. The times are simulated.
1024 devices in a mesh: ep: 64 (over z, y), tp: 16 (over x, core).
Axes of the slice: x: 8, y: 8, z: 8, core: 2. Of those that a mesh axis runs over, the one named last changes fastest.
Arguments:
- hidden: bfloat16 [1024, 2048], P('ep'), may hold values from -6 to 6
- lengths: int32 [1024], P(('ep', 'tp')), may hold values from 1 to 1535, 786432 in all
- latent_cache: bfloat16 [1024, 1536, 512], P(('ep', 'tp')), may hold values from -6 to 6
- cache_rotary: bfloat16 [1024, 32, 1536], P(('ep', 'tp')), may hold values from -1500 to 1500
- attn_gain: bfloat16 [2048], replicated, may hold values from 0.099609375 to 1.8984375
- w_query_nope: bfloat16 [2048, 1024], P(None, 'tp'), may hold values from -0.125 to 0.125
- w_query_rope: bfloat16 [2048, 512], P(None, 'tp'), may hold values from -0.125 to 0.125
- latent_weight: bfloat16 [2048, 512], replicated, may hold values from -0.125 to 0.125
- w_rotary_key: bfloat16 [2048, 32], replicated, may hold values from -0.125 to 0.125
- latent_norm_gain: bfloat16 [512], replicated, may hold values from 0.099609375 to 1.8984375
- key_up_weight: bfloat16 [1024, 512], P('tp'), may hold values from -0.75 to 0.75
- value_up_weight: bfloat16 [512, 1024], P(None, 'tp'), may hold values from -0.25 to 0.25
- head_gain: bfloat16 [1024], P('tp'), may hold values from 0.099609375 to 1.8984375
- w_output: bfloat16 [1024, 2048], P('tp'), may hold values from -0.1875 to 0.1875
- ffn_gain: bfloat16 [2048], replicated, may hold values from 0.099609375 to 1.8984375
- expert_ids: int32 [1024, 4], P('ep'), may hold values from 0 to 63, all different within a row; in each aligned block of 16 rows (0 to 15, 16 to 31, ...) at most 2 rows name the same one
- expert_weights: float32 [1024, 4], P('ep'), may hold values from 0.2 to 1.2
- w_expert_gate: bfloat16 [64, 2048, 2048], P('ep', None, 'tp'), may hold values from -0.125 to 0.125
- w_expert_up: bfloat16 [64, 2048, 2048], P('ep', None, 'tp'), may hold values from -0.125 to 0.125
- w_expert_down: bfloat16 [64, 2048, 2048], P('ep', 'tp'), may hold values from -0.125 to 0.125
- w_shared_gate: bfloat16 [2048, 1024], P(None, 'tp'), may hold values from -0.125 to 0.125
- w_shared_up: bfloat16 [2048, 1024], P(None, 'tp'), may hold values from -0.125 to 0.125
- w_shared_down: bfloat16 [1024, 2048], P('tp'), may hold values from -0.1875 to 0.1875
- w_dense_up: bfloat16 [2048, 2048], P(None, 'tp'), may hold values from -0.125 to 0.125
- w_dense_down: bfloat16 [2048, 2048], P('tp'), may hold values from -0.125 to 0.125
- dense_gate: bfloat16 [2048], replicated, may hold values from -0.125 to 0.125
Outputs:
- layer_out: bfloat16 [1024, 2048], P('ep', 'tp')
Inputs may be any that keep to these rules, and one draw needn't show every extreme that they name: `lengths`: past positions of each sequence; the longest has exactly 1535, so every cache has room for the new token. `expert_ids`: A row's 4 experts differ. Among the rows of one index of ep (16 rows), no expert is named by more than 2 of them, a bound that some block reaches.
All inputs are finite; a program needn't handle non-finite values. No bound on the sum of `lengths` on one device may be relied on, other than what follows from the above.
Results may differ from a plain program's by a relative error of at most 0.024.
Values may be sent and summed in bfloat16 or wider, within the bound.
No kernel may reach another device: no remote copies, remote signals or barrier semaphores. Data moves between devices by JAX's collectives and lax.ppermute only.
A program may use at most 32 MiB of HBM per device.

v0:
```python
import jax
import jax.numpy as jnp
from jax import lax
from jax.sharding import PartitionSpec as P

MODEL_WIDTH = 2048
PLAIN_QUERY = 64
ROPE = 32
LATENT_UNITS = 512


def gathered_total(x, axis):
    return lax.all_gather(x, axis).astype(jnp.float32).sum(0)


def split_up(x, dim, peers):
    before, after = (x.shape[:dim], x.shape[dim + 1 :])
    return jnp.moveaxis(x.reshape(*before, peers, -1, *after), dim, 0)


def summed_on_arrival(x, axis, dim):
    tiles = split_up(x, dim, lax.axis_size(axis))
    arrived = lax.all_to_all(tiles, axis, split_axis=0, concat_axis=0, tiled=True)
    return arrived.astype(jnp.float32).sum(axis=0)


def side_by_side(arrays, axis, dim, along):
    ends, at = ([], 0)
    for a in arrays[:-1]:
        at += a.shape[along]
        ends.append(at)
    both = jnp.concatenate(arrays, axis=along)
    return tuple(jnp.split(summed_on_arrival(both, axis, dim), ends, axis=along))


def norm_rows(values, gains):
    values = values.astype(jnp.float32)
    factor = lax.rsqrt(jnp.mean(values * values, axis=-1, keepdims=True) + 1e-06)
    return values * factor * gains.astype(jnp.float32)


def angles_at(positions, rot_width):
    half_width = rot_width // 2
    inverse = 1.0 / 10000.0 ** (jnp.arange(half_width, dtype=jnp.float32) / half_width)
    return positions.astype(jnp.float32)[..., None] * inverse


def rotate(values, angles):
    half_width = values.shape[-1] // 2
    first = values[..., :half_width]
    second = values[..., half_width:]
    cosines = jnp.cos(angles)
    sines = jnp.sin(angles)
    return jnp.concatenate(
        [first * cosines - second * sines, first * sines + second * cosines], axis=-1
    )


def on_device(
    hidden,
    lengths,
    latent_cache,
    cache_rotary,
    attn_gain,
    w_query_nope,
    w_query_rope,
    latent_weight,
    w_rotary_key,
    latent_norm_gain,
    key_up_weight,
    value_up_weight,
    head_gain,
    w_output,
    ffn_gain,
    expert_ids,
    expert_weights,
    w_expert_gate,
    w_expert_up,
    w_expert_down,
    w_shared_gate,
    w_shared_up,
    w_shared_down,
    w_dense_up,
    w_dense_down,
    dense_gate,
):
    tensor_split_count = lax.axis_size("tp")
    ep_size = lax.axis_size("ep")
    tp_index = lax.axis_index("tp")
    grouped_rows = hidden.shape[0]
    sequences_per_device = lengths.shape[0]
    heads_per_device = w_query_nope.shape[1] // PLAIN_QUERY
    normed = norm_rows(hidden, attn_gain).astype(jnp.bfloat16)
    query_unrotated = jnp.dot(normed, w_query_nope, preferred_element_type=jnp.float32).astype(
        jnp.bfloat16
    )
    query_unrotated = query_unrotated.reshape(grouped_rows, heads_per_device, PLAIN_QUERY)
    query_rope = jnp.dot(normed, w_query_rope, preferred_element_type=jnp.float32).astype(
        jnp.bfloat16
    )
    query_rope = query_rope.reshape(grouped_rows, 1, heads_per_device, ROPE)
    query_in_latent = jnp.einsum(
        "ghn,hnr->ghr",
        query_unrotated,
        key_up_weight.reshape(heads_per_device, PLAIN_QUERY, LATENT_UNITS),
        preferred_element_type=jnp.float32,
    ).astype(jnp.bfloat16)
    query_in_latent = query_in_latent.reshape(grouped_rows, 1, heads_per_device, LATENT_UNITS)
    own_rows = lax.dynamic_slice_in_dim(
        normed, tp_index * sequences_per_device, sequences_per_device, 0
    )
    angles = angles_at(lengths, ROPE)
    new_latent = norm_rows(
        jnp.dot(own_rows, latent_weight, preferred_element_type=jnp.float32), latent_norm_gain
    ).astype(jnp.bfloat16)
    new_key = rotate(
        jnp.dot(own_rows, w_rotary_key, preferred_element_type=jnp.float32), angles
    ).astype(jnp.bfloat16)
    in_cache = jnp.arange(latent_cache.shape[1], dtype=jnp.int32)[None, :] < lengths[:, None]
    score_scale = (PLAIN_QUERY + ROPE) ** (-0.5)
    latent_query_rows = lax.all_to_all(
        query_in_latent, "tp", split_axis=0, concat_axis=1, tiled=True
    )
    rot_query = lax.all_to_all(query_rope, "tp", split_axis=0, concat_axis=1, tiled=True)
    element_count = latent_query_rows.shape[2]
    latent_query_rows = latent_query_rows.reshape(sequences_per_device, -1, LATENT_UNITS)
    rot_query = rotate(
        rot_query.reshape(sequences_per_device, -1, ROPE).astype(jnp.float32), angles[:, None, :]
    )
    rot_query = rot_query.astype(jnp.bfloat16)
    cache_scores = jnp.einsum(
        "shr,slr->shl", latent_query_rows, latent_cache, preferred_element_type=jnp.float32
    )
    cache_scores = cache_scores + jnp.einsum(
        "shp,spl->shl", rot_query, cache_rotary, preferred_element_type=jnp.float32
    )
    cache_scores = jnp.where(in_cache[:, None, :], cache_scores * score_scale, -jnp.inf)
    own_scores = jnp.einsum(
        "shr,sr->sh", latent_query_rows, new_latent, preferred_element_type=jnp.float32
    )
    own_scores = (
        own_scores
        + jnp.einsum("shp,sp->sh", rot_query, new_key, preferred_element_type=jnp.float32)
    ) * score_scale
    peak = jnp.maximum(jnp.max(cache_scores, axis=-1), own_scores)
    cache_exp = jnp.exp(cache_scores - peak[:, :, None])
    own_exp = jnp.exp(own_scores - peak)
    weight_sum = jnp.sum(cache_exp, axis=-1) + own_exp
    cache_probs = (cache_exp / weight_sum[:, :, None]).astype(jnp.bfloat16)
    own_probs = (own_exp / weight_sum).astype(jnp.bfloat16)
    mixed_output = jnp.einsum(
        "shl,slr->shr", cache_probs, latent_cache, preferred_element_type=jnp.float32
    )
    mixed_output = (
        mixed_output
        + own_probs.astype(jnp.float32)[:, :, None] * new_latent.astype(jnp.float32)[:, None, :]
    )
    mixed_output = mixed_output.astype(jnp.bfloat16).reshape(
        sequences_per_device, tensor_split_count, element_count, LATENT_UNITS
    )
    attended_value = lax.all_to_all(mixed_output, "tp", split_axis=1, concat_axis=0, tiled=True)
    attended_value = attended_value.reshape(grouped_rows, heads_per_device, LATENT_UNITS)
    head_output = jnp.einsum(
        "ghr,rhv->ghv",
        attended_value,
        value_up_weight.reshape(LATENT_UNITS, heads_per_device, -1),
        preferred_element_type=jnp.float32,
    )
    head_output = (
        norm_rows(head_output, head_gain.reshape(heads_per_device, -1))
        .astype(jnp.bfloat16)
        .reshape(grouped_rows, -1)
    )
    attention = gathered_total(
        jnp.dot(head_output, w_output, preferred_element_type=jnp.float32).astype(jnp.bfloat16),
        "tp",
    ).astype(jnp.float32)
    middle = (hidden.astype(jnp.float32) + attention).astype(jnp.bfloat16)
    normed_ffn = norm_rows(middle, ffn_gain).astype(jnp.bfloat16)
    exp_dev = w_expert_gate.shape[0]
    n_experts = exp_dev * ep_size
    top_count = expert_ids.shape[1]
    capacity = max(2, grouped_rows * top_count // n_experts + 1)
    flat_ids = expert_ids.reshape(-1)
    matches = (flat_ids[:, None] == jnp.arange(n_experts, dtype=jnp.int32)[None, :]).astype(
        jnp.int32
    )
    slot_index = jnp.sum((jnp.cumsum(matches, axis=0) - matches) * matches, axis=1)
    target = (flat_ids * capacity + slot_index).reshape(grouped_rows, top_count)
    places = jnp.arange(n_experts * capacity, dtype=jnp.int32)
    chosen = places[:, None, None] == target[None, :, :]
    dispatch = jnp.any(chosen, axis=2).astype(jnp.bfloat16)
    combine = jnp.sum(jnp.where(chosen, expert_weights[None, :, :], 0.0), axis=2).T
    sent_rows = jnp.dot(dispatch, normed_ffn, preferred_element_type=jnp.float32).astype(
        jnp.bfloat16
    )
    sent_rows = sent_rows.reshape(ep_size, exp_dev * capacity, MODEL_WIDTH)
    arrived = lax.all_to_all(sent_rows, "ep", split_axis=0, concat_axis=0, tiled=True)
    arrived = arrived.reshape(ep_size, exp_dev, capacity, MODEL_WIDTH)
    gate_pre = jnp.einsum(
        "sjcd,jdf->sjcf", arrived, w_expert_gate, preferred_element_type=jnp.float32
    )
    up_pre = jnp.einsum("sjcd,jdf->sjcf", arrived, w_expert_up, preferred_element_type=jnp.float32)
    expert_act = (jax.nn.silu(gate_pre) * up_pre).astype(jnp.bfloat16)
    expert_part = jnp.einsum(
        "sjcf,jfd->sjcd", expert_act, w_expert_down, preferred_element_type=jnp.float32
    )
    expert_part = expert_part.reshape(-1, MODEL_WIDTH)
    shared_act = (
        jax.nn.silu(jnp.dot(normed_ffn, w_shared_gate, preferred_element_type=jnp.float32))
        * jnp.dot(normed_ffn, w_shared_up, preferred_element_type=jnp.float32)
    ).astype(jnp.bfloat16)
    dense_act = jax.nn.gelu(
        jnp.dot(normed_ffn, w_dense_up, preferred_element_type=jnp.float32)
    ).astype(jnp.bfloat16)
    mix_gate = jax.nn.sigmoid(jnp.dot(normed_ffn, dense_gate, preferred_element_type=jnp.float32))
    side_part = jnp.dot(shared_act, w_shared_down, preferred_element_type=jnp.float32) + mix_gate[
        :, None
    ] * jnp.dot(dense_act, w_dense_down, preferred_element_type=jnp.float32)
    expert_sum, side_sum = side_by_side(
        (expert_part.astype(jnp.bfloat16), side_part.astype(jnp.bfloat16)), "tp", 1, 0
    )
    slot_out = expert_sum.astype(jnp.bfloat16).reshape(ep_size, exp_dev * capacity, -1)
    returned = lax.all_to_all(slot_out, "ep", split_axis=0, concat_axis=0, tiled=True)
    routed = jnp.dot(
        combine,
        returned.reshape(n_experts * capacity, -1).astype(jnp.float32),
        precision=lax.Precision.HIGHEST,
    )
    col_count = side_sum.shape[1]
    own_middle = lax.dynamic_slice_in_dim(middle, tp_index * col_count, col_count, 1)
    return (own_middle.astype(jnp.float32) + routed + side_sum).astype(jnp.bfloat16)


def solution(mesh):
    placed = (
        P("ep", None),
        P(("ep", "tp")),
        P(("ep", "tp"), None, None),
        P(("ep", "tp"), None, None),
        P(),
        P(None, "tp"),
        P(None, "tp"),
        P(),
        P(),
        P(),
        P("tp", None),
        P(None, "tp"),
        P("tp"),
        P("tp", None),
        P(),
        P("ep", None),
        P("ep", None),
        P("ep", None, "tp"),
        P("ep", None, "tp"),
        P("ep", "tp", None),
        P(None, "tp"),
        P(None, "tp"),
        P("tp", None),
        P(None, "tp"),
        P("tp", None),
        P(),
    )
    return jax.shard_map(
        on_device, mesh=mesh, in_specs=placed, out_specs=P("ep", "tp"), check_vma=False
    )
```

profile of v0, /device:TPU:1, one launch (start us, length us, event | category | flops | bytes accessed | tf_op | source)
XLA Modules:
  0.0 196.8 jit_solution(16457032037740585583)
XLA Ops:
  6.5 0.8 convert_element_type.155
  7.4 1.0 fusion.43
  8.4 0.9 fusion.45
  9.3 1.1 fusion.25
  10.3 0.6 copy.67
  11.0 17.3 %all-to-all-start.1 = ((bf16[16,1,1,32]{3,2,1,0:T(2,128)(2,1)}), bf16[16,1,1,32]{3,2,1,0:T(2,128)(2,1)S(1)}, u32[]{:S(2)}, u32[]{:S(2)}) async-start(bf16[16,1,1,32]{3,2,1,0:T(2,128)(2,1)} %copy.67), calls=%async_computation.1 | async-start | bytes 16384 | tf_op jit(solution)/shard_map/all_to_all | solution.py:124
  28.3 0.4 fusion.73
  28.7 0.6 multiply_reduce_fusion.1
  30.8 0.3 fusion.18
  31.3 0.5 broadcast.235
  31.8 0.7 reduce.8
  32.5 0.6 reshape.350
  33.1 2.3 %all-to-all-done.1 = bf16[16,1,1,32]{3,2,1,0:T(2,128)(2,1)S(1)} async-done(((bf16[16,1,1,32]{3,2,1,0:T(2,128)(2,1)}), bf16[16,1,1,32]{3,2,1,0:T(2,128)(2,1)S(1)}, u32[]{:S(2)}, u32[]{:S(2)}) %all-to-all-start.1) | async-done | bytes 1056 | tf_op jit(solution)/shard_map/all_to_all | solution.py:124
  35.4 5.0 %all-to-all-start = ((bf16[16,2,256]{2,1,0:T(2,128)(2,1)}), bf16[16,2,256]{2,1,0:T(2,128)(2,1)S(1)}, u32[]{:S(2)}, u32[]{:S(2)}) async-start(bf16[16,2,256]{2,1,0:T(2,128)(2,1)} %reshape.350), calls=%async_computation | async-start | bytes 32768 | tf_op jit(solution)/shard_map/all_to_all | solution.py:121
  40.4 7.2 %all-to-all-done = bf16[16,2,256]{2,1,0:T(2,128)(2,1)S(1)} async-done(((bf16[16,2,256]{2,1,0:T(2,128)(2,1)}), bf16[16,2,256]{2,1,0:T(2,128)(2,1)S(1)}, u32[]{:S(2)}, u32[]{:S(2)}) %all-to-all-start) | async-done | bytes 16416 | tf_op jit(solution)/shard_map/all_to_all | solution.py:121
  47.8 2.0 %fusion.7 = f32[16,1536]{1,0:T(8,128)S(1)} fusion(bf16[1,1536,512]{2,1,0:T(8,128)(2,1)} %param.28, bf16[16,1,1,512]{3,2,1,0:T(2,128)(2,1)S(1)} %reshape.351), kind=kOutput, calls=%fused_computation.13 | convolution fusion | flops 25165824 | bytes 1687552 | tf_op jit(solution)/shard_map/shr,slr->shl/dot_general | solution.py:131
  49.9 0.3 fusion.127
  50.2 0.2 fusion.128
  50.4 0.2 fusion.48
  50.6 0.4 fusion.19
  51.0 0.7 reduce.9
  51.8 0.6 reshape.352
  52.4 3.7 %all-to-all-start.2 = ((bf16[16,2,256]{2,1,0:T(2,128)(2,1)}), bf16[16,2,256]{2,1,0:T(2,128)(2,1)S(1)}, u32[]{:S(2)}, u32[]{:S(2)}) async-start(bf16[16,2,256]{2,1,0:T(2,128)(2,1)} %reshape.352), calls=%async_computation.2 | async-start | bytes 32768 | tf_op jit(solution)/shard_map/all_to_all | solution.py:161
  56.1 7.3 %all-to-all-done.2 = bf16[16,2,256]{2,1,0:T(2,128)(2,1)S(1)} async-done(((bf16[16,2,256]{2,1,0:T(2,128)(2,1)}), bf16[16,2,256]{2,1,0:T(2,128)(2,1)S(1)}, u32[]{:S(2)}, u32[]{:S(2)}) %all-to-all-start.2) | async-done | bytes 16416 | tf_op jit(solution)/shard_map/all_to_all | solution.py:161
  63.5 0.2 multiply_reduce_fusion
  63.7 0.8 convolution_convert_fusion.2
  65.0 0.2 select_reduce_fusion.1
  65.4 40.0 %all-gather.3.cloned.1.call-done = bf16[256,2048]{1,0:T(8,128)(2,1)} async-done(((bf16[16,2048]{1,0:T(8,128)(2,1)}), bf16[256,2048]{1,0:T(8,128)(2,1)}) %all-gather.3.cloned.1.call-update) | async-done | bytes 1048592 | tf_op jit(solution)/shard_map/all_gather | solution.py:13
  105.5 1.4 convert_reduce_fusion
  107.0 0.3 convolution_convert_fusion.1
  107.4 1.1 reshape.324
  108.5 13.8 %all-to-all-start.3 = ((bf16[64,2,2048]{2,1,0:T(2,128)(2,1)}), bf16[64,2,2048]{2,1,0:T(2,128)(2,1)S(1)}, u32[]{:S(2)}, u32[]{:S(2)}) async-start(bf16[64,2,2048]{2,1,0:T(2,128)(2,1)} %reshape.324), calls=%async_computation.3 | async-start | bytes 1048576 | tf_op jit(solution)/shard_map/all_to_all | solution.py:198
  122.4 0.2 fusion.32
  122.6 1.2 fusion.118
  123.8 1.5 fusion.26
  125.3 1.5 fusion.4
  126.8 13.4 %all-to-all-done.3 = bf16[64,2,2048]{2,1,0:T(2,128)(2,1)S(1)} async-done(((bf16[64,2,2048]{2,1,0:T(2,128)(2,1)}), bf16[64,2,2048]{2,1,0:T(2,128)(2,1)S(1)}, u32[]{:S(2)}, u32[]{:S(2)}) %all-to-all-start.3) | async-done | bytes 524320 | tf_op jit(solution)/shard_map/all_to_all | solution.py:198
  140.2 1.4 convolution_bitcast_fusion.1
  141.5 2.6 %fusion = bf16[64,1,2,2048]{3,0,2,1:T(8,128)(2,1)} fusion(bf16[1,128,2048]{2,1,0:T(8,128)(2,1)} %param.45, bf16[1,2048,128]{2,1,0:T(8,128)(2,1)} %param.44, bf16[64,2,2048]{2,1,0:T(2,128)(2,1)S(1)} %all-to-all-done.3, f32[64,1,2,128]{3,0,2,1:T(8,128)S(1)} %convolution_bitcast_fusion.1), kind=kOutput, calls=%fused_computation.2 | convolution fusion | flops 134578176 | bytes 2162688 | tf_op jit(solution)/shard_map/sjcf,jfd->sjcd/dot_general | solution.py:205
  144.1 1.6 copy.73
  145.7 0.2 convert_element_type.190
  145.9 0.9 bitcast_bitcast_fusion
  146.8 7.1 %all-to-all-start.4 = ((bf16[16,144,128]{2,1,0:T(8,128)(2,1)}), bf16[16,144,128]{2,1,0:T(8,128)(2,1)S(1)}, u32[]{:S(2)}, u32[]{:S(2)}) async-start(bf16[16,144,128]{2,1,0:T(8,128)(2,1)} %bitcast_bitcast_fusion), calls=%async_computation.4 | async-start | bytes 1179648 | tf_op jit(solution)/shard_map/all_to_all | solution.py:23
  153.9 18.5 %all-to-all-done.4 = bf16[16,144,128]{2,1,0:T(8,128)(2,1)S(1)} async-done(((bf16[16,144,128]{2,1,0:T(8,128)(2,1)}), bf16[16,144,128]{2,1,0:T(8,128)(2,1)S(1)}, u32[]{:S(2)}, u32[]{:S(2)}) %all-to-all-start.4) | async-done | bytes 589856 | tf_op jit(solution)/shard_map/all_to_all | solution.py:23
  172.5 0.6 split.13
  173.1 5.2 %all-to-all-start.5 = ((bf16[64,2,128]{2,1,0:T(2,128)(2,1)}), bf16[64,2,128]{2,1,0:T(2,128)(2,1)S(1)}, u32[]{:S(2)}, u32[]{:S(2)}) async-start(bf16[64,2,128]{2,1,0:T(2,128)(2,1)} %bitcast.46), calls=%async_computation.5 | async-start | bytes 65536 | tf_op jit(solution)/shard_map/all_to_all | solution.py:224
  178.4 10.8 %all-to-all-done.5 = bf16[64,2,128]{2,1,0:T(2,128)(2,1)S(1)} async-done(((bf16[64,2,128]{2,1,0:T(2,128)(2,1)}), bf16[64,2,128]{2,1,0:T(2,128)(2,1)S(1)}, u32[]{:S(2)}, u32[]{:S(2)}) %all-to-all-start.5) | async-done | bytes 32800 | tf_op jit(solution)/shard_map/all_to_all | solution.py:224
  189.2 0.7 fusion.24
  (64 shorter events, 1.7 us)
Async XLA Ops:
  6.5 21.7 %copy-start = (bf16[2048,512]{1,0:T(8,128)(2,1)S(1)}, bf16[2048,512]{1,0:T(8,128)(2,1)}, u32[]{:S(2)}) copy-start(bf16[2048,512]{1,0:T(8,128)(2,1)} %param.33) | copy-start | bytes 6291460
  6.5 24.1 %copy-start.6 = (bf16[2048,32]{0,1:T(8,128)(2,1)S(1)}, bf16[2048,32]{0,1:T(8,128)(2,1)}, u32[]{:S(2)}) copy-start(bf16[2048,32]{0,1:T(8,128)(2,1)} %param.34) | copy-start | bytes 393220
  6.5 24.2 %copy-start.14 = (bf16[512]{0:T(512)(128)(2,1)S(1)}, bf16[512]{0:T(512)(128)(2,1)}, u32[]{:S(2)}) copy-start(bf16[512]{0:T(512)(128)(2,1)} %param.35) | copy-start | bytes 3076
  6.5 24.3 %copy-start.4 = (bf16[2048,64]{0,1:T(8,128)(2,1)S(1)}, bf16[2048,64]{0,1:T(8,128)(2,1)}, u32[]{:S(2)}) copy-start(bf16[2048,64]{0,1:T(8,128)(2,1)} %param.31) | copy-start | bytes 786436
  6.5 24.3 %copy-start.8 = (bf16[64,512]{1,0:T(8,128)(2,1)S(1)}, bf16[64,512]{1,0:T(8,128)(2,1)}, u32[]{:S(2)}) copy-start(bf16[64,512]{1,0:T(8,128)(2,1)} %param.36) | copy-start | bytes 196612
  11.0 24.4 %all-to-all-start.1 = ((bf16[16,1,1,32]{3,2,1,0:T(2,128)(2,1)}), bf16[16,1,1,32]{3,2,1,0:T(2,128)(2,1)S(1)}, u32[]{:S(2)}, u32[]{:S(2)}) async-start(bf16[16,1,1,32]{3,2,1,0:T(2,128)(2,1)} %copy.67), calls=%async_computation.1 | async-start | bytes 16384 | tf_op jit(solution)/shard_map/all_to_all | solution.py:124
  28.6 21.2 %copy-start.7 = (bf16[1,32,1536]{2,1,0:T(8,128)(2,1)S(1)}, bf16[1,32,1536]{2,1,0:T(8,128)(2,1)}, u32[]{:S(2)}) copy-start(bf16[1,32,1536]{2,1,0:T(8,128)(2,1)} %param.29) | copy-start | bytes 294916
  35.4 12.3 %all-to-all-start = ((bf16[16,2,256]{2,1,0:T(2,128)(2,1)}), bf16[16,2,256]{2,1,0:T(2,128)(2,1)S(1)}, u32[]{:S(2)}, u32[]{:S(2)}) async-start(bf16[16,2,256]{2,1,0:T(2,128)(2,1)} %reshape.350), calls=%async_computation | async-start | bytes 32768 | tf_op jit(solution)/shard_map/all_to_all | solution.py:121
  47.7 2.9 %copy-start.1 = (bf16[1,1536,512]{2,1,0:T(8,128)(2,1)S(1)}, bf16[1,1536,512]{2,1,0:T(8,128)(2,1)}, u32[]{:S(2)}) copy-start(bf16[1,1536,512]{2,1,0:T(8,128)(2,1)} %param.28) | copy-start | bytes 4718596
  47.8 8.3 %copy-start.15 = (bf16[64]{0:T(256)(128)(2,1)S(1)}, bf16[64]{0:T(256)(128)(2,1)}, u32[]{:S(2)}) copy-start(bf16[64]{0:T(256)(128)(2,1)} %param.38) | copy-start | bytes 388
  49.8 13.6 %copy-start.9 = (bf16[512,64]{0,1:T(8,128)(2,1)S(1)}, bf16[512,64]{0,1:T(8,128)(2,1)}, u32[]{:S(2)}) copy-start(bf16[512,64]{0,1:T(8,128)(2,1)} %param.37) | copy-start | bytes 196612
  49.8 13.9 %copy-start.5 = (bf16[64,2048]{1,0:T(8,128)(2,1)S(1)}, bf16[64,2048]{1,0:T(8,128)(2,1)}, u32[]{:S(2)}) copy-start(bf16[64,2048]{1,0:T(8,128)(2,1)} %param.39) | copy-start | bytes 786436
  49.8 14.8 %copy-start.11 = (bf16[2048]{0:T(1024)(128)(2,1)S(1)}, bf16[2048]{0:T(1024)(128)(2,1)}, u32[]{:S(2)}) copy-start(bf16[2048]{0:T(1024)(128)(2,1)} %param.40) | copy-start | bytes 12292
  49.9 14.8 %copy-start.10 = (s32[16,4]{0,1:T(4,128)S(1)}, s32[16,4]{0,1:T(4,128)}, u32[]{:S(2)}) copy-start(s32[16,4]{0,1:T(4,128)} %param.41) | copy-start | bytes 772
  50.6 56.2 %copy-start.2 = (bf16[16,2048]{1,0:T(8,128)(2,1)S(1)}, bf16[16,2048]{1,0:T(8,128)(2,1)}, u32[]{:S(2)}) copy-start(bf16[16,2048]{1,0:T(8,128)(2,1)} %param.26) | copy-start | bytes 196612
  52.4 11.0 %all-to-all-start.2 = ((bf16[16,2,256]{2,1,0:T(2,128)(2,1)}), bf16[16,2,256]{2,1,0:T(2,128)(2,1)S(1)}, u32[]{:S(2)}, u32[]{:S(2)}) async-start(bf16[16,2,256]{2,1,0:T(2,128)(2,1)} %reshape.352), calls=%async_computation.2 | async-start | bytes 32768 | tf_op jit(solution)/shard_map/all_to_all | solution.py:161
  56.1 49.4 %all-gather.3.cloned.1.call-start = ((), (), s32[]{:S(2)}) async-start(), calls=%async_computation.6 | async-start | bytes 1114112 | tf_op jit(solution)/shard_map/all_gather | solution.py:13
  106.9 15.5 %copy-start.12 = (bf16[2048]{0:T(1024)(128)(2,1)S(1)}, bf16[2048]{0:T(1024)(128)(2,1)}, u32[]{:S(2)}) copy-start(bf16[2048]{0:T(1024)(128)(2,1)} %param.51) | copy-start | bytes 12292
  107.4 17.9 %copy-start.3 = (bf16[128,2048]{1,0:T(8,128)(2,1)S(1)}, bf16[128,2048]{1,0:T(8,128)(2,1)}, u32[]{:S(2)}) copy-start(bf16[128,2048]{1,0:T(8,128)(2,1)} %param.50) | copy-start | bytes 1572868
  108.5 31.6 %all-to-all-start.3 = ((bf16[64,2,2048]{2,1,0:T(2,128)(2,1)}), bf16[64,2,2048]{2,1,0:T(2,128)(2,1)S(1)}, u32[]{:S(2)}, u32[]{:S(2)}) async-start(bf16[64,2,2048]{2,1,0:T(2,128)(2,1)} %reshape.324), calls=%async_computation.3 | async-start | bytes 1048576 | tf_op jit(solution)/shard_map/all_to_all | solution.py:198
  145.9 32.4 %copy-start.13 = (f32[16,4]{0,1:T(4,128)S(1)}, f32[16,4]{0,1:T(4,128)}, u32[]{:S(2)}) copy-start(f32[16,4]{0,1:T(4,128)} %param.42) | copy-start | bytes 772
  146.8 25.6 %all-to-all-start.4 = ((bf16[16,144,128]{2,1,0:T(8,128)(2,1)}), bf16[16,144,128]{2,1,0:T(8,128)(2,1)S(1)}, u32[]{:S(2)}, u32[]{:S(2)}) async-start(bf16[16,144,128]{2,1,0:T(8,128)(2,1)} %bitcast_bitcast_fusion), calls=%async_computation.4 | async-start | bytes 1179648 | tf_op jit(solution)/shard_map/all_to_all | solution.py:23
  173.1 16.1 %all-to-all-start.5 = ((bf16[64,2,128]{2,1,0:T(2,128)(2,1)}), bf16[64,2,128]{2,1,0:T(2,128)(2,1)S(1)}, u32[]{:S(2)}, u32[]{:S(2)}) async-start(bf16[64,2,128]{2,1,0:T(2,128)(2,1)} %bitcast.46), calls=%async_computation.5 | async-start | bytes 65536 | tf_op jit(solution)/shard_map/all_to_all | solution.py:224
Sparse Core Ops, SparseCore 0:
  64.7 40.7 all-gather.2
where the time goes:
time: 198 us; the launch traced here: 197 us
  waiting for transfers between devices  99.6 us (50%)
  starting transfers between devices  52.1 us (26%)
  matrix products  15.3 us (8%)
  between operations  15.1 us (8%)
  other arithmetic  8.32 us (4%)
  local copies, waits for them, and re-layouts  6.36 us (3%)
    all_gather x1, waiting for transfers between devices, gathered_total(): return lax.all_gather(x, axis).astype(jnp.float32).sum(0)  40 us
    all_to_all x1, waiting for transfers between devices, summed_on_arrival(): lax.all_to_all(tiles, axis, split_axis=0, concat_axis=0, tiled=True)  18.5 us
    all_to_all x1, starting transfers between devices, on_device(): lax.all_to_all(query_rope, 'tp', split_axis=0, concat_axis=1, tiled=True)  17.3 us
    all_to_all x1, starting transfers between devices, on_device(): lax.all_to_all(sent_rows, 'ep', split_axis=0, concat_axis=0, tiled=True)  13.8 us
    all_to_all x1, waiting for transfers between devices, on_device(): lax.all_to_all(sent_rows, 'ep', split_axis=0, concat_axis=0, tiled=True)  13.4 us
    all_to_all x1, waiting for transfers between devices, on_device(): lax.all_to_all(slot_out, 'ep', split_axis=0, concat_axis=0, tiled=True)  10.8 us
    all_to_all x1, waiting for transfers between devices, on_device(): lax.all_to_all(mixed_output, 'tp', split_axis=1, concat_axis=0, tiled=True)  7.31 us
    all_to_all x1, waiting for transfers between devices, on_device(): lax.all_to_all(query_in_latent, 'tp', split_axis=0, concat_axis=1, tiled=...  7.25 us
  transfers between devices with their start and end apart: 7, of which 7 were waited for; matrix products, arithmetic and copies ran while one was open for 4% of the time, Pallas kernels for 0%

commit v1 on v0

v1 whole, which is shorter than its diff:
```python
import jax
import jax.numpy as jnp
from jax import lax
from jax.sharding import PartitionSpec as P

MODEL_WIDTH = 2048
PLAIN_QUERY = 64
ROPE = 32
LATENT_UNITS = 512
CAP = 2


def exchange(x, axis):
    return lax.all_to_all(x, axis, split_axis=0, concat_axis=0, tiled=True)


def column_tiles(x, peers):
    rows, cols = x.shape
    return jnp.swapaxes(x.reshape(rows, peers, cols // peers), 0, 1)


def norm_rows(values, gains):
    values = values.astype(jnp.float32)
    factor = lax.rsqrt(jnp.mean(values * values, axis=-1, keepdims=True) + 1e-06)
    return values * factor * gains.astype(jnp.float32)


def angles_at(positions, rot_width):
    half_width = rot_width // 2
    inverse = 1.0 / 10000.0 ** (jnp.arange(half_width, dtype=jnp.float32) / half_width)
    return positions.astype(jnp.float32)[..., None] * inverse


def rotate(values, angles):
    half_width = values.shape[-1] // 2
    first = values[..., :half_width]
    second = values[..., half_width:]
    cosines = jnp.cos(angles)
    sines = jnp.sin(angles)
    return jnp.concatenate(
        [first * cosines - second * sines, first * sines + second * cosines], axis=-1
    )


def three_parts(values):
    parts = []
    for _ in range(3):
        part = lax.reduce_precision(values, 8, 7)
        parts.append(part.astype(jnp.bfloat16))
        values = values - part
    return parts


def dot32(a, b):
    return jnp.dot(a, b, preferred_element_type=jnp.float32)


def on_device(
    hidden,
    lengths,
    latent_cache,
    cache_rotary,
    attn_gain,
    w_query_nope,
    w_query_rope,
    latent_weight,
    w_rotary_key,
    latent_norm_gain,
    key_up_weight,
    value_up_weight,
    head_gain,
    w_output,
    ffn_gain,
    expert_ids,
    expert_weights,
    w_expert_gate,
    w_expert_up,
    w_expert_down,
    w_shared_gate,
    w_shared_up,
    w_shared_down,
    w_dense_up,
    w_dense_down,
    dense_gate,
):
    tp = lax.axis_size("tp")
    ep = lax.axis_size("ep")
    tp_index = lax.axis_index("tp")
    rows = hidden.shape[0]
    cols = MODEL_WIDTH // tp

    flat_ids = expert_ids.reshape(-1)
    matches = (flat_ids[:, None] == jnp.arange(ep, dtype=jnp.int32)[None, :]).astype(jnp.int32)
    slot_index = jnp.sum((jnp.cumsum(matches, axis=0) - matches) * matches, axis=1)
    target = (flat_ids * CAP + slot_index).reshape(rows, -1)
    places = jnp.arange(ep * CAP, dtype=jnp.int32)
    chosen = places[:, None, None] == target[None, :, :]
    dispatch = jnp.any(chosen, axis=2).astype(jnp.bfloat16)
    combine = jnp.sum(jnp.where(chosen, expert_weights[None, :, :], 0.0), axis=2).T
    combine_parts = jnp.concatenate(three_parts(combine), axis=0)

    normed = norm_rows(hidden, attn_gain).astype(jnp.bfloat16)
    query_nope = dot32(normed, w_query_nope).astype(jnp.bfloat16)
    query_rope = dot32(normed, w_query_rope).astype(jnp.bfloat16)
    query_latent = dot32(query_nope, key_up_weight).astype(jnp.bfloat16)
    queries = exchange(jnp.concatenate([query_latent, query_rope], axis=1), "tp")

    own_row = lax.dynamic_slice_in_dim(normed, tp_index, 1, 0)
    angles = angles_at(lengths, ROPE)
    new_latent = norm_rows(dot32(own_row, latent_weight), latent_norm_gain).astype(jnp.bfloat16)
    new_key = rotate(dot32(own_row, w_rotary_key), angles).astype(jnp.bfloat16)

    query_rows = queries[:, :LATENT_UNITS]
    rot_query = rotate(queries[:, LATENT_UNITS:].astype(jnp.float32), angles).astype(jnp.bfloat16)
    latents = latent_cache[0]
    in_cache = jnp.arange(latents.shape[0], dtype=jnp.int32) < lengths[0]
    score_scale = (PLAIN_QUERY + ROPE) ** (-0.5)
    cache_scores = jnp.einsum("hr,lr->hl", query_rows, latents, preferred_element_type=jnp.float32)
    cache_scores = cache_scores + dot32(rot_query, cache_rotary[0])
    cache_scores = jnp.where(in_cache[None, :], cache_scores * score_scale, -jnp.inf)
    own_scores = jnp.sum(
        query_rows.astype(jnp.float32) * new_latent.astype(jnp.float32), axis=1
    ) + jnp.sum(rot_query.astype(jnp.float32) * new_key.astype(jnp.float32), axis=1)
    own_scores = own_scores * score_scale
    peak = jnp.maximum(jnp.max(cache_scores, axis=-1), own_scores)
    cache_exp = jnp.exp(cache_scores - peak[:, None])
    own_exp = jnp.exp(own_scores - peak)
    weight_sum = jnp.sum(cache_exp, axis=-1) + own_exp
    cache_probs = (cache_exp / weight_sum[:, None]).astype(jnp.bfloat16)
    own_probs = (own_exp / weight_sum).astype(jnp.bfloat16)
    attended = dot32(cache_probs, latents) + own_probs.astype(jnp.float32)[
        :, None
    ] * new_latent.astype(jnp.float32)
    attended = exchange(attended.astype(jnp.bfloat16), "tp")

    head_out = norm_rows(dot32(attended, value_up_weight), head_gain).astype(jnp.bfloat16)
    share = dot32(head_out, w_output).astype(jnp.bfloat16)
    attention = exchange(column_tiles(share, tp), "tp").astype(jnp.float32).sum(axis=0)
    own_hidden = lax.dynamic_slice_in_dim(hidden, tp_index * cols, cols, 1)
    own_middle = (own_hidden.astype(jnp.float32) + attention).astype(jnp.bfloat16)
    tiles = exchange(jnp.broadcast_to(own_middle[None], (tp, rows, cols)), "tp")
    middle = jnp.swapaxes(tiles, 0, 1).reshape(rows, MODEL_WIDTH)
    normed_ffn = norm_rows(middle, ffn_gain).astype(jnp.bfloat16)

    sent = dot32(dispatch, normed_ffn).astype(jnp.bfloat16).reshape(ep, CAP, MODEL_WIDTH)
    arrived = exchange(sent, "ep").reshape(ep * CAP, MODEL_WIDTH)
    expert_act = jax.nn.silu(dot32(arrived, w_expert_gate[0])) * dot32(arrived, w_expert_up[0])
    part = dot32(expert_act.astype(jnp.bfloat16), w_expert_down[0]).astype(jnp.bfloat16)
    returned = exchange(part.reshape(ep, CAP, MODEL_WIDTH), "ep").reshape(ep * CAP, MODEL_WIDTH)

    shared_act = (
        jax.nn.silu(dot32(normed_ffn, w_shared_gate)) * dot32(normed_ffn, w_shared_up)
    ).astype(jnp.bfloat16)
    dense_act = jax.nn.gelu(dot32(normed_ffn, w_dense_up)).astype(jnp.bfloat16)
    mix_gate = jax.nn.sigmoid(dot32(normed_ffn, dense_gate))
    side_part = dot32(shared_act, w_shared_down) + mix_gate[:, None] * dot32(
        dense_act, w_dense_down
    )

    routed_part = dot32(combine_parts, returned).reshape(3, rows, MODEL_WIDTH).sum(axis=0)
    total = (routed_part + side_part).astype(jnp.bfloat16)
    total = exchange(column_tiles(total, tp), "tp").astype(jnp.float32).sum(axis=0)
    return (own_middle.astype(jnp.float32) + total).astype(jnp.bfloat16)


def solution(mesh):
    placed = (
        P("ep", None),
        P(("ep", "tp")),
        P(("ep", "tp"), None, None),
        P(("ep", "tp"), None, None),
        P(),
        P(None, "tp"),
        P(None, "tp"),
        P(),
        P(),
        P(),
        P("tp", None),
        P(None, "tp"),
        P("tp"),
        P("tp", None),
        P(),
        P("ep", None),
        P("ep", None),
        P("ep", None, "tp"),
        P("ep", None, "tp"),
        P("ep", "tp", None),
        P(None, "tp"),
        P(None, "tp"),
        P("tp", None),
        P(None, "tp"),
        P("tp", None),
        P(),
    )
    return jax.shard_map(
        on_device, mesh=mesh, in_specs=placed, out_specs=P("ep", "tp"), check_vma=False
    )
```

time: 198 us -> 152 us (0.77)
  waiting for transfers between devices: 99.6 us -> 58.6 us
  blocking collectives: 0 us -> 14.2 us
  between operations: 15.1 us -> 1.73 us
  starting transfers between devices: 52.1 us -> 48.5 us
    all_gather x1 -> x0, waiting for transfers between devices: 40 us -> none  [gathered_total(): return lax.all_gather(x, axis).astype(jnp.float32).sum(0)]
    all_to_all x0 -> x1, blocking collectives: none -> 14.2 us  [exchange(): return lax.all_to_all(x, axis, split_axis=0, concat_axis=0, tiled=True)]
    all_to_all x6, starting transfers between devices: 52.1 us -> 48.5 us  [exchange(): return lax.all_to_all(x, axis, split_axis=0, concat_axis=0, tiled=True)]
    dot_general x19 -> x17, matrix products: 15.3 us -> 13.7 us  [the longest x16 11.7 us: dot32(): return jnp.dot(a, b, preferred_element_type=jnp.float32)]
  transfers between devices with their start and end apart: 7 -> 6, of which waited for: 7 -> 6; matrix products, arithmetic and copies ran while one was open for 4% -> 3% of each run, Pallas kernels for 0% -> 0%
where the time goes in v1:
time: 152 us; the launch traced here: 151 us
  waiting for transfers between devices  58.6 us (39%)
  starting transfers between devices  48.5 us (32%)
  blocking collectives  14.2 us (9%)
  matrix products  13.7 us (9%)
  other arithmetic  7.69 us (5%)
  local copies, waits for them, and re-layouts  6.31 us (4%)
  between operations  1.73 us (1%)
    all_to_all x6, waiting for transfers between devices, exchange(): return lax.all_to_all(x, axis, split_axis=0, concat_axis=0, tiled=True)  58.6 us
    all_to_all x6, starting transfers between devices, exchange(): return lax.all_to_all(x, axis, split_axis=0, concat_axis=0, tiled=True)  48.5 us
    all_to_all x1, blocking collectives, exchange(): return lax.all_to_all(x, axis, split_axis=0, concat_axis=0, tiled=True)  14.2 us
    dot_general x16, matrix products, dot32(): return jnp.dot(a, b, preferred_element_type=jnp.float32)  11.7 us
  transfers between devices with their start and end apart: 6, of which 6 were waited for; matrix products, arithmetic and copies ran while one was open for 3% of the time, Pallas kernels for 0%

profile of v1, /device:TPU:1, one launch (start us, length us, event | category | flops | bytes accessed | tf_op | source)
XLA Modules:
  0.0 150.7 jit_solution(12148689820694784172)
XLA Ops:
  0.0 0.8 convert_element_type.156
  0.8 1.0 fusion.32
  1.8 0.9 fusion.34
  2.8 1.1 convolution_convert_fusion.4
  3.8 1.2 convolution_convert_fusion.3
  5.1 0.5 broadcast.197
  5.6 0.7 reduce.4
  6.3 0.7 reshape.193
  7.0 17.4 %all-to-all-start = ((bf16[16,2,272]{2,1,0:T(2,128)(2,1)}), bf16[16,2,272]{2,1,0:T(2,128)(2,1)S(1)}, u32[]{:S(2)}, u32[]{:S(2)}) async-start(bf16[16,2,272]{2,1,0:T(2,128)(2,1)} %reshape.193), calls=%async_computation | async-start | bytes 49152 | tf_op jit(solution)/shard_map/all_to_all | solution.py:14
  25.1 1.1 fusion.64
  26.3 0.4 fusion.66
  26.6 0.6 multiply_reduce_fusion.3
  28.0 3.8 %all-to-all-done = bf16[16,2,272]{2,1,0:T(2,128)(2,1)S(1)} async-done(((bf16[16,2,272]{2,1,0:T(2,128)(2,1)}), bf16[16,2,272]{2,1,0:T(2,128)(2,1)S(1)}, u32[]{:S(2)}, u32[]{:S(2)}) %all-to-all-start) | async-done | bytes 17440 | tf_op jit(solution)/shard_map/all_to_all | solution.py:14
  32.0 2.0 %fusion.7 = f32[16,1536]{1,0:T(8,128)S(1)} fusion(bf16[1,1536,512]{2,1,0:T(8,128)(2,1)} %param.28, bf16[16,544]{1,0:T(8,128)(2,1)S(1)} %bitcast.123), kind=kOutput, calls=%fused_computation.12 | convolution fusion | flops 25165824 | bytes 1687552 | tf_op jit(solution)/shard_map/hr,lr->hl/dot_general | solution.py:118
  34.3 0.2 multiply_reduce_fusion.2
  34.5 0.3 fusion.98
  34.8 0.2 fusion.39
  35.0 0.4 fusion.18
  35.4 0.7 reduce.5
  36.1 0.6 reshape.195
  36.7 3.7 %all-to-all-start.1 = ((bf16[16,2,256]{2,1,0:T(2,128)(2,1)}), bf16[16,2,256]{2,1,0:T(2,128)(2,1)S(1)}, u32[]{:S(2)}, u32[]{:S(2)}) async-start(bf16[16,2,256]{2,1,0:T(2,128)(2,1)} %reshape.195), calls=%async_computation.1 | async-start | bytes 32768 | tf_op jit(solution)/shard_map/all_to_all | solution.py:14
  40.5 7.2 %all-to-all-done.1 = bf16[16,2,256]{2,1,0:T(2,128)(2,1)S(1)} async-done(((bf16[16,2,256]{2,1,0:T(2,128)(2,1)}), bf16[16,2,256]{2,1,0:T(2,128)(2,1)S(1)}, u32[]{:S(2)}, u32[]{:S(2)}) %all-to-all-start.1) | async-done | bytes 16416 | tf_op jit(solution)/shard_map/all_to_all | solution.py:14
  47.7 0.2 multiply_reduce_fusion.1
  48.0 0.2 fusion.9
  48.2 0.7 copy.80
  48.9 3.7 %all-to-all-start.2 = ((bf16[16,16,128]{2,1,0:T(8,128)(2,1)}), bf16[16,16,128]{2,1,0:T(8,128)(2,1)S(1)}, u32[]{:S(2)}, u32[]{:S(2)}) async-start(bf16[16,16,128]{2,1,0:T(8,128)(2,1)} %bitcast.118), calls=%async_computation.2 | async-start | bytes 131072 | tf_op jit(solution)/shard_map/all_to_all | solution.py:14
  53.1 7.3 %all-to-all-done.2 = bf16[16,16,128]{2,1,0:T(8,128)(2,1)S(1)} async-done(((bf16[16,16,128]{2,1,0:T(8,128)(2,1)}), bf16[16,16,128]{2,1,0:T(8,128)(2,1)S(1)}, u32[]{:S(2)}, u32[]{:S(2)}) %all-to-all-start.2) | async-done | bytes 65568 | tf_op jit(solution)/shard_map/all_to_all | solution.py:14
  60.4 0.7 add_convert_fusion.1
  61.1 0.6 broadcast_in_dim.30
  61.7 3.4 %all-to-all-start.3 = ((bf16[16,16,128]{2,1,0:T(8,128)(2,1)}), bf16[16,16,128]{2,1,0:T(8,128)(2,1)S(1)}, u32[]{:S(2)}, u32[]{:S(2)}) async-start(bf16[16,16,128]{2,1,0:T(8,128)(2,1)} %broadcast_in_dim.30), calls=%async_computation.3 | async-start | bytes 131072 | tf_op jit(solution)/shard_map/all_to_all | solution.py:14
  65.3 7.7 %all-to-all-done.3 = bf16[16,16,128]{2,1,0:T(8,128)(2,1)S(1)} async-done(((bf16[16,16,128]{2,1,0:T(8,128)(2,1)}), bf16[16,16,128]{2,1,0:T(8,128)(2,1)S(1)}, u32[]{:S(2)}, u32[]{:S(2)}) %all-to-all-start.3) | async-done | bytes 65568 | tf_op jit(solution)/shard_map/all_to_all | solution.py:14
  73.2 0.3 convolution_convert_fusion.1
  73.6 1.1 reshape.177
  74.7 13.9 %all-to-all-start.4 = ((bf16[64,2,2048]{2,1,0:T(2,128)(2,1)}), bf16[64,2,2048]{2,1,0:T(2,128)(2,1)S(1)}, u32[]{:S(2)}, u32[]{:S(2)}) async-start(bf16[64,2,2048]{2,1,0:T(2,128)(2,1)} %reshape.177), calls=%async_computation.4 | async-start | bytes 1048576 | tf_op jit(solution)/shard_map/all_to_all | solution.py:14
  88.7 17.7 %all-to-all-done.4 = bf16[64,2,2048]{2,1,0:T(2,128)(2,1)S(1)} async-done(((bf16[64,2,2048]{2,1,0:T(2,128)(2,1)}), bf16[64,2,2048]{2,1,0:T(2,128)(2,1)S(1)}, u32[]{:S(2)}, u32[]{:S(2)}) %all-to-all-start.4) | async-done | bytes 524320 | tf_op jit(solution)/shard_map/all_to_all | solution.py:14
  106.4 0.2 reshape.178
  106.6 1.3 fusion.30
  108.0 1.7 %convolution_convert_fusion = bf16[128,2048]{1,0:T(8,128)(2,1)S(1)} fusion(bf16[128,2048]{1,0:T(8,128)(2,1)S(1)} %reshape.178, bf16[1,128,2048]{2,1,0:T(8,128)(2,1)} %param.45, bf16[1,2048,128]{2,1,0:T(8,128)(2,1)} %param.44, f32[128,128]{1,0:T(8,128)S(1)} %fusion.30), kind=kOutput, calls=%fused_computation | convolution fusion | flops 134578176 | bytes 2162688 | tf_op jit(solution)/shard_map/dot_general | solution.py:55
  109.7 1.1 reshape.179
  110.9 6.4 %all-to-all-start.5 = ((bf16[64,2,2048]{2,1,0:T(2,128)(2,1)}), bf16[64,2,2048]{2,1,0:T(2,128)(2,1)S(1)}, u32[]{:S(2)}, u32[]{:S(2)}) async-start(bf16[64,2,2048]{2,1,0:T(2,128)(2,1)} %reshape.179), calls=%async_computation.5 | async-start | bytes 1048576 | tf_op jit(solution)/shard_map/all_to_all | solution.py:14
  117.5 0.2 fusion.101
  117.6 1.3 fusion.22
  119.0 14.9 %all-to-all-done.5 = bf16[64,2,2048]{2,1,0:T(2,128)(2,1)S(1)} async-done(((bf16[64,2,2048]{2,1,0:T(2,128)(2,1)}), bf16[64,2,2048]{2,1,0:T(2,128)(2,1)S(1)}, u32[]{:S(2)}, u32[]{:S(2)}) %all-to-all-start.5) | async-done | bytes 524320 | tf_op jit(solution)/shard_map/all_to_all | solution.py:14
  133.9 0.2 reshape.187
  134.1 0.2 convolution_reduce_fusion
  134.3 1.6 %fusion.10 = bf16[2,16,8,128]{3,2,1,0:T(8,128)(2,1)S(1)} fusion(f32[16,2048]{1,0:T(8,128)S(1)} %convolution_reduce_fusion, f32[16,2048]{1,0:T(8,128)S(1)} %fusion.22, bf16[128,2048]{1,0:T(8,128)(2,1)} %param.50, f32[16]{0:T(128)S(1)} %fusion.26, bf16[16,2048]{1,0:T(8,128)(2,1)S(1)} %fusion.37, bf16[2048,128]{1,0:T(8,128)(2,1)} %param.49), kind=kOutput, calls=%fused_computation.16 | convolution fusion | flops 16926720 | bytes 1441856 | tf_op jit(solution)/shard_map/dot_general | solution.py:55
  135.9 14.2 %all_to_all.49 = bf16[16,16,128]{2,1,0:T(8,128)(2,1)S(1)} all-to-all(bf16[16,16,128]{2,1,0:T(8,128)(2,1)S(1)} %bitcast.121), channel_id=1, replica_groups=mesh['ep'=64,'tp'=16] {'tp'}, dimensions={0} | all-to-all | bytes 131072 | tf_op jit(solution)/shard_map/all_to_all | solution.py:14
  150.1 0.6 add_convert_fusion
  (64 shorter events, 2.0 us)
Async XLA Ops:
  0.0 26.2 %copy-start = (bf16[2048,512]{1,0:T(8,128)(2,1)S(1)}, bf16[2048,512]{1,0:T(8,128)(2,1)}, u32[]{:S(2)}) copy-start(bf16[2048,512]{1,0:T(8,128)(2,1)} %param.33) | copy-start | bytes 6291460
  1.8 26.1 %copy-start.11 = (bf16[512]{0:T(512)(128)(2,1)S(1)}, bf16[512]{0:T(512)(128)(2,1)}, u32[]{:S(2)}) copy-start(bf16[512]{0:T(512)(128)(2,1)} %param.35) | copy-start | bytes 3076
  7.0 24.9 %all-to-all-start = ((bf16[16,2,272]{2,1,0:T(2,128)(2,1)}), bf16[16,2,272]{2,1,0:T(2,128)(2,1)S(1)}, u32[]{:S(2)}, u32[]{:S(2)}) async-start(bf16[16,2,272]{2,1,0:T(2,128)(2,1)} %reshape.193), calls=%async_computation | async-start | bytes 49152 | tf_op jit(solution)/shard_map/all_to_all | solution.py:14
  26.2 8.2 %copy-start.5 = (bf16[1,32,1536]{2,1,0:T(8,128)(2,1)S(1)}, bf16[1,32,1536]{2,1,0:T(8,128)(2,1)}, u32[]{:S(2)}) copy-start(bf16[1,32,1536]{2,1,0:T(8,128)(2,1)} %param.29) | copy-start | bytes 294916
  32.0 3.1 %copy-start.1 = (bf16[1,1536,512]{2,1,0:T(8,128)(2,1)S(1)}, bf16[1,1536,512]{2,1,0:T(8,128)(2,1)}, u32[]{:S(2)}) copy-start(bf16[1,1536,512]{2,1,0:T(8,128)(2,1)} %param.28) | copy-start | bytes 4718596
  32.0 8.3 %copy-start.12 = (bf16[64]{0:T(256)(128)(2,1)S(1)}, bf16[64]{0:T(256)(128)(2,1)}, u32[]{:S(2)}) copy-start(bf16[64]{0:T(256)(128)(2,1)} %param.38) | copy-start | bytes 388
  32.0 8.3 %copy-start.7 = (s32[16,4]{0,1:T(4,128)S(1)}, s32[16,4]{0,1:T(4,128)}, u32[]{:S(2)}) copy-start(s32[16,4]{0,1:T(4,128)} %param.41) | copy-start | bytes 772
  34.0 13.7 %copy-start.6 = (bf16[512,64]{0,1:T(8,128)(2,1)S(1)}, bf16[512,64]{0,1:T(8,128)(2,1)}, u32[]{:S(2)}) copy-start(bf16[512,64]{0,1:T(8,128)(2,1)} %param.37) | copy-start | bytes 196612
  34.1 13.9 %copy-start.2 = (bf16[64,2048]{1,0:T(8,128)(2,1)S(1)}, bf16[64,2048]{1,0:T(8,128)(2,1)}, u32[]{:S(2)}) copy-start(bf16[64,2048]{1,0:T(8,128)(2,1)} %param.39) | copy-start | bytes 786436
  34.8 30.4 %copy-start.8 = (bf16[2048]{0:T(1024)(128)(2,1)S(1)}, bf16[2048]{0:T(1024)(128)(2,1)}, u32[]{:S(2)}) copy-start(bf16[2048]{0:T(1024)(128)(2,1)} %param.40) | copy-start | bytes 12292
  36.7 11.0 %all-to-all-start.1 = ((bf16[16,2,256]{2,1,0:T(2,128)(2,1)}), bf16[16,2,256]{2,1,0:T(2,128)(2,1)S(1)}, u32[]{:S(2)}, u32[]{:S(2)}) async-start(bf16[16,2,256]{2,1,0:T(2,128)(2,1)} %reshape.195), calls=%async_computation.1 | async-start | bytes 32768 | tf_op jit(solution)/shard_map/all_to_all | solution.py:14
  48.9 11.5 %all-to-all-start.2 = ((bf16[16,16,128]{2,1,0:T(8,128)(2,1)}), bf16[16,16,128]{2,1,0:T(8,128)(2,1)S(1)}, u32[]{:S(2)}, u32[]{:S(2)}) async-start(bf16[16,16,128]{2,1,0:T(8,128)(2,1)} %bitcast.118), calls=%async_computation.2 | async-start | bytes 131072 | tf_op jit(solution)/shard_map/all_to_all | solution.py:14
  60.4 28.2 %copy-start.9 = (bf16[2048]{0:T(1024)(128)(2,1)S(1)}, bf16[2048]{0:T(1024)(128)(2,1)}, u32[]{:S(2)}) copy-start(bf16[2048]{0:T(1024)(128)(2,1)} %param.51) | copy-start | bytes 12292
  60.4 28.3 %copy-start.10 = (f32[16,4]{0,1:T(4,128)S(1)}, f32[16,4]{0,1:T(4,128)}, u32[]{:S(2)}) copy-start(f32[16,4]{0,1:T(4,128)} %param.42) | copy-start | bytes 772
  61.7 11.3 %all-to-all-start.3 = ((bf16[16,16,128]{2,1,0:T(8,128)(2,1)}), bf16[16,16,128]{2,1,0:T(8,128)(2,1)S(1)}, u32[]{:S(2)}, u32[]{:S(2)}) async-start(bf16[16,16,128]{2,1,0:T(8,128)(2,1)} %broadcast_in_dim.30), calls=%async_computation.3 | async-start | bytes 131072 | tf_op jit(solution)/shard_map/all_to_all | solution.py:14
  74.7 31.7 %all-to-all-start.4 = ((bf16[64,2,2048]{2,1,0:T(2,128)(2,1)}), bf16[64,2,2048]{2,1,0:T(2,128)(2,1)S(1)}, u32[]{:S(2)}, u32[]{:S(2)}) async-start(bf16[64,2,2048]{2,1,0:T(2,128)(2,1)} %reshape.177), calls=%async_computation.4 | async-start | bytes 1048576 | tf_op jit(solution)/shard_map/all_to_all | solution.py:14
  109.7 7.8 %copy-start.3 = (bf16[2048,64]{0,1:T(8,128)(2,1)S(1)}, bf16[2048,64]{0,1:T(8,128)(2,1)}, u32[]{:S(2)}) copy-start(bf16[2048,64]{0,1:T(8,128)(2,1)} %param.46) | copy-start | bytes 786436
  109.7 7.9 %copy-start.4 = (bf16[64,2048]{1,0:T(8,128)(2,1)S(1)}, bf16[64,2048]{1,0:T(8,128)(2,1)}, u32[]{:S(2)}) copy-start(bf16[64,2048]{1,0:T(8,128)(2,1)} %param.48) | copy-start | bytes 786436
  110.9 23.1 %all-to-all-start.5 = ((bf16[64,2,2048]{2,1,0:T(2,128)(2,1)}), bf16[64,2,2048]{2,1,0:T(2,128)(2,1)S(1)}, u32[]{:S(2)}, u32[]{:S(2)}) async-start(bf16[64,2,2048]{2,1,0:T(2,128)(2,1)} %reshape.179), calls=%async_computation.5 | async-start | bytes 1048576 | tf_op jit(solution)/shard_map/all_to_all | solution.py:14

commit v2 on v1

v2 whole, which is shorter than its diff:
```python
import jax
import jax.numpy as jnp
from jax import lax
from jax.experimental import pallas as pl
from jax.experimental.pallas import tpu as pltpu
from jax.sharding import PartitionSpec as P

MODEL_WIDTH = 2048
PLAIN_QUERY = 64
ROPE = 32
HALF = 16
LATENT_UNITS = 512
CAP = 2
LANES = 128
F32 = jnp.float32
BF16 = jnp.bfloat16
EPS = 1e-06


def exchange(x, axis):
    return lax.all_to_all(x, axis, split_axis=0, concat_axis=0, tiled=True)


def dot32(a, b):
    return jnp.dot(a, b, preferred_element_type=F32)


def dot_t(a, b):
    return lax.dot_general(a, b, (((1,), (1,)), ((), ())), preferred_element_type=F32)


def call(body, outs, args, smem=(), scratch=()):
    vmem = pl.BlockSpec(memory_space=pltpu.VMEM)
    in_specs = [
        pl.BlockSpec(memory_space=pltpu.SMEM) if i in smem else vmem for i in range(len(args))
    ]
    return pl.pallas_call(
        body,
        out_shape=outs,
        in_specs=in_specs,
        out_specs=jax.tree.map(lambda _: vmem, outs),
        scratch_shapes=list(scratch),
    )(*args)


def shape(dims, dtype):
    return jax.ShapeDtypeStruct(dims, dtype)


def query_body(hidden, gain, w_nope, w_rope, key_up, out, normed_out):
    values = hidden[...].astype(F32)
    factor = lax.rsqrt(jnp.mean(values * values, axis=-1, keepdims=True) + EPS)
    normed = (values * factor * gain[...]).astype(BF16)
    normed_out[...] = normed
    nope = dot_t(normed, w_nope[...]).astype(BF16)
    rope = dot_t(normed, w_rope[...]).astype(BF16).astype(F32)
    latent = dot32(nope, key_up[...]).astype(BF16).astype(F32)
    for s in range(LATENT_UNITS // LANES):
        out[:, s, :] = latent[:, s * LANES : (s + 1) * LANES]
    rows = out.shape[0]
    out[:, 4, :] = jnp.concatenate([rope, jnp.zeros((rows, LANES - ROPE), F32)], axis=1)
    for s in range(5, 8):
        out[:, s, :] = jnp.zeros((rows, LANES), F32)


def rotated(values, cos, sin):
    first, second = values[:, :HALF], values[:, HALF:ROPE]
    return jnp.concatenate([first * cos - second * sin, first * sin + second * cos], axis=1)


def new_token_body(index, normed, w_latent, w_key, gain, cos, sin, latent_out, key_out):
    latent = dot32(normed[...], w_latent[...])
    key = dot_t(normed[...], w_key[...])
    rows = lax.broadcasted_iota(jnp.int32, (latent.shape[0], 1), 0)
    mine = rows == index[0]
    latent = jnp.sum(jnp.where(mine, latent, 0.0), axis=0, keepdims=True)
    key = jnp.sum(jnp.where(mine, key, 0.0), axis=0, keepdims=True)
    factor = lax.rsqrt(jnp.mean(latent * latent, axis=-1, keepdims=True) + EPS)
    latent_out[...] = (latent * factor * gain[...]).astype(BF16).astype(F32)
    key_out[...] = rotated(key, cos[...], sin[...]).astype(BF16).astype(F32)


def attention_body(lengths, queries, latents, rotary, new_latent, new_key, cos, sin, out):
    parts = [queries[:, s, :] for s in range(LATENT_UNITS // LANES)]
    query = jnp.concatenate(parts, axis=1)
    rope = rotated(queries[:, 4, :], cos[...], sin[...]).astype(BF16)
    scale = (PLAIN_QUERY + ROPE) ** (-0.5)
    cache = latents[0]
    scores = dot_t(query.astype(BF16), cache) + dot32(rope, rotary[0])
    place = lax.broadcasted_iota(jnp.int32, scores.shape, 1)
    scores = jnp.where(place < lengths[0], scores * scale, -jnp.inf)
    own = jnp.sum(query * new_latent[...], axis=1, keepdims=True)
    own = own + jnp.sum(rope.astype(F32) * new_key[...], axis=1, keepdims=True)
    own = own * scale
    peak = jnp.maximum(jnp.max(scores, axis=1, keepdims=True), own)
    cache_exp = jnp.exp(scores - peak)
    own_exp = jnp.exp(own - peak)
    total = jnp.sum(cache_exp, axis=1, keepdims=True) + own_exp
    probs = (cache_exp / total).astype(BF16)
    own_probs = (own_exp / total).astype(BF16).astype(F32)
    mixed = dot32(probs, cache) + own_probs * new_latent[...]
    mixed = mixed.astype(BF16).astype(F32)
    for s in range(LATENT_UNITS // LANES):
        out[:, s, :] = mixed[:, s * LANES : (s + 1) * LANES]
    for s in range(4, 8):
        out[:, s, :] = jnp.zeros((out.shape[0], LANES), F32)


def head_body(attended, value_up, gain, w_output, out):
    parts = [attended[:, s, :] for s in range(LATENT_UNITS // LANES)]
    values = jnp.concatenate(parts, axis=1).astype(BF16)
    head = dot_t(values, value_up[...])
    factor = lax.rsqrt(jnp.mean(head * head, axis=-1, keepdims=True) + EPS)
    head = (head * factor * gain[...]).astype(BF16)
    share = dot32(head, w_output[...]).astype(BF16)
    for j in range(out.shape[0]):
        out[j] = share[:, j * LANES : (j + 1) * LANES]


def middle_body(index, shares, hidden, out):
    total = shares[0].astype(F32)
    for j in range(1, shares.shape[0]):
        total = total + shares[j].astype(F32)
    start = pl.multiple_of(index[0] * LANES, LANES)
    middle = (hidden[:, pl.ds(start, LANES)].astype(F32) + total).astype(BF16)
    for j in range(out.shape[0]):
        out[j] = middle


def dispatch_body(tiles, gain, dispatch, normed_out, out, wide):
    count = tiles.shape[0]
    values = [tiles[j].astype(F32) for j in range(count)]
    square = values[0] * values[0]
    for j in range(1, count):
        square = square + values[j] * values[j]
    mean = jnp.sum(square, axis=1, keepdims=True) * (1.0 / MODEL_WIDTH)
    factor = lax.rsqrt(mean + EPS)
    slots = dispatch.shape[0]
    for j in range(count):
        tile = slice(j * LANES, (j + 1) * LANES)
        normed = (values[j] * factor * gain[:, tile]).astype(BF16)
        normed_out[:, tile] = normed
        wide[pl.ds(j, slots, stride=count), :] = dot32(dispatch[...], normed)
    rows = slots * count // out.shape[0]
    for p in range(out.shape[0]):
        out[p] = wide[p * rows : (p + 1) * rows, :].astype(BF16)


def side_body(normed, w_gate, w_up, w_shared_down, w_dense_up, w_dense_down, gate, out):
    x = normed[...]
    pre = dot_t(x, w_gate[...])
    shared = (pre / (1.0 + jnp.exp(-pre)) * dot_t(x, w_up[...])).astype(BF16)
    dense = jax.nn.gelu(dot32(x, w_dense_up[...])).astype(BF16)
    logit = jnp.sum(x.astype(F32) * gate[...], axis=1, keepdims=True)
    mix = 1.0 / (1.0 + jnp.exp(-logit))
    out[...] = dot32(shared, w_shared_down[...]) + mix * dot32(dense, w_dense_down[...])


def expert_body(arrived, w_gate, w_up, w_down, out, wide, rows_in):
    peers, rows, _ = arrived.shape
    count = MODEL_WIDTH // LANES
    slots = peers * rows // count
    for p in range(peers):
        wide[p * rows : (p + 1) * rows, :] = arrived[p].astype(F32)
    for j in range(count):
        tile = slice(j * LANES, (j + 1) * LANES)
        rows_in[:, tile] = wide[pl.ds(j, slots, stride=count), :].astype(BF16)
    x = rows_in[...]
    pre = dot32(x, w_gate[0])
    act = (pre / (1.0 + jnp.exp(-pre)) * dot32(x, w_up[0])).astype(BF16)
    part = dot32(act, w_down[0])
    for j in range(count):
        wide[pl.ds(j, slots, stride=count), :] = part[:, j * LANES : (j + 1) * LANES]
    for p in range(peers):
        out[p] = wide[p * rows : (p + 1) * rows, :].astype(BF16)


def combine_body(returned, weights, side, out, wide):
    peers, rows, _ = returned.shape
    count = MODEL_WIDTH // LANES
    slots = peers * rows // count
    tokens = side.shape[0]
    for p in range(peers):
        wide[p * rows : (p + 1) * rows, :] = returned[p].astype(F32)
    for j in range(count):
        block = wide[pl.ds(j, slots, stride=count), :].astype(BF16)
        sums = dot32(weights[...], block)
        routed = sums[:tokens] + sums[tokens : 2 * tokens] + sums[2 * tokens :]
        out[j] = (routed + side[:, j * LANES : (j + 1) * LANES]).astype(BF16)


def final_body(tiles, middle, out):
    total = tiles[0].astype(F32)
    for j in range(1, tiles.shape[0]):
        total = total + tiles[j].astype(F32)
    out[...] = (middle[0].astype(F32) + total).astype(BF16)


def three_parts(values):
    parts = []
    for _ in range(3):
        part = lax.reduce_precision(values, 8, 7)
        parts.append(part.astype(BF16))
        values = values - part
    return jnp.concatenate(parts, axis=0)


def row(gain):
    return gain.astype(F32)[None, :]


def on_device(
    hidden,
    lengths,
    latent_cache,
    cache_rotary,
    attn_gain,
    w_query_nope,
    w_query_rope,
    latent_weight,
    w_rotary_key,
    latent_norm_gain,
    key_up_weight,
    value_up_weight,
    head_gain,
    w_output,
    ffn_gain,
    expert_ids,
    expert_weights,
    w_expert_gate,
    w_expert_up,
    w_expert_down,
    w_shared_gate,
    w_shared_up,
    w_shared_down,
    w_dense_up,
    w_dense_down,
    dense_gate,
):
    tp = lax.axis_size("tp")
    ep = lax.axis_size("ep")
    index = lax.axis_index("tp").astype(jnp.int32).reshape(1)
    rows = hidden.shape[0]
    slots = ep * CAP
    small = shape((tp, 8, LANES), F32)
    tiles = shape((tp, rows, LANES), BF16)
    routed_rows = slots * tp // ep
    large = shape((ep, routed_rows, LANES), BF16)
    wide = pltpu.VMEM((slots * tp, LANES), F32)

    payload, normed = call(
        query_body,
        (small, shape(hidden.shape, BF16)),
        (hidden, row(attn_gain), w_query_nope.T, w_query_rope.T, key_up_weight),
    )
    queries = exchange(payload, "tp")

    inverse = 1.0 / 10000.0 ** (jnp.arange(HALF, dtype=F32) / HALF)
    angles = lengths.astype(F32)[:, None] * inverse[None, :]
    cos, sin = jnp.cos(angles), jnp.sin(angles)
    new_latent, new_key = call(
        new_token_body,
        (shape((1, LATENT_UNITS), F32), shape((1, ROPE), F32)),
        (index, normed, latent_weight, w_rotary_key.T, row(latent_norm_gain), cos, sin),
        smem=(0,),
    )

    flat_ids = expert_ids.reshape(-1)
    matches = (flat_ids[:, None] == jnp.arange(ep, dtype=jnp.int32)[None, :]).astype(jnp.int32)
    slot_index = jnp.sum((jnp.cumsum(matches, axis=0) - matches) * matches, axis=1)
    target = (flat_ids * CAP + slot_index).reshape(rows, -1)
    places = jnp.arange(slots, dtype=jnp.int32)
    chosen = places[:, None, None] == target[None, :, :]
    dispatch = jnp.any(chosen, axis=2).astype(BF16)
    combine = three_parts(jnp.sum(jnp.where(chosen, expert_weights[None, :, :], 0.0), axis=2).T)

    payload = call(
        attention_body,
        small,
        (lengths, queries, latent_cache, cache_rotary, new_latent, new_key, cos, sin),
        smem=(0,),
    )
    attended = exchange(payload, "tp")

    payload = call(head_body, tiles, (attended, value_up_weight.T, row(head_gain), w_output))
    shares = exchange(payload, "tp")
    own_middle = call(middle_body, tiles, (index, shares, hidden), smem=(0,))
    middle = exchange(own_middle, "tp")

    normed_ffn, payload = call(
        dispatch_body,
        (shape(hidden.shape, BF16), large),
        (middle, row(ffn_gain), dispatch),
        scratch=(wide,),
    )
    arrived = exchange(payload, "ep")
    side = call(
        side_body,
        shape(hidden.shape, F32),
        (
            normed_ffn,
            w_shared_gate.T,
            w_shared_up.T,
            w_shared_down,
            w_dense_up,
            w_dense_down,
            row(dense_gate),
        ),
    )
    payload = call(
        expert_body,
        large,
        (arrived, w_expert_gate, w_expert_up, w_expert_down),
        scratch=(wide, pltpu.VMEM((slots, MODEL_WIDTH), BF16)),
    )
    returned = exchange(payload, "ep")

    payload = call(combine_body, tiles, (returned, combine, side), scratch=(wide,))
    parts = exchange(payload, "tp")
    return call(final_body, shape((rows, LANES), BF16), (parts, own_middle))


def solution(mesh):
    placed = (
        P("ep", None),
        P(("ep", "tp")),
        P(("ep", "tp"), None, None),
        P(("ep", "tp"), None, None),
        P(),
        P(None, "tp"),
        P(None, "tp"),
        P(),
        P(),
        P(),
        P("tp", None),
        P(None, "tp"),
        P("tp"),
        P("tp", None),
        P(),
        P("ep", None),
        P("ep", None),
        P("ep", None, "tp"),
        P("ep", None, "tp"),
        P("ep", "tp", None),
        P(None, "tp"),
        P(None, "tp"),
        P("tp", None),
        P(None, "tp"),
        P("tp", None),
        P(),
    )
    return jax.shard_map(
        on_device, mesh=mesh, in_specs=placed, out_specs=P("ep", "tp"), check_vma=False
    )
```

time: 152 us -> 156 us (1.026)
  blocking collectives: 14.2 us -> 47.6 us
  Pallas kernels: 0 us -> 24.1 us
  waiting for transfers between devices: 58.6 us -> 35.3 us
  matrix products: 13.7 us -> 0 us
  starting transfers between devices: 48.5 us -> 36.3 us
  other arithmetic: 7.69 us -> 6 us
    all_to_all x1 -> x2, blocking collectives: 14.2 us -> 47.6 us  [exchange(): return lax.all_to_all(x, axis, split_axis=0, concat_axis=0, tiled=True)]
    pallas_call x0 -> x10, Pallas kernels: none -> 24.1 us  [call(): pl.pallas_call(body, out_shape=outs, in_specs=in_specs, out_specs=jax.tre...]
    all_to_all x6 -> x5, waiting for transfers between devices: 58.6 us -> 35.3 us  [exchange(): return lax.all_to_all(x, axis, split_axis=0, concat_axis=0, tiled=True)]
    dot_general x17 -> x0, matrix products: 13.7 us -> none  [the longest x16 11.7 us: dot32(): return jnp.dot(a, b, preferred_element_type=jnp.float32)]
    all_to_all x6 -> x5, starting transfers between devices: 48.5 us -> 36.3 us  [exchange(): return lax.all_to_all(x, axis, split_axis=0, concat_axis=0, tiled=True)]
    broadcast_in_dim x0 -> x5, other arithmetic: none -> 4.24 us  [row(): return gain.astype(F32)[None, :]]
    reshape x6 -> x0, local copies, waits for them, and re-layouts: 3.32 us -> none  [the longest x1 1.13 us: on_device(): dot32(dispatch, normed_ffn).astype(jnp.bfloat16)]
    convert_element_type x12 -> x2, other arithmetic: 3.27 us -> 0.01 us  [the longest x1 0.01 us: three_parts(): parts.append(part.astype(BF16))]
  transfers between devices with their start and end apart: 6 -> 5, of which waited for: 6 -> 5; matrix products, arithmetic and copies ran while one was open for 3% -> 4% of each run, Pallas kernels for 0% -> 4%
where the time goes in v2:
time: 156 us; the launch traced here: 155 us
  blocking collectives  47.6 us (31%)
  starting transfers between devices  36.3 us (23%)
  waiting for transfers between devices  35.3 us (23%)
  Pallas kernels  24.1 us (15%)
  other arithmetic  6 us (4%)
  local copies, waits for them, and re-layouts  5.02 us (3%)
    all_to_all x2, blocking collectives, exchange(): return lax.all_to_all(x, axis, split_axis=0, concat_axis=0, tiled=True)  47.6 us
    all_to_all x5, starting transfers between devices, exchange(): return lax.all_to_all(x, axis, split_axis=0, concat_axis=0, tiled=True)  36.3 us
    all_to_all x5, waiting for transfers between devices, exchange(): return lax.all_to_all(x, axis, split_axis=0, concat_axis=0, tiled=True)  35.3 us
    pallas_call x10, Pallas kernels, call(): pl.pallas_call(body, out_shape=outs, in_specs=in_specs, out_specs=jax.tre...  24.1 us
    broadcast_in_dim x5, other arithmetic, row(): return gain.astype(F32)[None, :]  4.24 us
    unnamed x21, local copies, waits for them, and re-layouts  4.05 us
  transfers between devices with their start and end apart: 5, of which 5 were waited for; matrix products, arithmetic and copies ran while one was open for 4% of the time, Pallas kernels for 4%

profile of v2, /device:TPU:1, one launch (start us, length us, event | category | flops | bytes accessed | tf_op | source)
XLA Modules:
  0.0 155.0 jit_solution(15547672439118381728)
XLA Ops:
  0.0 1.3 broadcast_in_dim.54
  1.3 2.2 %shard_map.244 = (f32[16,8,128]{2,1,0:T(8,128)}, bf16[16,2048]{1,0:T(8,128)(2,1)}) custom-call(bf16[16,2048]{1,0:T(8,128)(2,1)} %hidden.3, f32[1,2048]{1,0:T(1,128)} %bitcast.29, bf16[64,2048]{1,0:T(8,128)(2,1)} %bitcast.22, bf16[32,2048]{1,0:T(8,128)(2,1)} %bitcast.25, bf16[64,512]{1,0:T(8,128)(2,1)} %key_up.1), custom_call_target="tpu_custom_call" | custom-call | tf_op jit(solution)/shard_map/pallas_call | solution.py:37
  3.4 17.4 %all-to-all-start = ((f32[16,8,128]{2,1,0:T(8,128)}), f32[16,8,128]{2,1,0:T(8,128)S(1)}, u32[]{:S(2)}, u32[]{:S(2)}) async-start(f32[16,8,128]{2,1,0:T(8,128)} %get-tuple-element.11), calls=%async_computation | async-start | bytes 131072 | tf_op jit(solution)/shard_map/all_to_all | solution.py:21
  21.5 1.3 broadcast_in_dim.55
  22.7 0.8 copy.37
  23.5 0.1 eq.29
  23.6 0.6 fusion.4
  24.2 2.8 %shard_map.245 = (f32[1,512]{1,0:T(1,128)}, f32[1,32]{1,0:T(1,128)}) custom-call(s32[1]{0:T(128)} %bitcast.index, bf16[16,2048]{1,0:T(8,128)(2,1)} %get-tuple-element.12.normed, bf16[2048,512]{1,0:T(8,128)(2,1)} %w_latent.1, bf16[32,2048]{1,0:T(8,128)(2,1)} %bitcast.26, f32[1,512]{1,0:T(1,128)} %bitcast.31, f32[1,16]{1,0:T(1,128)} %get-tuple-element.21.cos, ...), custom_call_target="tpu_custom_call" | custom-call | tf_op jit(solution)/shard_map/pallas_call | solution.py:37
  27.0 1.6 %all-to-all-done.queries = f32[16,8,128]{2,1,0:T(8,128)S(1)} async-done(((f32[16,8,128]{2,1,0:T(8,128)}), f32[16,8,128]{2,1,0:T(8,128)S(1)}, u32[]{:S(2)}, u32[]{:S(2)}) %all-to-all-start) | async-done | bytes 65568 | tf_op jit(solution)/shard_map/all_to_all | solution.py:21
  28.7 0.6 copy-done.1
  29.3 3.2 %shard_map.246 = f32[16,8,128]{2,1,0:T(8,128)} custom-call(s32[1]{0:T(128)S(6)} %copy.40.lengths, f32[16,8,128]{2,1,0:T(8,128)} %copy-done.1, bf16[1,1536,512]{2,1,0:T(8,128)(2,1)} %latents.1, bf16[1,32,1536]{2,1,0:T(8,128)(2,1)} %rotary.1, f32[1,512]{1,0:T(1,128)} %get-tuple-element.13.new_latent, f32[1,32]{1,0:T(1,128)} %get-tuple-element.14.new_key, ...), custom_call_target="tpu_custom_call" | custom-call | tf_op jit(solution)/shard_map/pallas_call | solution.py:37
  32.5 5.6 %all-to-all-start.1 = ((f32[16,8,128]{2,1,0:T(8,128)}), f32[16,8,128]{2,1,0:T(8,128)S(1)}, u32[]{:S(2)}, u32[]{:S(2)}) async-start(f32[16,8,128]{2,1,0:T(8,128)} %shard_map.246), calls=%async_computation.1 | async-start | bytes 131072 | tf_op jit(solution)/shard_map/all_to_all | solution.py:21
  38.1 0.0 copy-done.9
  38.1 0.5 bitcast_convert_fusion.gain
  38.7 7.3 %all-to-all-done.1.attended = f32[16,8,128]{2,1,0:T(8,128)S(1)} async-done(((f32[16,8,128]{2,1,0:T(8,128)}), f32[16,8,128]{2,1,0:T(8,128)S(1)}, u32[]{:S(2)}, u32[]{:S(2)}) %all-to-all-start.1) | async-done | bytes 65568 | tf_op jit(solution)/shard_map/all_to_all | solution.py:21
  45.9 0.6 copy-done.4
  46.5 2.1 %shard_map.247 = bf16[16,16,128]{2,1,0:T(8,128)(2,1)} custom-call(f32[16,8,128]{2,1,0:T(8,128)} %copy-done.4, bf16[64,512]{1,0:T(8,128)(2,1)} %bitcast.27, f32[1,64]{1,0:T(1,128)} %bitcast_convert_fusion.gain, bf16[64,2048]{1,0:T(8,128)(2,1)} %w_output.1), custom_call_target="tpu_custom_call" | custom-call | tf_op jit(solution)/shard_map/pallas_call | solution.py:37
  48.6 3.4 %all-to-all-start.2 = ((bf16[16,16,128]{2,1,0:T(8,128)(2,1)}), bf16[16,16,128]{2,1,0:T(8,128)(2,1)S(1)}, u32[]{:S(2)}, u32[]{:S(2)}) async-start(bf16[16,16,128]{2,1,0:T(8,128)(2,1)} %shard_map.247), calls=%async_computation.2 | async-start | bytes 131072 | tf_op jit(solution)/shard_map/all_to_all | solution.py:21
  52.0 0.1 fusion
  52.1 0.1 reduce_window_sum.11
  52.2 0.2 select_reduce_fusion.1
  52.4 0.1 reduce_sum.21
  52.5 0.1 copy.38
  52.5 7.3 %all-to-all-done.2.shares = bf16[16,16,128]{2,1,0:T(8,128)(2,1)S(1)} async-done(((bf16[16,16,128]{2,1,0:T(8,128)(2,1)}), bf16[16,16,128]{2,1,0:T(8,128)(2,1)S(1)}, u32[]{:S(2)}, u32[]{:S(2)}) %all-to-all-start.2) | async-done | bytes 65568 | tf_op jit(solution)/shard_map/all_to_all | solution.py:21
  59.8 0.6 copy-done.2
  60.5 1.5 shard_map.248.middle
  62.0 3.4 %all-to-all-start.3 = ((bf16[16,16,128]{2,1,0:T(8,128)(2,1)}), bf16[16,16,128]{2,1,0:T(8,128)(2,1)S(1)}, u32[]{:S(2)}, u32[]{:S(2)}) async-start(bf16[16,16,128]{2,1,0:T(8,128)(2,1)} %shard_map.248.middle), calls=%async_computation.3 | async-start | bytes 131072 | tf_op jit(solution)/shard_map/all_to_all | solution.py:21
  65.4 0.0 copy-done.5
  65.4 0.1 fusion.1
  65.5 0.7 copy.39.dispatch
  66.3 0.0 copy-done.6
  66.3 0.6 broadcast_in_dim.57
  66.8 6.4 %all-to-all-done.3.tiles = bf16[16,16,128]{2,1,0:T(8,128)(2,1)S(1)} async-done(((bf16[16,16,128]{2,1,0:T(8,128)(2,1)}), bf16[16,16,128]{2,1,0:T(8,128)(2,1)S(1)}, u32[]{:S(2)}, u32[]{:S(2)}) %all-to-all-start.3) | async-done | bytes 65568 | tf_op jit(solution)/shard_map/all_to_all | solution.py:21
  73.3 0.6 copy-done.3
  73.9 2.3 %shard_map.249 = (bf16[16,2048]{1,0:T(8,128)(2,1)}, bf16[64,32,128]{2,1,0:T(8,128)(2,1)}) custom-call(bf16[16,16,128]{2,1,0:T(8,128)(2,1)} %copy-done.3, f32[1,2048]{1,0:T(1,128)} %bitcast.30, bf16[128,16]{1,0:T(8,128)(2,1)} %copy.39.dispatch), custom_call_target="tpu_custom_call" | custom-call | tf_op jit(solution)/shard_map/pallas_call | solution.py:37
  76.2 31.9 %all_to_all.35.arrived = bf16[64,32,128]{2,1,0:T(8,128)(2,1)} all-to-all(bf16[64,32,128]{2,1,0:T(8,128)(2,1)} %get-tuple-element.15), channel_id=1, replica_groups=mesh['ep'=64,'tp'=16] {'ep'}, dimensions={0} | all-to-all | bytes 1048576 | tf_op jit(solution)/shard_map/all_to_all | solution.py:21
  108.0 3.6 %shard_map.250 = bf16[64,32,128]{2,1,0:T(8,128)(2,1)} custom-call(bf16[64,32,128]{2,1,0:T(8,128)(2,1)} %all_to_all.35.arrived, bf16[1,2048,128]{2,1,0:T(8,128)(2,1)} %w_gate.1, bf16[1,2048,128]{2,1,0:T(8,128)(2,1)} %w_up.1, bf16[1,128,2048]{2,1,0:T(8,128)(2,1)} %w_down.1), custom_call_target="tpu_custom_call" | custom-call | tf_op jit(solution)/shard_map/pallas_call | solution.py:37
  111.7 6.4 %all-to-all-start.5 = ((bf16[64,32,128]{2,1,0:T(8,128)(2,1)}), bf16[64,32,128]{2,1,0:T(8,128)(2,1)S(1)}, u32[]{:S(2)}, u32[]{:S(2)}) async-start(bf16[64,32,128]{2,1,0:T(8,128)(2,1)} %shard_map.250), calls=%async_computation.5 | async-start | bytes 1048576 | tf_op jit(solution)/shard_map/all_to_all | solution.py:21
  118.1 0.0 copy-done.7
  118.1 0.6 broadcast_in_dim.58
  118.7 0.1 select_reduce_fusion
  118.8 0.6 pad_maximum_fusion.weights
  119.4 2.6 %shard_map.251.side = f32[16,2048]{1,0:T(8,128)} custom-call(bf16[16,2048]{1,0:T(8,128)(2,1)} %get-tuple-element.16.normed, bf16[64,2048]{1,0:T(8,128)(2,1)} %bitcast.23, bf16[64,2048]{1,0:T(8,128)(2,1)} %bitcast.24, bf16[64,2048]{1,0:T(8,128)(2,1)} %w_shared_down.1, bf16[2048,128]{1,0:T(8,128)(2,1)} %w_dense_up.1, bf16[128,2048]{1,0:T(8,128)(2,1)} %w_dense_down.1, ...), custom_call_target="tpu_custom_call" | custom-call | tf_op jit(solution)/shard_map/pallas_call | solution.py:37
  122.1 12.7 %all-to-all-done.5.returned = bf16[64,32,128]{2,1,0:T(8,128)(2,1)S(1)} async-done(((bf16[64,32,128]{2,1,0:T(8,128)(2,1)}), bf16[64,32,128]{2,1,0:T(8,128)(2,1)S(1)}, u32[]{:S(2)}, u32[]{:S(2)}) %all-to-all-start.5) | async-done | bytes 524320 | tf_op jit(solution)/shard_map/all_to_all | solution.py:21
  134.7 0.8 copy-done
  135.5 2.2 %shard_map.252 = bf16[16,16,128]{2,1,0:T(8,128)(2,1)} custom-call(bf16[64,32,128]{2,1,0:T(8,128)(2,1)} %copy-done, bf16[48,128]{1,0:T(8,128)(2,1)} %pad_maximum_fusion.weights, f32[16,2048]{1,0:T(8,128)} %shard_map.251.side), custom_call_target="tpu_custom_call" | custom-call | tf_op jit(solution)/shard_map/pallas_call | solution.py:37
  137.8 15.7 %all_to_all.36.tiles = bf16[16,16,128]{2,1,0:T(8,128)(2,1)} all-to-all(bf16[16,16,128]{2,1,0:T(8,128)(2,1)} %shard_map.252), channel_id=1, replica_groups=mesh['ep'=64,'tp'=16] {'tp'}, dimensions={0} | all-to-all | bytes 131072 | tf_op jit(solution)/shard_map/all_to_all | solution.py:21
  153.5 1.5 shard_map.253
  (14 shorter events, 0.0 us)
Async XLA Ops:
  3.4 25.2 %all-to-all-start = ((f32[16,8,128]{2,1,0:T(8,128)}), f32[16,8,128]{2,1,0:T(8,128)S(1)}, u32[]{:S(2)}, u32[]{:S(2)}) async-start(f32[16,8,128]{2,1,0:T(8,128)} %get-tuple-element.11), calls=%async_computation | async-start | bytes 131072 | tf_op jit(solution)/shard_map/all_to_all | solution.py:21
  24.2 13.9 %copy-start.9 = (bf16[64]{0:T(256)(128)(2,1)S(1)}, bf16[64]{0:T(256)(128)(2,1)}, u32[]{:S(2)}) copy-start(bf16[64]{0:T(256)(128)(2,1)} %param.38) | copy-start | bytes 388
  24.2 41.2 %copy-start.5 = (s32[16,4]{0,1:T(4,128)S(1)}, s32[16,4]{0,1:T(4,128)}, u32[]{:S(2)}) copy-start(s32[16,4]{0,1:T(4,128)} %param.41) | copy-start | bytes 772
  27.0 39.2 %copy-start.6 = (bf16[2048]{0:T(1024)(128)(2,1)S(1)}, bf16[2048]{0:T(1024)(128)(2,1)}, u32[]{:S(2)}) copy-start(bf16[2048]{0:T(1024)(128)(2,1)} %param.40) | copy-start | bytes 12292
  28.7 0.6 copy-start.1
  32.5 13.4 %all-to-all-start.1 = ((f32[16,8,128]{2,1,0:T(8,128)}), f32[16,8,128]{2,1,0:T(8,128)S(1)}, u32[]{:S(2)}, u32[]{:S(2)}) async-start(f32[16,8,128]{2,1,0:T(8,128)} %shard_map.246), calls=%async_computation.1 | async-start | bytes 131072 | tf_op jit(solution)/shard_map/all_to_all | solution.py:21
  45.9 0.6 copy-start.4
  48.6 11.2 %all-to-all-start.2 = ((bf16[16,16,128]{2,1,0:T(8,128)(2,1)}), bf16[16,16,128]{2,1,0:T(8,128)(2,1)S(1)}, u32[]{:S(2)}, u32[]{:S(2)}) async-start(bf16[16,16,128]{2,1,0:T(8,128)(2,1)} %shard_map.247), calls=%async_computation.2 | async-start | bytes 131072 | tf_op jit(solution)/shard_map/all_to_all | solution.py:21
  59.8 0.6 copy-start.2
  62.0 11.3 %all-to-all-start.3 = ((bf16[16,16,128]{2,1,0:T(8,128)(2,1)}), bf16[16,16,128]{2,1,0:T(8,128)(2,1)S(1)}, u32[]{:S(2)}, u32[]{:S(2)}) async-start(bf16[16,16,128]{2,1,0:T(8,128)(2,1)} %shard_map.248.middle), calls=%async_computation.3 | async-start | bytes 131072 | tf_op jit(solution)/shard_map/all_to_all | solution.py:21
  73.3 0.6 copy-start.3
  108.0 10.1 %copy-start.7 = (bf16[2048]{0:T(1024)(128)(2,1)S(1)}, bf16[2048]{0:T(1024)(128)(2,1)}, u32[]{:S(2)}) copy-start(bf16[2048]{0:T(1024)(128)(2,1)} %param.51) | copy-start | bytes 12292
  108.0 10.7 %copy-start.8 = (f32[16,4]{0,1:T(4,128)S(1)}, f32[16,4]{0,1:T(4,128)}, u32[]{:S(2)}) copy-start(f32[16,4]{0,1:T(4,128)} %param.42) | copy-start | bytes 772
  111.7 23.1 %all-to-all-start.5 = ((bf16[64,32,128]{2,1,0:T(8,128)(2,1)}), bf16[64,32,128]{2,1,0:T(8,128)(2,1)S(1)}, u32[]{:S(2)}, u32[]{:S(2)}) async-start(bf16[64,32,128]{2,1,0:T(8,128)(2,1)} %shard_map.250), calls=%async_computation.5 | async-start | bytes 1048576 | tf_op jit(solution)/shard_map/all_to_all | solution.py:21
  134.7 0.8 copy-start

commit v3 on v2

--- a/solution.py
+++ b/solution.py
@@ -29,28 +29,41 @@
     return lax.dot_general(a, b, (((1,), (1,)), ((), ())), preferred_element_type=F32)
 
 
-def call(body, outs, args, smem=(), scratch=()):
+def call(body, outs, args, smem=(), hbm=(), raw=(), scratch=(), leave=False):
     vmem = pl.BlockSpec(memory_space=pltpu.VMEM)
-    in_specs = [
-        pl.BlockSpec(memory_space=pltpu.SMEM) if i in smem else vmem for i in range(len(args))
+    kinds = {i: pl.BlockSpec(memory_space=pltpu.SMEM) for i in smem}
+    kinds.update({i: pl.BlockSpec(memory_space=pl.ANY) for i in raw})
+    free = set(smem) | set(hbm) | set(raw)
+    args = [
+        x if i in free else pltpu.with_memory_space_constraint(x, pltpu.VMEM)
+        for i, x in enumerate(args)
     ]
+    place = (lambda o: o) if leave else (lambda o: pltpu.VMEM(o.shape, o.dtype))
     return pl.pallas_call(
         body,
-        out_shape=outs,
-        in_specs=in_specs,
+        out_shape=jax.tree.map(place, outs),
+        in_specs=[kinds.get(i, vmem) for i in range(len(args))],
         out_specs=jax.tree.map(lambda _: vmem, outs),
         scratch_shapes=list(scratch),
     )(*args)
 
 
+def together(*values):
+    return lax.optimization_barrier(values)
+
+
 def shape(dims, dtype):
     return jax.ShapeDtypeStruct(dims, dtype)
+
+
+def row(gain):
+    return gain[...].astype(F32).reshape(1, -1)
 
 
 def query_body(hidden, gain, w_nope, w_rope, key_up, out, normed_out):
     values = hidden[...].astype(F32)
     factor = lax.rsqrt(jnp.mean(values * values, axis=-1, keepdims=True) + EPS)
-    normed = (values * factor * gain[...]).astype(BF16)
+    normed = (values * factor * row(gain)).astype(BF16)
     normed_out[...] = normed
     nope = dot_t(normed, w_nope[...]).astype(BF16)
     rope = dot_t(normed, w_rope[...]).astype(BF16).astype(F32)
@@ -68,7 +81,15 @@
     return jnp.concatenate([first * cos - second * sin, first * sin + second * cos], axis=1)
 
 
-def new_token_body(index, normed, w_latent, w_key, gain, cos, sin, latent_out, key_out):
+def new_token_body(
+    index, normed, w_latent, w_key, gain, cos, sin, cache, rotary, latent_out, key_out, cache_out, rotary_out, sems
+):
+    copies = [
+        pltpu.make_async_copy(cache, cache_out, sems.at[0]),
+        pltpu.make_async_copy(rotary, rotary_out, sems.at[1]),
+    ]
+    for copy in copies:
+        copy.start()
     latent = dot32(normed[...], w_latent[...])
     key = dot_t(normed[...], w_key[...])
     rows = lax.broadcasted_iota(jnp.int32, (latent.shape[0], 1), 0)
@@ -76,8 +97,10 @@
     latent = jnp.sum(jnp.where(mine, latent, 0.0), axis=0, keepdims=True)
     key = jnp.sum(jnp.where(mine, key, 0.0), axis=0, keepdims=True)
     factor = lax.rsqrt(jnp.mean(latent * latent, axis=-1, keepdims=True) + EPS)
-    latent_out[...] = (latent * factor * gain[...]).astype(BF16).astype(F32)
+    latent_out[...] = (latent * factor * row(gain)).astype(BF16).astype(F32)
     key_out[...] = rotated(key, cos[...], sin[...]).astype(BF16).astype(F32)
+    for copy in copies:
+        copy.wait()
 
 
 def attention_body(lengths, queries, latents, rotary, new_latent, new_key, cos, sin, out):
@@ -111,7 +134,7 @@
     values = jnp.concatenate(parts, axis=1).astype(BF16)
     head = dot_t(values, value_up[...])
     factor = lax.rsqrt(jnp.mean(head * head, axis=-1, keepdims=True) + EPS)
-    head = (head * factor * gain[...]).astype(BF16)
+    head = (head * factor * row(gain)).astype(BF16)
     share = dot32(head, w_output[...]).astype(BF16)
     for j in range(out.shape[0]):
         out[j] = share[:, j * LANES : (j + 1) * LANES]
@@ -136,9 +159,10 @@
     mean = jnp.sum(square, axis=1, keepdims=True) * (1.0 / MODEL_WIDTH)
     factor = lax.rsqrt(mean + EPS)
     slots = dispatch.shape[0]
+    gains = row(gain)
     for j in range(count):
         tile = slice(j * LANES, (j + 1) * LANES)
-        normed = (values[j] * factor * gain[:, tile]).astype(BF16)
+        normed = (values[j] * factor * gains[:, tile]).astype(BF16)
         normed_out[:, tile] = normed
         wide[pl.ds(j, slots, stride=count), :] = dot32(dispatch[...], normed)
     rows = slots * count // out.shape[0]
@@ -151,7 +175,7 @@
     pre = dot_t(x, w_gate[...])
     shared = (pre / (1.0 + jnp.exp(-pre)) * dot_t(x, w_up[...])).astype(BF16)
     dense = jax.nn.gelu(dot32(x, w_dense_up[...])).astype(BF16)
-    logit = jnp.sum(x.astype(F32) * gate[...], axis=1, keepdims=True)
+    logit = jnp.sum(x.astype(F32) * row(gate), axis=1, keepdims=True)
     mix = 1.0 / (1.0 + jnp.exp(-logit))
     out[...] = dot32(shared, w_shared_down[...]) + mix * dot32(dense, w_dense_down[...])
 
@@ -203,10 +227,6 @@
         parts.append(part.astype(BF16))
         values = values - part
     return jnp.concatenate(parts, axis=0)
-
-
-def row(gain):
-    return gain.astype(F32)[None, :]
 
 
 def on_device(
@@ -251,20 +271,38 @@
     payload, normed = call(
         query_body,
         (small, shape(hidden.shape, BF16)),
-        (hidden, row(attn_gain), w_query_nope.T, w_query_rope.T, key_up_weight),
+        (hidden, attn_gain, w_query_nope.T, w_query_rope.T, key_up_weight),
+        hbm=range(5),
     )
     queries = exchange(payload, "tp")
 
     inverse = 1.0 / 10000.0 ** (jnp.arange(HALF, dtype=F32) / HALF)
     angles = lengths.astype(F32)[:, None] * inverse[None, :]
     cos, sin = jnp.cos(angles), jnp.sin(angles)
-    new_latent, new_key = call(
+    new_latent, new_key, cache, rotary = call(
         new_token_body,
-        (shape((1, LATENT_UNITS), F32), shape((1, ROPE), F32)),
-        (index, normed, latent_weight, w_rotary_key.T, row(latent_norm_gain), cos, sin),
+        (
+            shape((1, LATENT_UNITS), F32),
+            shape((1, ROPE), F32),
+            shape(latent_cache.shape, BF16),
+            shape(cache_rotary.shape, BF16),
+        ),
+        (
+            index,
+            normed,
+            latent_weight,
+            w_rotary_key.T,
+            latent_norm_gain,
+            cos,
+            sin,
+            latent_cache,
+            cache_rotary,
+        ),
         smem=(0,),
-    )
-
+        hbm=(2, 3, 4, 5, 6),
+        raw=(7, 8),
+        scratch=(pltpu.SemaphoreType.DMA((2,)),),
+    )
     flat_ids = expert_ids.reshape(-1)
     matches = (flat_ids[:, None] == jnp.arange(ep, dtype=jnp.int32)[None, :]).astype(jnp.int32)
     slot_index = jnp.sum((jnp.cumsum(matches, axis=0) - matches) * matches, axis=1)
@@ -272,17 +310,17 @@
     places = jnp.arange(slots, dtype=jnp.int32)
     chosen = places[:, None, None] == target[None, :, :]
     dispatch = jnp.any(chosen, axis=2).astype(BF16)
-    combine = three_parts(jnp.sum(jnp.where(chosen, expert_weights[None, :, :], 0.0), axis=2).T)
+    queries, new_latent, new_key, dispatch = together(queries, new_latent, new_key, dispatch)
 
     payload = call(
         attention_body,
         small,
-        (lengths, queries, latent_cache, cache_rotary, new_latent, new_key, cos, sin),
+        (lengths, queries, cache, rotary, new_latent, new_key, cos, sin),
         smem=(0,),
     )
     attended = exchange(payload, "tp")
 
-    payload = call(head_body, tiles, (attended, value_up_weight.T, row(head_gain), w_output))
+    payload = call(head_body, tiles, (attended, value_up_weight.T, head_gain, w_output))
     shares = exchange(payload, "tp")
     own_middle = call(middle_body, tiles, (index, shares, hidden), smem=(0,))
     middle = exchange(own_middle, "tp")
@@ -290,7 +328,7 @@
     normed_ffn, payload = call(
         dispatch_body,
         (shape(hidden.shape, BF16), large),
-        (middle, row(ffn_gain), dispatch),
+        (middle, ffn_gain, dispatch),
         scratch=(wide,),
     )
     arrived = exchange(payload, "ep")
@@ -304,9 +342,12 @@
             w_shared_down,
             w_dense_up,
             w_dense_down,
-            row(dense_gate),
+            dense_gate,
         ),
-    )
+        hbm=range(1, 7),
+    )
+    combine = three_parts(jnp.sum(jnp.where(chosen, expert_weights[None, :, :], 0.0), axis=2).T)
+    arrived, side, combine = together(arrived, side, combine)
     payload = call(
         expert_body,
         large,
@@ -317,7 +358,7 @@
 
     payload = call(combine_body, tiles, (returned, combine, side), scratch=(wide,))
     parts = exchange(payload, "tp")
-    return call(final_body, shape((rows, LANES), BF16), (parts, own_middle))
+    return call(final_body, shape((rows, LANES), BF16), (parts, own_middle), leave=True)
 
 
 def solution(mesh):

time: 156 us -> 137 us (0.88)
  blocking collectives: 47.6 us -> 71.5 us
  waiting for transfers between devices: 35.3 us -> 16.8 us
  Pallas kernels: 24.1 us -> 12.7 us
  starting transfers between devices: 36.3 us -> 31.5 us
  other arithmetic: 6 us -> 1.83 us
  local copies, waits for them, and re-layouts: 5.02 us -> 1.19 us
    all_to_all x2 -> x5, blocking collectives: 47.6 us -> 71.5 us  [exchange(): return lax.all_to_all(x, axis, split_axis=0, concat_axis=0, tiled=True)]
    all_to_all x5 -> x2, waiting for transfers between devices: 35.3 us -> 16.8 us  [exchange(): return lax.all_to_all(x, axis, split_axis=0, concat_axis=0, tiled=True)]
    pallas_call x10, Pallas kernels: 24.1 us -> 12.7 us  [call(): pl.pallas_call(body, out_shape=jax.tree.map(place, outs), in_specs=[kinds...]
    all_to_all x5 -> x2, starting transfers between devices: 36.3 us -> 31.5 us  [exchange(): return lax.all_to_all(x, axis, split_axis=0, concat_axis=0, tiled=True)]
    broadcast_in_dim x5 -> x0, other arithmetic: 4.24 us -> none  [row(): return gain.astype(F32)[None, :]]
    unnamed x21 -> x23, local copies, waits for them, and re-layouts: 4.05 us -> 0.81 us
  transfers between devices with their start and end apart: 5 -> 2, of which waited for: 5 -> 2; matrix products, arithmetic and copies ran while one was open for 4% -> 2% of each run, Pallas kernels for 4% -> 4%
where the time goes in v3:
time: 137 us; the launch traced here: 136 us
  blocking collectives  71.5 us (52%)
  starting transfers between devices  31.5 us (23%)
  waiting for transfers between devices  16.8 us (12%)
  Pallas kernels  12.7 us (9%)
  other arithmetic  1.83 us (1%)
    all_to_all x5, blocking collectives, exchange(): return lax.all_to_all(x, axis, split_axis=0, concat_axis=0, tiled=True)  71.5 us
    all_to_all x2, starting transfers between devices, exchange(): return lax.all_to_all(x, axis, split_axis=0, concat_axis=0, tiled=True)  31.5 us
    all_to_all x2, waiting for transfers between devices, exchange(): return lax.all_to_all(x, axis, split_axis=0, concat_axis=0, tiled=True)  16.8 us
    pallas_call x10, Pallas kernels, call(): pl.pallas_call(body, out_shape=jax.tree.map(place, outs), in_specs=[kinds...  12.7 us
  transfers between devices with their start and end apart: 2, of which 2 were waited for; matrix products, arithmetic and copies ran while one was open for 2% of the time, Pallas kernels for 4%

profile of v3, /device:TPU:1, one launch (start us, length us, event | category | flops | bytes accessed | tf_op | source)
XLA Modules:
  0.0 136.4 jit_solution(9994991303468634885)
XLA Ops:
  0.0 2.2 %shard_map.244 = (f32[16,8,128]{2,1,0:T(8,128)}, bf16[16,2048]{1,0:T(8,128)(2,1)S(1)}) custom-call(bf16[16,2048]{1,0:T(8,128)(2,1)} %hidden.3, bf16[2048]{0:T(1024)(128)(2,1)} %gain.4, bf16[64,2048]{1,0:T(8,128)(2,1)} %bitcast.16, bf16[32,2048]{1,0:T(8,128)(2,1)} %bitcast.19, bf16[64,512]{1,0:T(8,128)(2,1)} %key_up.1), custom_call_target="tpu_custom_call" | custom-call | tf_op jit(solution)/shard_map/pallas_call | solution.py:42
  2.2 17.4 %all-to-all-start = ((f32[16,8,128]{2,1,0:T(8,128)}), f32[16,8,128]{2,1,0:T(8,128)S(1)}, u32[]{:S(2)}, u32[]{:S(2)}) async-start(f32[16,8,128]{2,1,0:T(8,128)} %get-tuple-element.20), calls=%async_computation | async-start | bytes 131072 | tf_op jit(solution)/shard_map/all_to_all | solution.py:21
  19.6 0.8 copy.37
  20.3 0.1 eq.29
  20.4 0.1 fusion
  20.5 0.1 reduce_window_sum.11
  20.6 0.2 select_reduce_fusion.1
  20.8 0.1 reduce_sum.21
  20.9 0.1 copy.38
  20.9 0.7 multiply_add_fusion
  21.6 0.1 fusion.1
  22.4 0.1 copy.39
  22.5 0.6 fusion.4
  23.1 0.0 copy-start.7
  23.1 0.0 copy-start.8
  23.1 3.1 %shard_map.245 = (f32[1,512]{1,0:T(1,128)S(1)}, f32[1,32]{1,0:T(1,128)S(1)}, bf16[1,1536,512]{2,1,0:T(8,128)(2,1)S(1)}, bf16[1,32,1536]{2,1,0:T(8,128)(2,1)S(1)}) custom-call(s32[1]{0:T(128)} %bitcast.index, bf16[16,2048]{1,0:T(8,128)(2,1)S(1)} %get-tuple-element.21.normed, bf16[2048,512]{1,0:T(8,128)(2,1)} %w_latent.1, bf16[32,2048]{1,0:T(8,128)(2,1)} %bitcast.20, ...), custom_call_target="tpu_custom_call" | custom-call | tf_op jit(solution)/shard_map/pallas_call | solution.py:42
  26.2 0.0 copy-start.3
  26.3 0.0 copy-start.5
  26.3 0.0 copy-start.9
  26.3 0.0 copy-start.4
  26.3 0.0 copy-start.6
  26.3 1.1 all-to-all-done.queries
  27.4 0.0 copy-done.7
  27.4 0.0 copy-done.8
  27.4 1.2 shard_map.246
  28.6 13.8 %all_to_all.35.attended = f32[16,8,128]{2,1,0:T(8,128)S(1)} all-to-all(f32[16,8,128]{2,1,0:T(8,128)S(1)} %shard_map.246), channel_id=1, replica_groups=mesh['ep'=64,'tp'=16] {'tp'}, dimensions={0} | all-to-all | bytes 131072 | tf_op jit(solution)/shard_map/all_to_all | solution.py:21
  42.4 0.0 copy-done.3
  42.4 0.0 copy-done.5
  42.4 0.0 copy-done.9
  42.4 0.4 shard_map.247
  42.8 10.3 %all_to_all.36.shares = bf16[16,16,128]{2,1,0:T(8,128)(2,1)S(1)} all-to-all(bf16[16,16,128]{2,1,0:T(8,128)(2,1)S(1)} %shard_map.247), channel_id=1, replica_groups=mesh['ep'=64,'tp'=16] {'tp'}, dimensions={0} | all-to-all | bytes 131072 | tf_op jit(solution)/shard_map/all_to_all | solution.py:21
  53.1 0.0 copy-done.4
  53.1 10.4 %all_to_all.37.tiles = bf16[16,16,128]{2,1,0:T(8,128)(2,1)S(1)} all-to-all(bf16[16,16,128]{2,1,0:T(8,128)(2,1)S(1)} %shard_map.248.middle), channel_id=1, replica_groups=mesh['ep'=64,'tp'=16] {'tp'}, dimensions={0} | all-to-all | bytes 131072 | tf_op jit(solution)/shard_map/all_to_all | solution.py:21
  63.5 0.0 copy-done.6
  63.5 1.4 %shard_map.249 = (bf16[16,2048]{1,0:T(8,128)(2,1)S(1)}, bf16[64,32,128]{2,1,0:T(8,128)(2,1)}) custom-call(bf16[16,16,128]{2,1,0:T(8,128)(2,1)S(1)} %all_to_all.37.tiles, bf16[2048]{0:T(1024)(128)(2,1)S(1)} %copy-done.6, bf16[128,16]{1,0:T(8,128)(2,1)S(1)} %convert_element_type.20.dispatch), custom_call_target="tpu_custom_call" | custom-call | tf_op jit(solution)/shard_map/pallas_call | solution.py:42
  65.0 14.1 %all-to-all-start.4 = ((bf16[64,32,128]{2,1,0:T(8,128)(2,1)}), bf16[64,32,128]{2,1,0:T(8,128)(2,1)S(1)}, u32[]{:S(2)}, u32[]{:S(2)}) async-start(bf16[64,32,128]{2,1,0:T(8,128)(2,1)} %get-tuple-element.30), calls=%async_computation.4 | async-start | bytes 1048576 | tf_op jit(solution)/shard_map/all_to_all | solution.py:21
  79.1 0.0 copy-done.10
  79.1 0.1 select_reduce_fusion
  79.2 2.0 %shard_map.250.side = f32[16,2048]{1,0:T(8,128)S(1)} custom-call(bf16[16,2048]{1,0:T(8,128)(2,1)S(1)} %get-tuple-element.31.normed, bf16[64,2048]{1,0:T(8,128)(2,1)} %bitcast.17, bf16[64,2048]{1,0:T(8,128)(2,1)} %bitcast.18, bf16[64,2048]{1,0:T(8,128)(2,1)} %w_shared_down.1, bf16[2048,128]{1,0:T(8,128)(2,1)} %w_dense_up.1, bf16[128,2048]{1,0:T(8,128)(2,1)} %w_dense_down.1, ...), custom_call_target="tpu_custom_call" | custom-call | tf_op jit(solution)/shard_map/pallas_call | solution.py:42
  81.2 15.7 %all-to-all-done.4.arrived = bf16[64,32,128]{2,1,0:T(8,128)(2,1)S(1)} async-done(((bf16[64,32,128]{2,1,0:T(8,128)(2,1)}), bf16[64,32,128]{2,1,0:T(8,128)(2,1)S(1)}, u32[]{:S(2)}, u32[]{:S(2)}) %all-to-all-start.4) | async-done | bytes 524320 | tf_op jit(solution)/shard_map/all_to_all | solution.py:21
  96.9 0.0 copy-done
  96.9 0.0 copy-done.1
  96.9 0.0 copy-done.2
  96.9 1.3 shard_map.251
  98.2 22.9 %all_to_all.38.returned = bf16[64,32,128]{2,1,0:T(8,128)(2,1)S(1)} all-to-all(bf16[64,32,128]{2,1,0:T(8,128)(2,1)S(1)} %shard_map.251), channel_id=1, replica_groups=mesh['ep'=64,'tp'=16] {'ep'}, dimensions={0} | all-to-all | bytes 1048576 | tf_op jit(solution)/shard_map/all_to_all | solution.py:21
  121.1 0.5 shard_map.252
  121.6 14.1 %all_to_all.39.tiles = bf16[16,16,128]{2,1,0:T(8,128)(2,1)S(1)} all-to-all(bf16[16,16,128]{2,1,0:T(8,128)(2,1)S(1)} %shard_map.252), channel_id=1, replica_groups=mesh['ep'=64,'tp'=16] {'tp'}, dimensions={0} | all-to-all | bytes 131072 | tf_op jit(solution)/shard_map/all_to_all | solution.py:21
  135.8 0.6 shard_map.253
  (8 shorter events, 0.1 us)
Async XLA Ops:
  2.2 25.2 %all-to-all-start = ((f32[16,8,128]{2,1,0:T(8,128)}), f32[16,8,128]{2,1,0:T(8,128)S(1)}, u32[]{:S(2)}, u32[]{:S(2)}) async-start(f32[16,8,128]{2,1,0:T(8,128)} %get-tuple-element.20), calls=%async_computation | async-start | bytes 131072 | tf_op jit(solution)/shard_map/all_to_all | solution.py:21
  23.1 4.3 %copy-start.7 = (f32[1,16]{1,0:T(1,128)S(1)}, f32[1,16]{1,0:T(1,128)}, u32[]{:S(2)}) copy-start(f32[1,16]{1,0:T(1,128)} %get-tuple-element.38.sin) | copy-start | bytes 196
  23.1 4.3 %copy-start.8 = (f32[1,16]{1,0:T(1,128)S(1)}, f32[1,16]{1,0:T(1,128)}, u32[]{:S(2)}) copy-start(f32[1,16]{1,0:T(1,128)} %get-tuple-element.39.cos) | copy-start | bytes 196
  26.2 16.1 %copy-start.3 = (bf16[64,2048]{1,0:T(8,128)(2,1)S(1)}, bf16[64,2048]{1,0:T(8,128)(2,1)}, u32[]{:S(2)}) copy-start(bf16[64,2048]{1,0:T(8,128)(2,1)} %w_output.1) | copy-start | bytes 786436
  26.3 16.1 %copy-start.5 = (bf16[512,64]{0,1:T(8,128)(2,1)S(1)}, bf16[512,64]{0,1:T(8,128)(2,1)}, u32[]{:S(2)}) copy-start(bf16[512,64]{0,1:T(8,128)(2,1)} %param.37) | copy-start | bytes 196612
  26.3 16.1 %copy-start.9 = (bf16[64]{0:T(256)(128)(2,1)S(1)}, bf16[64]{0:T(256)(128)(2,1)}, u32[]{:S(2)}) copy-start(bf16[64]{0:T(256)(128)(2,1)} %gain.6) | copy-start | bytes 388
  26.3 26.8 %copy-start.4 = (bf16[16,2048]{1,0:T(8,128)(2,1)S(1)}, bf16[16,2048]{1,0:T(8,128)(2,1)}, u32[]{:S(2)}) copy-start(bf16[16,2048]{1,0:T(8,128)(2,1)} %hidden.3) | copy-start | bytes 196612
  26.3 37.2 %copy-start.6 = (bf16[2048]{0:T(1024)(128)(2,1)S(1)}, bf16[2048]{0:T(1024)(128)(2,1)}, u32[]{:S(2)}) copy-start(bf16[2048]{0:T(1024)(128)(2,1)} %gain.7) | copy-start | bytes 12292
  27.4 51.7 %copy-start.10 = (f32[16,4]{0,1:T(4,128)S(1)}, f32[16,4]{0,1:T(4,128)}, u32[]{:S(2)}) copy-start(f32[16,4]{0,1:T(4,128)} %param.42) | copy-start | bytes 772
  65.0 31.9 %copy-start = (bf16[1,2048,128]{2,1,0:T(8,128)(2,1)S(1)}, bf16[1,2048,128]{2,1,0:T(8,128)(2,1)}, u32[]{:S(2)}) copy-start(bf16[1,2048,128]{2,1,0:T(8,128)(2,1)} %w_gate.1) | copy-start | bytes 1572868
  65.0 31.9 %copy-start.1 = (bf16[1,2048,128]{2,1,0:T(8,128)(2,1)S(1)}, bf16[1,2048,128]{2,1,0:T(8,128)(2,1)}, u32[]{:S(2)}) copy-start(bf16[1,2048,128]{2,1,0:T(8,128)(2,1)} %w_up.1) | copy-start | bytes 1572868
  65.0 31.9 %copy-start.2 = (bf16[1,128,2048]{2,1,0:T(8,128)(2,1)S(1)}, bf16[1,128,2048]{2,1,0:T(8,128)(2,1)}, u32[]{:S(2)}) copy-start(bf16[1,128,2048]{2,1,0:T(8,128)(2,1)} %w_down.1) | copy-start | bytes 1572868
  65.0 31.9 %all-to-all-start.4 = ((bf16[64,32,128]{2,1,0:T(8,128)(2,1)}), bf16[64,32,128]{2,1,0:T(8,128)(2,1)S(1)}, u32[]{:S(2)}, u32[]{:S(2)}) async-start(bf16[64,32,128]{2,1,0:T(8,128)(2,1)} %get-tuple-element.30), calls=%async_computation.4 | async-start | bytes 1048576 | tf_op jit(solution)/shard_map/all_to_all | solution.py:21

commit v4 on v3

v4 whole, which is shorter than its diff:
```python
import jax
import jax.numpy as jnp
from jax import lax
from jax.experimental import pallas as pl
from jax.experimental.pallas import tpu as pltpu
from jax.sharding import PartitionSpec as P

MODEL_WIDTH = 2048
PLAIN_QUERY = 64
ROPE = 32
HALF = 16
LATENT_UNITS = 512
CAP = 2
LANES = 128
F32 = jnp.float32
BF16 = jnp.bfloat16
EPS = 1e-06


def exchange(x, axis, groups=None):
    return lax.all_to_all(
        x, axis, split_axis=0, concat_axis=0, axis_index_groups=groups, tiled=True
    )


def core_swap(x):
    return lax.ppermute(x, "tp", [(i, i ^ 1) for i in range(lax.axis_size("tp"))])


def dot32(a, b):
    return jnp.dot(a, b, preferred_element_type=F32)


def dot_t(a, b):
    return lax.dot_general(a, b, (((1,), (1,)), ((), ())), preferred_element_type=F32)


def call(body, outs, args, smem=(), hbm=(), raw=(), scratch=(), leave=()):
    vmem = pl.BlockSpec(memory_space=pltpu.VMEM)
    kinds = {i: pl.BlockSpec(memory_space=pltpu.SMEM) for i in smem}
    kinds.update({i: pl.BlockSpec(memory_space=pl.ANY) for i in raw})
    free = set(smem) | set(hbm) | set(raw)
    scalars = set(smem)
    args = [
        x
        if i in scalars
        else pltpu.with_memory_space_constraint(x, pltpu.HBM if i in free else pltpu.VMEM)
        for i, x in enumerate(args)
    ]
    leaves, tree = jax.tree.flatten(outs)
    outs = tree.unflatten(
        (pltpu.HBM if i in leave else pltpu.VMEM)(o.shape, o.dtype) for i, o in enumerate(leaves)
    )
    return pl.pallas_call(
        body,
        out_shape=outs,
        in_specs=[kinds.get(i, vmem) for i in range(len(args))],
        out_specs=tree.unflatten(vmem for _ in leaves),
        scratch_shapes=list(scratch),
        compiler_params=pltpu.CompilerParams(vmem_limit_bytes=16 * 1024 * 1024),
    )(*args)


def together(*values):
    return lax.optimization_barrier(values)


def shape(dims, dtype):
    return jax.ShapeDtypeStruct(dims, dtype)


def row(gain):
    return gain[...].astype(F32).reshape(1, -1)


def query_body(hidden, gain, w_nope, w_rope, key_up, out, normed_out):
    values = hidden[...].astype(F32)
    factor = lax.rsqrt(jnp.mean(values * values, axis=-1, keepdims=True) + EPS)
    normed = (values * factor * row(gain)).astype(BF16)
    normed_out[...] = normed
    nope = dot_t(normed, w_nope[...]).astype(BF16)
    rope = dot_t(normed, w_rope[...]).astype(BF16).astype(F32)
    latent = dot32(nope, key_up[...]).astype(BF16).astype(F32)
    for s in range(LATENT_UNITS // LANES):
        out[:, s, :] = latent[:, s * LANES : (s + 1) * LANES]
    rows = out.shape[0]
    out[:, 4, :] = jnp.concatenate([rope, jnp.zeros((rows, LANES - ROPE), F32)], axis=1)
    for s in range(5, 8):
        out[:, s, :] = jnp.zeros((rows, LANES), F32)


def rotated(values, cos, sin):
    first, second = values[:, :HALF], values[:, HALF:ROPE]
    return jnp.concatenate([first * cos - second * sin, first * sin + second * cos], axis=1)


def new_token_body(
    index, normed, w_latent, w_key, gain, cos, sin, cache, rotary, out, cache_out, sems
):
    places, width = cache.shape[1:]
    copies = [pltpu.make_async_copy(cache.at[0], cache_out.at[pl.ds(0, places)], sems.at[0])]
    for k in range(rotary.shape[2] // width):
        source = rotary.at[0, :, pl.ds(k * width, width)]
        target = cache_out.at[pl.ds(places + k * ROPE, ROPE)]
        copies.append(pltpu.make_async_copy(source, target, sems.at[k + 1]))
    for copy in copies:
        copy.start()
    latent = dot32(normed[...], w_latent[...])
    key = dot_t(normed[...], w_key[...])
    rows = lax.broadcasted_iota(jnp.int32, (latent.shape[0], 1), 0)
    mine = rows == index[0]
    latent = jnp.sum(jnp.where(mine, latent, 0.0), axis=0, keepdims=True)
    key = jnp.sum(jnp.where(mine, key, 0.0), axis=0, keepdims=True)
    factor = lax.rsqrt(jnp.mean(latent * latent, axis=-1, keepdims=True) + EPS)
    out[:, :LATENT_UNITS] = (latent * factor * row(gain)).astype(BF16).astype(F32)
    key = rotated(key, cos[...], sin[...]).astype(BF16).astype(F32)
    out[:, LATENT_UNITS:] = jnp.concatenate([key, jnp.zeros((1, LANES - ROPE), F32)], axis=1)
    for copy in copies:
        copy.wait()


def attention_body(lengths, queries, caches, token, cos, sin, out):
    new_latent = token[:, :LATENT_UNITS]
    new_key = token[:, LATENT_UNITS : LATENT_UNITS + ROPE]
    parts = [queries[:, s, :] for s in range(LATENT_UNITS // LANES)]
    query = jnp.concatenate(parts, axis=1)
    rope = rotated(queries[:, 4, :], cos[...], sin[...]).astype(BF16)
    scale = (PLAIN_QUERY + ROPE) ** (-0.5)
    count = caches.shape[0] * LATENT_UNITS // (LATENT_UNITS + ROPE)
    cache = caches[:count, :]
    turned = [
        dot32(rope, caches[count + k * ROPE : count + (k + 1) * ROPE, :])
        for k in range(count // LATENT_UNITS)
    ]
    scores = dot_t(query.astype(BF16), cache) + jnp.concatenate(turned, axis=1)
    place = lax.broadcasted_iota(jnp.int32, scores.shape, 1)
    scores = jnp.where(place < lengths[0], scores * scale, -jnp.inf)
    own = jnp.sum(query * new_latent, axis=1, keepdims=True)
    own = own + jnp.sum(rope.astype(F32) * new_key, axis=1, keepdims=True)
    own = own * scale
    peak = jnp.maximum(jnp.max(scores, axis=1, keepdims=True), own)
    cache_exp = jnp.exp(scores - peak)
    own_exp = jnp.exp(own - peak)
    total = jnp.sum(cache_exp, axis=1, keepdims=True) + own_exp
    probs = (cache_exp / total).astype(BF16)
    own_probs = (own_exp / total).astype(BF16).astype(F32)
    mixed = dot32(probs, cache) + own_probs * new_latent
    mixed = mixed.astype(BF16).astype(F32)
    heads = mixed.shape[0]
    even = lax.broadcasted_iota(jnp.int32, mixed.shape, 0) % 2 == 0
    first = jnp.where(even, mixed, pltpu.roll(mixed, 1, 0))
    second = jnp.where(even, pltpu.roll(mixed, heads - 1, 0), mixed)
    count = LATENT_UNITS // LANES
    for s in range(count):
        tile = slice(s * LANES, (s + 1) * LANES)
        out[:, s, :] = first[:, tile]
        out[:, count + s, :] = second[:, tile]


def tile_at(number):
    return pl.ds(pl.multiple_of(number * LANES, LANES), LANES)


def slot_rows(ids_t, slots):
    top, tokens = ids_t.shape
    place = lax.broadcasted_iota(jnp.int32, (slots, tokens), 0)
    hits = [ids_t[k : k + 1, :] == place // CAP for k in range(top)]
    named = jnp.zeros((slots, tokens), F32)
    for hit in hits:
        named = named + jnp.where(hit, 1.0, 0.0)
    i = lax.broadcasted_iota(jnp.int32, (tokens, tokens), 0)
    j = lax.broadcasted_iota(jnp.int32, (tokens, tokens), 1)
    before = dot32(named.astype(BF16), jnp.where(i < j, 1.0, 0.0).astype(BF16))
    return jnp.where(before == (place % CAP).astype(F32), named, 0.0), hits


def prepare_body(index, ids_t, weights_t, value_up, gain, w_output, pack, combine):
    other = 1 - index[0] % 2
    rows = value_up.shape[0]
    pack[:rows, :LATENT_UNITS] = value_up[...]
    for m in range(8):
        at = LATENT_UNITS + m * LANES
        pack[:rows, at : at + LANES] = w_output[:, tile_at(2 * m + other)]
    wide_gain = jnp.concatenate([row(gain), jnp.zeros((1, LANES - rows), F32)], axis=1)
    pack[rows:, :] = jnp.zeros((16, pack.shape[1]), BF16)
    pack[rows:, :LANES] = jnp.broadcast_to(wide_gain, (16, LANES)).astype(BF16)

    tokens = ids_t.shape[1]
    taken, hits = slot_rows(ids_t, combine.shape[1])
    total = jnp.zeros(taken.shape, F32)
    for k, hit in enumerate(hits):
        total = total + jnp.where(hit, weights_t[k : k + 1, :], 0.0)
    total = jnp.where(taken > 0.0, total, 0.0)
    i = lax.broadcasted_iota(jnp.int32, (tokens, tokens), 0)
    j = lax.broadcasted_iota(jnp.int32, (tokens, tokens), 1)
    unit = jnp.where(i == j, 1.0, 0.0).astype(BF16)
    for p in range(3):
        part = total.astype(BF16)
        combine[p * tokens : (p + 1) * tokens, :] = dot_t(unit, part).astype(BF16)
        total = total - part.astype(F32)


def head_values(values, value_up, gains):
    head = dot_t(values.astype(BF16), value_up)
    factor = lax.rsqrt(jnp.mean(head * head, axis=-1, keepdims=True) + EPS)
    return (head * factor * gains).astype(BF16)


def head_body(index, attended, value_up, gain, w_output, pack, out):
    core = index[0] % 2
    count = LATENT_UNITS // LANES
    first = jnp.concatenate([attended[:, s, :] for s in range(count)], axis=1)
    second = jnp.concatenate([attended[:, count + s, :] for s in range(count)], axis=1)
    rows = value_up.shape[0]
    own = head_values(jnp.where(core == 0, first, second), value_up[...], row(gain))
    gains = pack[rows:, :LANES].astype(F32)[:1, :rows]
    other = head_values(
        jnp.where(core == 0, second, first), pack[:rows, :LATENT_UNITS], gains
    )
    tokens = own.shape[0]
    shares = dot32(other, pack[:rows, LATENT_UNITS:])
    for m in range(8):
        share = dot32(own, w_output[:, tile_at(2 * m + core)])
        share = (share + shares[:, m * LANES : (m + 1) * LANES]).astype(BF16)
        for p in range(out.shape[0]):
            out[p, m * tokens : (m + 1) * tokens, :] = share


def middle_body(index, shares, hidden, ids_t, middle_out, out, wide):
    core = index[0] % 2
    peers = shares.shape[0]
    tokens = hidden.shape[0]
    slots = wide.shape[0] // 8
    dispatch = slot_rows(ids_t, slots)[0].astype(BF16)
    for m in range(8):
        at = slice(m * tokens, (m + 1) * tokens)
        total = shares[0, at, :].astype(F32)
        for p in range(1, peers):
            total = total + shares[p, at, :].astype(F32)
        middle = (hidden[:, tile_at(2 * m + core)].astype(F32) + total).astype(BF16)
        middle_out[at, :] = middle
        wide[pl.ds(m, slots, stride=8), :] = dot32(dispatch, middle)
    rows = out.shape[1]
    for p in range(out.shape[0]):
        out[p] = wide[p * rows : (p + 1) * rows, :].astype(BF16)


def side_body(
    index, middle, other, gain, w_gate, w_up, w_shared_down, w_dense_up, w_dense_down, gate,
    own_out, other_out,
):
    core = index[0] % 2
    tokens = middle.shape[0] // 8
    tiles = []
    for j in range(16):
        at = slice(j // 2 * tokens, (j // 2 + 1) * tokens)
        mine, theirs = middle[at, :].astype(F32), other[at, :].astype(F32)
        tiles.append(jnp.where(core == j % 2, mine, theirs))
    values = jnp.concatenate(tiles, axis=1)
    factor = lax.rsqrt(jnp.mean(values * values, axis=-1, keepdims=True) + EPS)
    x = (values * factor * row(gain)).astype(BF16)
    pre = dot_t(x, w_gate[...])
    shared = (pre / (1.0 + jnp.exp(-pre)) * dot_t(x, w_up[...])).astype(BF16)
    dense = jax.nn.gelu(dot32(x, w_dense_up[...])).astype(BF16)
    logit = jnp.sum(x.astype(F32) * row(gate), axis=1, keepdims=True)
    mix = 1.0 / (1.0 + jnp.exp(-logit))
    side = dot32(shared, w_shared_down[...]) + mix * dot32(dense, w_dense_down[...])
    for m in range(8):
        at = slice(m * tokens, (m + 1) * tokens)
        low = side[:, 2 * m * LANES : (2 * m + 1) * LANES]
        high = side[:, (2 * m + 1) * LANES : (2 * m + 2) * LANES]
        own_out[at, :] = jnp.where(core == 0, low, high)
        other_out[at, :] = jnp.where(core == 0, high, low)


def expert_body(
    index, arrived, other, gain, *refs,
):
    weights, (out, wide, wide_other, rows_in, gains, *held, sems) = refs[:6], refs[6:]
    copies = [
        pltpu.make_async_copy(weight.at[0], place, sems.at[k])
        for k, (weight, place) in enumerate(zip(weights, held))
    ]
    for copy in copies:
        copy.start()
    core = index[0] % 2
    peers, rows, _ = arrived.shape
    slots = peers * rows // 8
    gains[...] = row(gain)
    for p in range(peers):
        at = slice(p * rows, (p + 1) * rows)
        wide[at, :] = arrived[p].astype(F32)
        wide_other[at, :] = other[p].astype(F32)
    square = jnp.zeros((slots, LANES), F32)
    for m in range(8):
        mine = wide[pl.ds(m, slots, stride=8), :]
        theirs = wide_other[pl.ds(m, slots, stride=8), :]
        square = square + mine * mine + theirs * theirs
    mean = jnp.sum(square, axis=1, keepdims=True) * (1.0 / MODEL_WIDTH)
    factor = lax.rsqrt(mean + EPS)
    for m in range(8):
        for source, number in ((wide, 2 * m + core), (wide_other, 2 * m + 1 - core)):
            values = source[pl.ds(m, slots, stride=8), :]
            normed = values * factor * gains[:, tile_at(number)]
            rows_in[:, tile_at(number)] = normed.astype(BF16)
    x = rows_in[...]
    acts = []
    for gate, up in ((0, 1), (3, 4)):
        copies[gate].wait()
        pre = dot32(x, held[gate][...])
        copies[up].wait()
        acts.append((pre / (1.0 + jnp.exp(-pre)) * dot32(x, held[up][...])).astype(BF16))
    copies[2].wait()
    copies[5].wait()
    for m in range(8):
        at = tile_at(2 * m + core)
        part = dot32(acts[0], held[2][:, at]) + dot32(acts[1], held[5][:, at])
        wide[pl.ds(m, slots, stride=8), :] = part
    for p in range(peers):
        out[p] = wide[p * rows : (p + 1) * rows, :].astype(BF16)


def combine_body(returned, weights, side, out, wide):
    peers, rows, _ = returned.shape
    slots = peers * rows // 8
    tokens = side.shape[0] // 8
    for p in range(peers):
        wide[p * rows : (p + 1) * rows, :] = returned[p].astype(F32)
    for m in range(8):
        block = wide[pl.ds(m, slots, stride=8), :].astype(BF16)
        sums = dot32(weights[...], block)
        routed = sums[:tokens] + sums[tokens : 2 * tokens] + sums[2 * tokens :]
        at = slice(m * tokens, (m + 1) * tokens)
        out[m] = (routed + side[at, :]).astype(BF16)


def final_body(index, tiles, middle, out):
    total = tiles[0].astype(F32)
    for j in range(1, tiles.shape[0]):
        total = total + tiles[j].astype(F32)
    tokens = out.shape[0]
    start = pl.multiple_of(index[0] // 2 * tokens, tokens)
    out[...] = (middle[pl.ds(start, tokens), :].astype(F32) + total).astype(BF16)


def on_device(
    hidden,
    lengths,
    latent_cache,
    cache_rotary,
    attn_gain,
    w_query_nope,
    w_query_rope,
    latent_weight,
    w_rotary_key,
    latent_norm_gain,
    key_up_weight,
    value_up_weight,
    head_gain,
    w_output,
    ffn_gain,
    expert_ids,
    expert_weights,
    w_expert_gate,
    w_expert_up,
    w_expert_down,
    w_shared_gate,
    w_shared_up,
    w_shared_down,
    w_dense_up,
    w_dense_down,
    dense_gate,
):
    tp = lax.axis_size("tp")
    ep = lax.axis_size("ep")
    index = lax.axis_index("tp").astype(jnp.int32).reshape(1)
    tokens = hidden.shape[0]
    slots = ep * CAP
    places = latent_cache.shape[1]
    chips = tp // 2
    same_core = [list(range(core, tp, 2)) for core in range(2)]
    small = shape((tp, 8, LANES), F32)
    half = (chips * tokens, LANES)
    large = shape((ep, slots * chips // ep, LANES), BF16)
    wide = pltpu.VMEM((slots * chips, LANES), F32)

    payload, normed = call(
        query_body,
        (small, shape(hidden.shape, BF16)),
        (hidden, attn_gain, w_query_nope.T, w_query_rope.T, key_up_weight),
        hbm=range(5),
        leave=(0,),
    )
    queries = exchange(payload, "tp")

    inverse = 1.0 / 10000.0 ** (jnp.arange(HALF, dtype=F32) / HALF)
    angles = lengths.astype(F32)[:, None] * inverse[None, :]
    cos, sin = jnp.cos(angles), jnp.sin(angles)
    token, cache = call(
        new_token_body,
        (
            shape((1, LATENT_UNITS + LANES), F32),
            shape((places + places * ROPE // LATENT_UNITS, LATENT_UNITS), BF16),
        ),
        (
            index,
            normed,
            latent_weight,
            w_rotary_key.T,
            latent_norm_gain,
            cos,
            sin,
            latent_cache,
            cache_rotary,
        ),
        smem=(0,),
        hbm=(2, 3, 4, 5, 6),
        raw=(7, 8),
        scratch=(pltpu.SemaphoreType.DMA((1 + places // LATENT_UNITS,)),),
    )
    queries, token = together(queries, token)

    payload = call(
        attention_body,
        small,
        (lengths, queries, cache, token, cos, sin),
        smem=(0,),
        leave=(0,),
    )
    payload, later = together(payload, index)
    attended = exchange(payload, "tp")
    pack, combine = call(
        prepare_body,
        (
            shape((PLAIN_QUERY + 16, LATENT_UNITS + chips * LANES), BF16),
            shape((3 * tokens, slots), BF16),
        ),
        (later, expert_ids.T, expert_weights.T, value_up_weight.T, head_gain, w_output),
        smem=(0,),
        hbm=range(1, 6),
    )
    pack = core_swap(pack)
    attended, pack, combine = together(attended, pack, combine)

    payload = call(
        head_body,
        shape((chips,) + half, BF16),
        (index, attended, value_up_weight.T, head_gain, w_output, pack),
        smem=(0,),
        leave=(0,),
    )
    own_weights = (w_expert_gate, w_expert_up, w_expert_down)
    payload, *weights = together(payload, *own_weights)
    shares = exchange(payload, "tp", same_core)
    weights = [core_swap(w) for w in weights]
    shares, *weights = together(shares, *weights)

    middle, payload = call(
        middle_body,
        (shape(half, BF16), large),
        (index, shares, hidden, expert_ids.T),
        smem=(0,),
        scratch=(wide,),
        leave=(1,),
    )
    payload, later = together(payload, middle)
    arrived = exchange(payload, "ep")
    other = core_swap(later)
    arrived, other = together(arrived, other)
    payload = call(
        expert_body,
        large,
        (
            index,
            arrived,
            core_swap(arrived),
            ffn_gain,
            *own_weights,
            *weights,
        ),
        smem=(0,),
        raw=range(4, 10),
        leave=(0,),
        scratch=(
            wide,
            wide,
            pltpu.VMEM((slots, MODEL_WIDTH), BF16),
            pltpu.VMEM((1, MODEL_WIDTH), F32),
            *(pltpu.VMEM(w.shape[1:], BF16) for w in own_weights * 2),
            pltpu.SemaphoreType.DMA((6,)),
        ),
    )
    payload, later, other = together(payload, later, other)
    returned = exchange(payload, "ep")
    side, away = call(
        side_body,
        (shape(half, F32), shape(half, F32)),
        (
            index,
            later,
            other,
            ffn_gain,
            w_shared_gate.T,
            w_shared_up.T,
            w_shared_down,
            w_dense_up,
            w_dense_down,
            dense_gate,
        ),
        smem=(0,),
        hbm=range(3, 10),
        leave=(1,),
    )
    away = core_swap(away)
    returned, side = together(returned, side + away)

    payload = call(
        combine_body,
        shape((chips, tokens, LANES), BF16),
        (returned, combine, side),
        scratch=(wide,),
    )
    parts = exchange(payload, "tp", same_core)
    return call(
        final_body, shape((tokens, LANES), BF16), (index, parts, middle), smem=(0,), leave=(0,)
    )


def solution(mesh):
    placed = (
        P("ep", None),
        P(("ep", "tp")),
        P(("ep", "tp"), None, None),
        P(("ep", "tp"), None, None),
        P(),
        P(None, "tp"),
        P(None, "tp"),
        P(),
        P(),
        P(),
        P("tp", None),
        P(None, "tp"),
        P("tp"),
        P("tp", None),
        P(),
        P("ep", None),
        P("ep", None),
        P("ep", None, "tp"),
        P("ep", None, "tp"),
        P("ep", "tp", None),
        P(None, "tp"),
        P(None, "tp"),
        P("tp", None),
        P(None, "tp"),
        P("tp", None),
        P(),
    )
    return jax.shard_map(
        on_device, mesh=mesh, in_specs=placed, out_specs=P("ep", "tp"), check_vma=False
    )
```

time: 137 us -> 136 us (level); the launches traced: 136 us -> 133 us
  blocking collectives: 71.5 us -> 36.6 us
  starting transfers between devices: 31.5 us -> 54.2 us
  waiting for transfers between devices: 16.8 us -> 23.1 us
  Pallas kernels: 12.7 us -> 17.9 us
    all_to_all x5 -> x3, blocking collectives: 71.5 us -> 36.6 us  [exchange(): lax.all_to_all(x, axis, split_axis=0, concat_axis=0, axis_index_groups=gr...]
    ppermute x0 -> x7, starting transfers between devices: none -> 18.3 us  [core_swap(): lax.ppermute(x, 'tp', [(i, i ^ 1) for i in range(lax.axis_size('tp'))])]
    pallas_call x10, Pallas kernels: 12.7 us -> 17.9 us  [call(): pl.pallas_call(body, out_shape=outs, in_specs=[kinds.get(i, vmem) for i i...]
    all_to_all x2 -> x3, starting transfers between devices: 31.5 us -> 36 us  [exchange(): lax.all_to_all(x, axis, split_axis=0, concat_axis=0, axis_index_groups=gr...]
    all_to_all x2 -> x3, waiting for transfers between devices: 16.8 us -> 20 us  [exchange(): lax.all_to_all(x, axis, split_axis=0, concat_axis=0, axis_index_groups=gr...]
    ppermute x0 -> x7, waiting for transfers between devices: none -> 3.08 us  [core_swap(): lax.ppermute(x, 'tp', [(i, i ^ 1) for i in range(lax.axis_size('tp'))])]
  transfers between devices with their start and end apart: 2 -> 10, of which waited for: 2 -> 6; matrix products, arithmetic and copies ran while one was open for 2% -> 0% of each run, Pallas kernels for 4% -> 4%
where the time goes in v4:
time: 136 us; the launch traced here: 133 us
  starting transfers between devices  54.2 us (40%)
  blocking collectives  36.6 us (27%)
  waiting for transfers between devices  23.1 us (17%)
  Pallas kernels  17.9 us (13%)
    all_to_all x3, blocking collectives, exchange(): lax.all_to_all(x, axis, split_axis=0, concat_axis=0, axis_index_groups=gr...  36.6 us
    all_to_all x3, starting transfers between devices, exchange(): lax.all_to_all(x, axis, split_axis=0, concat_axis=0, axis_index_groups=gr...  36 us
    all_to_all x3, waiting for transfers between devices, exchange(): lax.all_to_all(x, axis, split_axis=0, concat_axis=0, axis_index_groups=gr...  20 us
    ppermute x7, starting transfers between devices, core_swap(): lax.ppermute(x, 'tp', [(i, i ^ 1) for i in range(lax.axis_size('tp'))])  18.3 us
    pallas_call x10, Pallas kernels, call(): pl.pallas_call(body, out_shape=outs, in_specs=[kinds.get(i, vmem) for i i...  17.9 us
    ppermute x7, waiting for transfers between devices, core_swap(): lax.ppermute(x, 'tp', [(i, i ^ 1) for i in range(lax.axis_size('tp'))])  3.08 us
  transfers between devices with their start and end apart: 10, of which 6 were waited for; matrix products, arithmetic and copies ran while one was open for 0% of the time, Pallas kernels for 4%

profile of v4, /device:TPU:1, one launch (start us, length us, event | category | flops | bytes accessed | tf_op | source)
XLA Modules:
  0.0 133.5 jit_solution(13803039581351200634)
XLA Ops:
  0.0 2.2 %shard_map.244 = (f32[16,8,128]{2,1,0:T(8,128)}, bf16[16,2048]{1,0:T(8,128)(2,1)S(1)}) custom-call(bf16[16,2048]{1,0:T(8,128)(2,1)} %hidden.3, bf16[2048]{0:T(1024)(128)(2,1)} %gain.6, bf16[64,2048]{1,0:T(8,128)(2,1)} %bitcast.14, bf16[32,2048]{1,0:T(8,128)(2,1)} %bitcast.17, bf16[64,512]{1,0:T(8,128)(2,1)} %key_up.1), custom_call_target="tpu_custom_call" | custom-call | tf_op jit(solution)/shard_map/pallas_call | solution.py:54
  2.2 17.4 %all-to-all-start = ((f32[16,8,128]{2,1,0:T(8,128)}), f32[16,8,128]{2,1,0:T(8,128)S(1)}, u32[]{:S(2)}, u32[]{:S(2)}) async-start(f32[16,8,128]{2,1,0:T(8,128)} %get-tuple-element.39), calls=%async_computation | async-start | bytes 131072 | tf_op jit(solution)/shard_map/all_to_all | solution.py:21
  20.2 0.6 fusion
  20.9 3.1 %shard_map.245 = (f32[1,640]{1,0:T(1,128)S(1)}, bf16[1632,512]{1,0:T(8,128)(2,1)S(1)}) custom-call(s32[1]{0:T(128)} %bitcast.index, bf16[16,2048]{1,0:T(8,128)(2,1)S(1)} %get-tuple-element.40.normed, bf16[2048,512]{1,0:T(8,128)(2,1)} %w_latent.1, bf16[32,2048]{1,0:T(8,128)(2,1)} %bitcast.18, bf16[512]{0:T(512)(128)(2,1)} %gain.7, ...), custom_call_target="tpu_custom_call" | custom-call | tf_op jit(solution)/shard_map/pallas_call | solution.py:54
  24.0 0.0 copy-start
  24.0 0.0 copy-start.2
  24.0 0.0 copy-start.5
  24.0 0.0 copy-start.8
  24.0 0.0 copy-start.9
  24.1 3.3 %all-to-all-done.queries = f32[16,8,128]{2,1,0:T(8,128)S(1)} async-done(((f32[16,8,128]{2,1,0:T(8,128)}), f32[16,8,128]{2,1,0:T(8,128)S(1)}, u32[]{:S(2)}, u32[]{:S(2)}) %all-to-all-start) | async-done | bytes 65568 | tf_op jit(solution)/shard_map/all_to_all | solution.py:21
  27.4 0.0 copy-done.6
  27.4 0.0 copy-done.7
  27.4 0.0 copy-start.4
  27.4 1.8 %shard_map.246 = f32[16,8,128]{2,1,0:T(8,128)} custom-call(s32[1]{0:T(128)S(6)} %copy.27.lengths, f32[16,8,128]{2,1,0:T(8,128)S(1)} %all-to-all-done.queries, bf16[1632,512]{1,0:T(8,128)(2,1)S(1)} %get-tuple-element.43.caches, f32[1,640]{1,0:T(1,128)S(1)} %get-tuple-element.44.token, f32[1,16]{1,0:T(1,128)S(1)} %copy-done.7, f32[1,16]{1,0:T(1,128)S(1)} %copy-done.6), custom_call_target="tpu_custom_call" | custom-call | tf_op jit(solution)/shard_map/pallas_call | solution.py:54
  29.3 1.3 %shard_map.247 = (bf16[80,1536]{1,0:T(8,128)(2,1)S(1)}, bf16[48,128]{1,0:T(8,128)(2,1)S(1)}) custom-call(s32[1]{0:T(128)} %bitcast.index, s32[4,16]{1,0:T(4,128)} %bitcast.12, f32[4,16]{1,0:T(4,128)} %bitcast.19, bf16[64,512]{1,0:T(8,128)(2,1)} %bitcast.10, bf16[64]{0:T(256)(128)(2,1)} %gain.9, bf16[64,2048]{1,0:T(8,128)(2,1)} %w_output.3), custom_call_target="tpu_custom_call" | custom-call | tf_op jit(solution)/shard_map/pallas_call | solution.py:54
  30.6 2.1 %collective-permute-start = (bf16[80,1536]{1,0:T(8,128)(2,1)S(1)}, bf16[80,1536]{1,0:T(8,128)(2,1)S(1)}, u32[]{:S(2)}, u32[]{:S(2)}) collective-permute-start(bf16[80,1536]{1,0:T(8,128)(2,1)S(1)} %get-tuple-element.47), channel_id=1, source_target_pairs={{0,1},{1,0},{2,3},{3,2},{4,5},{5,4},{6,7},{7,6},{8,9},{9,8},{10,11... | collective-permute-start | bytes 737288 | tf_op jit(solution)/shard_map/ppermute | solution.py:27
  32.7 11.7 %all_to_all.30.attended = f32[16,8,128]{2,1,0:T(8,128)S(1)} all-to-all(f32[16,8,128]{2,1,0:T(8,128)} %shard_map.246), channel_id=1, replica_groups=mesh['ep'=64,'tp'=16] {'tp'}, dimensions={0} | all-to-all | bytes 131072 | tf_op jit(solution)/shard_map/all_to_all | solution.py:21
  44.4 0.0 collective-permute-done.pack
  44.4 0.0 copy-done
  44.4 0.0 copy-done.2
  44.4 1.1 shard_map.248
  45.6 2.0 %collective-permute-start.1 = (bf16[1,2048,128]{2,1,0:T(8,128)(2,1)S(1)}, bf16[1,2048,128]{2,1,0:T(8,128)(2,1)S(1)}, u32[]{:S(2)}, u32[]{:S(2)}) collective-permute-start(bf16[1,2048,128]{2,1,0:T(8,128)(2,1)S(1)} %copy-done.8), channel_id=1, source_target_pairs={{0,1},{1,0},{2,3},{3,2},{4,5},{5,4},{6,7},{7,6},{8,9},{9,8},{10,11... | collective-permute-start | bytes 1572872 | tf_op jit(solution)/shard_map/ppermute | solution.py:27
  47.6 2.3 %collective-permute-start.2 = (bf16[1,2048,128]{2,1,0:T(8,128)(2,1)S(1)}, bf16[1,2048,128]{2,1,0:T(8,128)(2,1)S(1)}, u32[]{:S(2)}, u32[]{:S(2)}) collective-permute-start(bf16[1,2048,128]{2,1,0:T(8,128)(2,1)S(1)} %copy-done.9), channel_id=1, source_target_pairs={{0,1},{1,0},{2,3},{3,2},{4,5},{5,4},{6,7},{7,6},{8,9},{9,8},{10,11... | collective-permute-start | bytes 1572872 | tf_op jit(solution)/shard_map/ppermute | solution.py:27
  49.9 2.0 %collective-permute-start.3 = (bf16[1,128,2048]{2,1,0:T(8,128)(2,1)S(1)}, bf16[1,128,2048]{2,1,0:T(8,128)(2,1)S(1)}, u32[]{:S(2)}, u32[]{:S(2)}) collective-permute-start(bf16[1,128,2048]{2,1,0:T(8,128)(2,1)S(1)} %copy-done.10), channel_id=1, source_target_pairs={{0,1},{1,0},{2,3},{3,2},{4,5},{5,4},{6,7},{7,6},{8,9},{9,8},{10,11... | collective-permute-start | bytes 1572872 | tf_op jit(solution)/shard_map/ppermute | solution.py:27
  51.9 15.6 %all_to_all.31.shares = bf16[8,128,128]{2,1,0:T(8,128)(2,1)S(1)} all-to-all(bf16[8,128,128]{2,1,0:T(8,128)(2,1)} %shard_map.248), channel_id=1, replica_groups={{0,2,4,6,8,10,12,14},{1,3,5,7,9,11,13,15},{16,18,20,22,24,26,28,30},{17..., dimensions={0} | all-to-all | bytes 524288 | tf_op jit(solution)/shard_map/all_to_all | solution.py:21
  67.6 0.0 collective-permute-done.1.refs_3_
  67.6 0.0 collective-permute-done.2.refs_4_
  67.6 0.0 collective-permute-done.3.refs_5_
  67.6 0.0 copy-done.1
  67.6 0.0 copy-done.4
  67.6 0.0 copy-start.13
  67.6 1.2 shard_map.249
  68.8 14.0 %all-to-all-start.3 = ((bf16[64,16,128]{2,1,0:T(8,128)(2,1)}), bf16[64,16,128]{2,1,0:T(8,128)(2,1)S(1)}, u32[]{:S(2)}, u32[]{:S(2)}) async-start(bf16[64,16,128]{2,1,0:T(8,128)(2,1)} %get-tuple-element.58), calls=%async_computation.3 | async-start | bytes 524288 | tf_op jit(solution)/shard_map/all_to_all | solution.py:21
  82.8 2.7 %collective-permute-start.4 = (bf16[128,128]{1,0:T(8,128)(2,1)S(1)}, bf16[128,128]{1,0:T(8,128)(2,1)S(1)}, u32[]{:S(2)}, u32[]{:S(2)}) collective-permute-start(bf16[128,128]{1,0:T(8,128)(2,1)S(1)} %get-tuple-element.66.middle), channel_id=1, source_target_pairs={{0,1},{1,0},{2,3},{3,2},{4,5},{5,4},{6,7},{7,6},{8,9},{9,8},{10,11... | collective-permute-start | bytes 98312 | tf_op jit(solution)/shard_map/ppermute | solution.py:27
  85.5 0.8 collective-permute-done.4.other
  86.4 9.4 %all-to-all-done.3.arrived = bf16[64,16,128]{2,1,0:T(8,128)(2,1)S(1)} async-done(((bf16[64,16,128]{2,1,0:T(8,128)(2,1)}), bf16[64,16,128]{2,1,0:T(8,128)(2,1)S(1)}, u32[]{:S(2)}, u32[]{:S(2)}) %all-to-all-start.3) | async-done | bytes 262176 | tf_op jit(solution)/shard_map/all_to_all | solution.py:21
  95.7 4.8 %collective-permute-start.5 = (bf16[64,16,128]{2,1,0:T(8,128)(2,1)S(1)}, bf16[64,16,128]{2,1,0:T(8,128)(2,1)S(1)}, u32[]{:S(2)}, u32[]{:S(2)}) collective-permute-start(bf16[64,16,128]{2,1,0:T(8,128)(2,1)S(1)} %all-to-all-done.3.arrived), channel_id=1, source_target_pairs={{0,1},{1,0},{2,3},{3,2},{4,5},{5,4},{6,7},{7,6},{8,9},{9,8},{10,11... | collective-permute-start | bytes 786440 | tf_op jit(solution)/shard_map/ppermute | solution.py:27
  100.6 1.1 collective-permute-done.5.other
  101.7 0.0 copy-done.13
  101.7 3.5 %shard_map.250 = bf16[64,16,128]{2,1,0:T(8,128)(2,1)} custom-call(s32[1]{0:T(128)} %bitcast.index, bf16[64,16,128]{2,1,0:T(8,128)(2,1)S(1)} %all-to-all-done.3.arrived, bf16[64,16,128]{2,1,0:T(8,128)(2,1)S(1)} %collective-permute-done.5.other, bf16[2048]{0:T(1024)(128)(2,1)S(1)} %copy-done.3, bf16[1,2048,128]{2,1,0:T(8,128)(2,1)} %refs_0_.1, ...), custom_call_target="tpu_custom_call" | custom-call | tf_op jit(solution)/shard_map/pallas_call | solution.py:54
  105.2 4.6 %all-to-all-start.4 = ((bf16[64,16,128]{2,1,0:T(8,128)(2,1)}), bf16[64,16,128]{2,1,0:T(8,128)(2,1)S(1)}, u32[]{:S(2)}, u32[]{:S(2)}) async-start(bf16[64,16,128]{2,1,0:T(8,128)(2,1)} %shard_map.250), calls=%async_computation.4 | async-start | bytes 524288 | tf_op jit(solution)/shard_map/all_to_all | solution.py:21
  109.9 2.7 %shard_map.251 = (f32[128,128]{1,0:T(8,128)S(1)}, f32[128,128]{1,0:T(8,128)}) custom-call(s32[1]{0:T(128)} %bitcast.index, bf16[128,128]{1,0:T(8,128)(2,1)S(1)} %get-tuple-element.66.middle, bf16[128,128]{1,0:T(8,128)(2,1)S(1)} %collective-permute-done.4.other, bf16[2048]{0:T(1024)(128)(2,1)} %gain.11, bf16[64,2048]{1,0:T(8,128)(2,1)} %bitcast.15, ...), custom_call_target="tpu_custom_call" | custom-call | tf_op jit(solution)/shard_map/pallas_call | solution.py:54
  112.6 2.3 %collective-permute-start.6 = (f32[128,128]{1,0:T(8,128)}, f32[128,128]{1,0:T(8,128)S(1)}, u32[]{:S(2)}, u32[]{:S(2)}) collective-permute-start(f32[128,128]{1,0:T(8,128)} %get-tuple-element.69), channel_id=1, source_target_pairs={{0,1},{1,0},{2,3},{3,2},{4,5},{5,4},{6,7},{7,6},{8,9},{9,8},{10,11... | collective-permute-start | bytes 196616 | tf_op jit(solution)/shard_map/ppermute | solution.py:27
  114.9 1.1 collective-permute-done.6
  116.0 7.3 %all-to-all-done.4.returned = bf16[64,16,128]{2,1,0:T(8,128)(2,1)S(1)} async-done(((bf16[64,16,128]{2,1,0:T(8,128)(2,1)}), bf16[64,16,128]{2,1,0:T(8,128)(2,1)S(1)}, u32[]{:S(2)}, u32[]{:S(2)}) %all-to-all-start.4) | async-done | bytes 262176 | tf_op jit(solution)/shard_map/all_to_all | solution.py:21
  123.3 0.2 shard_map.252
  123.6 9.3 %all_to_all.32.tiles = bf16[8,16,128]{2,1,0:T(8,128)(2,1)S(1)} all-to-all(bf16[8,16,128]{2,1,0:T(8,128)(2,1)S(1)} %shard_map.252), channel_id=1, replica_groups={{0,2,4,6,8,10,12,14},{1,3,5,7,9,11,13,15},{16,18,20,22,24,26,28,30},{17..., dimensions={0} | all-to-all | bytes 65536 | tf_op jit(solution)/shard_map/all_to_all | solution.py:21
  132.9 0.6 shard_map.253
  (15 shorter events, 0.0 us)
Async XLA Ops:
  2.2 25.2 %all-to-all-start = ((f32[16,8,128]{2,1,0:T(8,128)}), f32[16,8,128]{2,1,0:T(8,128)S(1)}, u32[]{:S(2)}, u32[]{:S(2)}) async-start(f32[16,8,128]{2,1,0:T(8,128)} %get-tuple-element.39), calls=%async_computation | async-start | bytes 131072 | tf_op jit(solution)/shard_map/all_to_all | solution.py:21
  20.9 6.5 %copy-start.6 = (f32[1,16]{1,0:T(1,128)S(1)}, f32[1,16]{1,0:T(1,128)}, u32[]{:S(2)}) copy-start(f32[1,16]{1,0:T(1,128)} %get-tuple-element.73.sin) | copy-start | bytes 196
  20.9 6.5 %copy-start.7 = (f32[1,16]{1,0:T(1,128)S(1)}, f32[1,16]{1,0:T(1,128)}, u32[]{:S(2)}) copy-start(f32[1,16]{1,0:T(1,128)} %get-tuple-element.74.cos) | copy-start | bytes 196
  24.0 20.4 %copy-start = (bf16[64,2048]{1,0:T(8,128)(2,1)S(1)}, bf16[64,2048]{1,0:T(8,128)(2,1)}, u32[]{:S(2)}) copy-start(bf16[64,2048]{1,0:T(8,128)(2,1)} %w_output.3) | copy-start | bytes 786436
  24.0 20.4 %copy-start.2 = (bf16[512,64]{0,1:T(8,128)(2,1)S(1)}, bf16[512,64]{0,1:T(8,128)(2,1)}, u32[]{:S(2)}) copy-start(bf16[512,64]{0,1:T(8,128)(2,1)} %param.37) | copy-start | bytes 196612
  24.0 20.4 %copy-start.5 = (bf16[64]{0:T(256)(128)(2,1)S(1)}, bf16[64]{0:T(256)(128)(2,1)}, u32[]{:S(2)}) copy-start(bf16[64]{0:T(256)(128)(2,1)} %gain.9) | copy-start | bytes 388
  24.0 21.5 %copy-start.8 = (bf16[1,2048,128]{2,1,0:T(8,128)(2,1)S(1)}, bf16[1,2048,128]{2,1,0:T(8,128)(2,1)}, u32[]{:S(2)}) copy-start(bf16[1,2048,128]{2,1,0:T(8,128)(2,1)} %refs_0_.1) | copy-start | bytes 1572868
  24.0 23.5 %copy-start.9 = (bf16[1,2048,128]{2,1,0:T(8,128)(2,1)S(1)}, bf16[1,2048,128]{2,1,0:T(8,128)(2,1)}, u32[]{:S(2)}) copy-start(bf16[1,2048,128]{2,1,0:T(8,128)(2,1)} %refs_1_.1) | copy-start | bytes 1572868
  27.4 22.5 %copy-start.10 = (bf16[1,128,2048]{2,1,0:T(8,128)(2,1)S(1)}, bf16[1,128,2048]{2,1,0:T(8,128)(2,1)}, u32[]{:S(2)}) copy-start(bf16[1,128,2048]{2,1,0:T(8,128)(2,1)} %refs_2_.1) | copy-start | bytes 1572868
  27.4 40.2 %copy-start.1 = (bf16[16,2048]{1,0:T(8,128)(2,1)S(1)}, bf16[16,2048]{1,0:T(8,128)(2,1)}, u32[]{:S(2)}) copy-start(bf16[16,2048]{1,0:T(8,128)(2,1)} %hidden.3) | copy-start | bytes 196612
  27.4 40.2 %copy-start.4 = (s32[16,4]{0,1:T(4,128)S(1)}, s32[16,4]{0,1:T(4,128)}, u32[]{:S(2)}) copy-start(s32[16,4]{0,1:T(4,128)} %param.41) | copy-start | bytes 772
  29.3 72.5 %copy-start.3 = (bf16[2048]{0:T(1024)(128)(2,1)S(1)}, bf16[2048]{0:T(1024)(128)(2,1)}, u32[]{:S(2)}) copy-start(bf16[2048]{0:T(1024)(128)(2,1)} %gain.11) | copy-start | bytes 12292
  30.6 13.8 %collective-permute-start = (bf16[80,1536]{1,0:T(8,128)(2,1)S(1)}, bf16[80,1536]{1,0:T(8,128)(2,1)S(1)}, u32[]{:S(2)}, u32[]{:S(2)}) collective-permute-start(bf16[80,1536]{1,0:T(8,128)(2,1)S(1)} %get-tuple-element.47), channel_id=1, source_target_pairs={{0,1},{1,0},{2,3},{3,2},{4,5},{5,4},{6,7},{7,6},{8,9},{9,8},{10,11... | collective-permute-start | bytes 737288 | tf_op jit(solution)/shard_map/ppermute | solution.py:27
  45.6 22.0 %collective-permute-start.1 = (bf16[1,2048,128]{2,1,0:T(8,128)(2,1)S(1)}, bf16[1,2048,128]{2,1,0:T(8,128)(2,1)S(1)}, u32[]{:S(2)}, u32[]{:S(2)}) collective-permute-start(bf16[1,2048,128]{2,1,0:T(8,128)(2,1)S(1)} %copy-done.8), channel_id=1, source_target_pairs={{0,1},{1,0},{2,3},{3,2},{4,5},{5,4},{6,7},{7,6},{8,9},{9,8},{10,11... | collective-permute-start | bytes 1572872 | tf_op jit(solution)/shard_map/ppermute | solution.py:27
  47.6 20.0 %collective-permute-start.2 = (bf16[1,2048,128]{2,1,0:T(8,128)(2,1)S(1)}, bf16[1,2048,128]{2,1,0:T(8,128)(2,1)S(1)}, u32[]{:S(2)}, u32[]{:S(2)}) collective-permute-start(bf16[1,2048,128]{2,1,0:T(8,128)(2,1)S(1)} %copy-done.9), channel_id=1, source_target_pairs={{0,1},{1,0},{2,3},{3,2},{4,5},{5,4},{6,7},{7,6},{8,9},{9,8},{10,11... | collective-permute-start | bytes 1572872 | tf_op jit(solution)/shard_map/ppermute | solution.py:27
  49.9 17.7 %collective-permute-start.3 = (bf16[1,128,2048]{2,1,0:T(8,128)(2,1)S(1)}, bf16[1,128,2048]{2,1,0:T(8,128)(2,1)S(1)}, u32[]{:S(2)}, u32[]{:S(2)}) collective-permute-start(bf16[1,128,2048]{2,1,0:T(8,128)(2,1)S(1)} %copy-done.10), channel_id=1, source_target_pairs={{0,1},{1,0},{2,3},{3,2},{4,5},{5,4},{6,7},{7,6},{8,9},{9,8},{10,11... | collective-permute-start | bytes 1572872 | tf_op jit(solution)/shard_map/ppermute | solution.py:27
  67.6 34.1 %copy-start.11 = (bf16[1,2048,128]{2,1,0:T(8,128)(2,1)}, bf16[1,2048,128]{2,1,0:T(8,128)(2,1)S(1)}, u32[]{:S(2)}) copy-start(bf16[1,2048,128]{2,1,0:T(8,128)(2,1)S(1)} %collective-permute-done.1.refs_3_) | copy-start | bytes 1572868
  67.6 34.1 %copy-start.12 = (bf16[1,2048,128]{2,1,0:T(8,128)(2,1)}, bf16[1,2048,128]{2,1,0:T(8,128)(2,1)S(1)}, u32[]{:S(2)}) copy-start(bf16[1,2048,128]{2,1,0:T(8,128)(2,1)S(1)} %collective-permute-done.2.refs_4_) | copy-start | bytes 1572868
  67.6 34.1 %copy-start.13 = (bf16[1,128,2048]{2,1,0:T(8,128)(2,1)}, bf16[1,128,2048]{2,1,0:T(8,128)(2,1)S(1)}, u32[]{:S(2)}) copy-start(bf16[1,128,2048]{2,1,0:T(8,128)(2,1)S(1)} %collective-permute-done.3.refs_5_) | copy-start | bytes 1572868
  68.8 26.9 %all-to-all-start.3 = ((bf16[64,16,128]{2,1,0:T(8,128)(2,1)}), bf16[64,16,128]{2,1,0:T(8,128)(2,1)S(1)}, u32[]{:S(2)}, u32[]{:S(2)}) async-start(bf16[64,16,128]{2,1,0:T(8,128)(2,1)} %get-tuple-element.58), calls=%async_computation.3 | async-start | bytes 524288 | tf_op jit(solution)/shard_map/all_to_all | solution.py:21
  82.8 3.6 %collective-permute-start.4 = (bf16[128,128]{1,0:T(8,128)(2,1)S(1)}, bf16[128,128]{1,0:T(8,128)(2,1)S(1)}, u32[]{:S(2)}, u32[]{:S(2)}) collective-permute-start(bf16[128,128]{1,0:T(8,128)(2,1)S(1)} %get-tuple-element.66.middle), channel_id=1, source_target_pairs={{0,1},{1,0},{2,3},{3,2},{4,5},{5,4},{6,7},{7,6},{8,9},{9,8},{10,11... | collective-permute-start | bytes 98312 | tf_op jit(solution)/shard_map/ppermute | solution.py:27
  95.7 6.0 %collective-permute-start.5 = (bf16[64,16,128]{2,1,0:T(8,128)(2,1)S(1)}, bf16[64,16,128]{2,1,0:T(8,128)(2,1)S(1)}, u32[]{:S(2)}, u32[]{:S(2)}) collective-permute-start(bf16[64,16,128]{2,1,0:T(8,128)(2,1)S(1)} %all-to-all-done.3.arrived), channel_id=1, source_target_pairs={{0,1},{1,0},{2,3},{3,2},{4,5},{5,4},{6,7},{7,6},{8,9},{9,8},{10,11... | collective-permute-start | bytes 786440 | tf_op jit(solution)/shard_map/ppermute | solution.py:27
  105.2 18.1 %all-to-all-start.4 = ((bf16[64,16,128]{2,1,0:T(8,128)(2,1)}), bf16[64,16,128]{2,1,0:T(8,128)(2,1)S(1)}, u32[]{:S(2)}, u32[]{:S(2)}) async-start(bf16[64,16,128]{2,1,0:T(8,128)(2,1)} %shard_map.250), calls=%async_computation.4 | async-start | bytes 524288 | tf_op jit(solution)/shard_map/all_to_all | solution.py:21
  112.6 3.4 %collective-permute-start.6 = (f32[128,128]{1,0:T(8,128)}, f32[128,128]{1,0:T(8,128)S(1)}, u32[]{:S(2)}, u32[]{:S(2)}) collective-permute-start(f32[128,128]{1,0:T(8,128)} %get-tuple-element.69), channel_id=1, source_target_pairs={{0,1},{1,0},{2,3},{3,2},{4,5},{5,4},{6,7},{7,6},{8,9},{9,8},{10,11... | collective-permute-start | bytes 196616 | tf_op jit(solution)/shard_map/ppermute | solution.py:27

commit v5 on v4

--- a/solution.py
+++ b/solution.py
@@ -276,14 +276,25 @@
 def expert_body(
     index, arrived, other, gain, *refs,
 ):
-    weights, (out, wide, wide_other, rows_in, gains, *held, sems) = refs[:6], refs[6:]
-    copies = [
-        pltpu.make_async_copy(weight.at[0], place, sems.at[k])
-        for k, (weight, place) in enumerate(zip(weights, held))
-    ]
+    weights, (out, wide, wide_other, rows_in, gains, own_in, other_in, down, sems) = (
+        refs[:6],
+        refs[6:],
+    )
+    core = index[0] % 2
+    width = weights[0].shape[2]
+    pairs = []
+    for block, place in ((0, own_in), (1, other_in)):
+        for k in range(2):
+            target = place.at[:, pl.ds(k * width, width)]
+            pairs.append((weights[3 * block + k].at[0], target))
+    for block in range(2):
+        for m in range(8):
+            source = weights[3 * block + 2].at[0, :, tile_at(2 * m + core)]
+            target = down.at[pl.ds(block * width, width), pl.ds(m * LANES, LANES)]
+            pairs.append((source, target))
+    copies = [pltpu.make_async_copy(*pair, sems.at[k]) for k, pair in enumerate(pairs)]
     for copy in copies:
         copy.start()
-    core = index[0] % 2
     peers, rows, _ = arrived.shape
     slots = peers * rows // 8
     gains[...] = row(gain)
@@ -305,17 +316,17 @@
             rows_in[:, tile_at(number)] = normed.astype(BF16)
     x = rows_in[...]
     acts = []
-    for gate, up in ((0, 1), (3, 4)):
-        copies[gate].wait()
-        pre = dot32(x, held[gate][...])
-        copies[up].wait()
-        acts.append((pre / (1.0 + jnp.exp(-pre)) * dot32(x, held[up][...])).astype(BF16))
-    copies[2].wait()
-    copies[5].wait()
-    for m in range(8):
-        at = tile_at(2 * m + core)
-        part = dot32(acts[0], held[2][:, at]) + dot32(acts[1], held[5][:, at])
-        wide[pl.ds(m, slots, stride=8), :] = part
+    for block, place in ((0, own_in), (1, other_in)):
+        copies[2 * block].wait()
+        copies[2 * block + 1].wait()
+        both = dot32(x, place[...])
+        pre = both[:, :width]
+        acts.append((pre / (1.0 + jnp.exp(-pre)) * both[:, width:]).astype(BF16))
+    for copy in copies[4:]:
+        copy.wait()
+    part = dot32(jnp.concatenate(acts, axis=1), down[...])
+    for m in range(8):
+        wide[pl.ds(m, slots, stride=8), :] = part[:, m * LANES : (m + 1) * LANES]
     for p in range(peers):
         out[p] = wide[p * rows : (p + 1) * rows, :].astype(BF16)
 
@@ -447,13 +458,8 @@
         shape((chips,) + half, BF16),
         (index, attended, value_up_weight.T, head_gain, w_output, pack),
         smem=(0,),
-        leave=(0,),
-    )
-    own_weights = (w_expert_gate, w_expert_up, w_expert_down)
-    payload, *weights = together(payload, *own_weights)
+    )
     shares = exchange(payload, "tp", same_core)
-    weights = [core_swap(w) for w in weights]
-    shares, *weights = together(shares, *weights)
 
     middle, payload = call(
         middle_body,
@@ -463,10 +469,11 @@
         scratch=(wide,),
         leave=(1,),
     )
-    payload, later = together(payload, middle)
+    own_weights = (w_expert_gate, w_expert_up, w_expert_down)
+    payload, later, *weights = together(payload, middle, *own_weights)
     arrived = exchange(payload, "ep")
-    other = core_swap(later)
-    arrived, other = together(arrived, other)
+    weights = [core_swap(w) for w in weights]
+    arrived, *weights = together(arrived, *weights)
     payload = call(
         expert_body,
         large,
@@ -486,12 +493,15 @@
             wide,
             pltpu.VMEM((slots, MODEL_WIDTH), BF16),
             pltpu.VMEM((1, MODEL_WIDTH), F32),
-            *(pltpu.VMEM(w.shape[1:], BF16) for w in own_weights * 2),
-            pltpu.SemaphoreType.DMA((6,)),
+            pltpu.VMEM((MODEL_WIDTH, 2 * w_expert_gate.shape[2]), BF16),
+            pltpu.VMEM((MODEL_WIDTH, 2 * w_expert_gate.shape[2]), BF16),
+            pltpu.VMEM((2 * w_expert_down.shape[1], chips * LANES), BF16),
+            pltpu.SemaphoreType.DMA((4 + 2 * chips,)),
         ),
     )
-    payload, later, other = together(payload, later, other)
+    payload, later = together(payload, later)
     returned = exchange(payload, "ep")
+    other = core_swap(later)
     side, away = call(
         side_body,
         (shape(half, F32), shape(half, F32)),

time: 136 us -> 134 us (0.985)
  blocking collectives: 36.6 us -> 63.2 us
  starting transfers between devices: 54.2 us -> 39.5 us
  waiting for transfers between devices: 23.1 us -> 10.7 us
    all_to_all x3 -> x4, blocking collectives: 36.6 us -> 63.2 us  [exchange(): lax.all_to_all(x, axis, split_axis=0, concat_axis=0, axis_index_groups=gr...]
    all_to_all x3 -> x2, starting transfers between devices: 36 us -> 22 us  [exchange(): lax.all_to_all(x, axis, split_axis=0, concat_axis=0, axis_index_groups=gr...]
    all_to_all x3 -> x2, waiting for transfers between devices: 20 us -> 7.62 us  [exchange(): lax.all_to_all(x, axis, split_axis=0, concat_axis=0, axis_index_groups=gr...]
  transfers between devices with their start and end apart: 10 -> 9, of which waited for: 6 -> 5; matrix products, arithmetic and copies ran while one was open for 0% -> 0% of each run, Pallas kernels for 4% -> 4%
where the time goes in v5:
time: 134 us; the launch traced here: 132 us
  blocking collectives  63.2 us (47%)
  starting transfers between devices  39.5 us (29%)
  Pallas kernels  17 us (13%)
  waiting for transfers between devices  10.7 us (8%)
    all_to_all x4, blocking collectives, exchange(): lax.all_to_all(x, axis, split_axis=0, concat_axis=0, axis_index_groups=gr...  63.2 us
    all_to_all x2, starting transfers between devices, exchange(): lax.all_to_all(x, axis, split_axis=0, concat_axis=0, axis_index_groups=gr...  22 us
    ppermute x7, starting transfers between devices, core_swap(): lax.ppermute(x, 'tp', [(i, i ^ 1) for i in range(lax.axis_size('tp'))])  17.5 us
    pallas_call x10, Pallas kernels, call(): pl.pallas_call(body, out_shape=outs, in_specs=[kinds.get(i, vmem) for i i...  17 us
    all_to_all x2, waiting for transfers between devices, exchange(): lax.all_to_all(x, axis, split_axis=0, concat_axis=0, axis_index_groups=gr...  7.62 us
    ppermute x7, waiting for transfers between devices, core_swap(): lax.ppermute(x, 'tp', [(i, i ^ 1) for i in range(lax.axis_size('tp'))])  3.08 us
  transfers between devices with their start and end apart: 9, of which 5 were waited for; matrix products, arithmetic and copies ran while one was open for 0% of the time, Pallas kernels for 4%

profile of v5, /device:TPU:1, one launch (start us, length us, event | category | flops | bytes accessed | tf_op | source)
XLA Modules:
  0.0 132.0 jit_solution(16355025348408470628)
XLA Ops:
  0.0 2.2 %shard_map.244 = (f32[16,8,128]{2,1,0:T(8,128)}, bf16[16,2048]{1,0:T(8,128)(2,1)S(1)}) custom-call(bf16[16,2048]{1,0:T(8,128)(2,1)} %hidden.3, bf16[2048]{0:T(1024)(128)(2,1)} %gain.6, bf16[64,2048]{1,0:T(8,128)(2,1)} %bitcast.14, bf16[32,2048]{1,0:T(8,128)(2,1)} %bitcast.17, bf16[64,512]{1,0:T(8,128)(2,1)} %key_up.1), custom_call_target="tpu_custom_call" | custom-call | tf_op jit(solution)/shard_map/pallas_call | solution.py:54
  2.2 17.4 %all-to-all-start = ((f32[16,8,128]{2,1,0:T(8,128)}), f32[16,8,128]{2,1,0:T(8,128)S(1)}, u32[]{:S(2)}, u32[]{:S(2)}) async-start(f32[16,8,128]{2,1,0:T(8,128)} %get-tuple-element.35), calls=%async_computation | async-start | bytes 131072 | tf_op jit(solution)/shard_map/all_to_all | solution.py:21
  20.2 0.6 fusion
  20.8 3.1 %shard_map.245 = (f32[1,640]{1,0:T(1,128)S(1)}, bf16[1632,512]{1,0:T(8,128)(2,1)S(1)}) custom-call(s32[1]{0:T(128)} %bitcast.index, bf16[16,2048]{1,0:T(8,128)(2,1)S(1)} %get-tuple-element.36.normed, bf16[2048,512]{1,0:T(8,128)(2,1)} %w_latent.1, bf16[32,2048]{1,0:T(8,128)(2,1)} %bitcast.18, bf16[512]{0:T(512)(128)(2,1)} %gain.7, ...), custom_call_target="tpu_custom_call" | custom-call | tf_op jit(solution)/shard_map/pallas_call | solution.py:54
  23.9 0.0 copy-start
  24.0 0.0 copy-start.2
  24.0 0.0 copy-start.5
  24.0 3.4 %all-to-all-done.queries = f32[16,8,128]{2,1,0:T(8,128)S(1)} async-done(((f32[16,8,128]{2,1,0:T(8,128)}), f32[16,8,128]{2,1,0:T(8,128)S(1)}, u32[]{:S(2)}, u32[]{:S(2)}) %all-to-all-start) | async-done | bytes 65568 | tf_op jit(solution)/shard_map/all_to_all | solution.py:21
  27.4 0.0 copy-done.6
  27.4 0.0 copy-done.7
  27.4 0.0 copy-start.8
  27.4 0.0 copy-start.9
  27.4 0.0 copy-start.10
  27.4 1.8 %shard_map.246 = f32[16,8,128]{2,1,0:T(8,128)} custom-call(s32[1]{0:T(128)S(6)} %copy.27.lengths, f32[16,8,128]{2,1,0:T(8,128)S(1)} %all-to-all-done.queries, bf16[1632,512]{1,0:T(8,128)(2,1)S(1)} %get-tuple-element.39.caches, f32[1,640]{1,0:T(1,128)S(1)} %get-tuple-element.40.token, f32[1,16]{1,0:T(1,128)S(1)} %copy-done.7, f32[1,16]{1,0:T(1,128)S(1)} %copy-done.6), custom_call_target="tpu_custom_call" | custom-call | tf_op jit(solution)/shard_map/pallas_call | solution.py:54
  29.3 1.3 %shard_map.247 = (bf16[80,1536]{1,0:T(8,128)(2,1)S(1)}, bf16[48,128]{1,0:T(8,128)(2,1)S(1)}) custom-call(s32[1]{0:T(128)} %bitcast.index, s32[4,16]{1,0:T(4,128)} %bitcast.12, f32[4,16]{1,0:T(4,128)} %bitcast.19, bf16[64,512]{1,0:T(8,128)(2,1)} %bitcast.10, bf16[64]{0:T(256)(128)(2,1)} %gain.9, bf16[64,2048]{1,0:T(8,128)(2,1)} %w_output.3), custom_call_target="tpu_custom_call" | custom-call | tf_op jit(solution)/shard_map/pallas_call | solution.py:54
  30.6 2.1 %collective-permute-start = (bf16[80,1536]{1,0:T(8,128)(2,1)S(1)}, bf16[80,1536]{1,0:T(8,128)(2,1)S(1)}, u32[]{:S(2)}, u32[]{:S(2)}) collective-permute-start(bf16[80,1536]{1,0:T(8,128)(2,1)S(1)} %get-tuple-element.43), channel_id=1, source_target_pairs={{0,1},{1,0},{2,3},{3,2},{4,5},{5,4},{6,7},{7,6},{8,9},{9,8},{10,11... | collective-permute-start | bytes 737288 | tf_op jit(solution)/shard_map/ppermute | solution.py:27
  32.7 11.7 %all_to_all.30.attended = f32[16,8,128]{2,1,0:T(8,128)S(1)} all-to-all(f32[16,8,128]{2,1,0:T(8,128)} %shard_map.246), channel_id=1, replica_groups=mesh['ep'=64,'tp'=16] {'tp'}, dimensions={0} | all-to-all | bytes 131072 | tf_op jit(solution)/shard_map/all_to_all | solution.py:21
  44.4 0.0 collective-permute-done.pack
  44.4 0.0 copy-done
  44.4 0.0 copy-done.2
  44.4 0.0 copy-done.5
  44.4 0.4 shard_map.248
  44.8 14.8 %all_to_all.31.shares = bf16[8,128,128]{2,1,0:T(8,128)(2,1)S(1)} all-to-all(bf16[8,128,128]{2,1,0:T(8,128)(2,1)S(1)} %shard_map.248), channel_id=1, replica_groups={{0,2,4,6,8,10,12,14},{1,3,5,7,9,11,13,15},{16,18,20,22,24,26,28,30},{17..., dimensions={0} | all-to-all | bytes 524288 | tf_op jit(solution)/shard_map/all_to_all | solution.py:21
  59.6 0.0 copy-done.1
  59.6 0.0 copy-done.4
  59.6 1.1 shard_map.249
  60.7 0.0 copy-done.8
  60.7 2.3 %collective-permute-start.1 = (bf16[1,2048,128]{2,1,0:T(8,128)(2,1)S(1)}, bf16[1,2048,128]{2,1,0:T(8,128)(2,1)S(1)}, u32[]{:S(2)}, u32[]{:S(2)}) collective-permute-start(bf16[1,2048,128]{2,1,0:T(8,128)(2,1)S(1)} %copy-done.8), channel_id=1, source_target_pairs={{0,1},{1,0},{2,3},{3,2},{4,5},{5,4},{6,7},{7,6},{8,9},{9,8},{10,11... | collective-permute-start | bytes 1572872 | tf_op jit(solution)/shard_map/ppermute | solution.py:27
  63.0 2.0 %collective-permute-start.2 = (bf16[1,2048,128]{2,1,0:T(8,128)(2,1)S(1)}, bf16[1,2048,128]{2,1,0:T(8,128)(2,1)S(1)}, u32[]{:S(2)}, u32[]{:S(2)}) collective-permute-start(bf16[1,2048,128]{2,1,0:T(8,128)(2,1)S(1)} %copy-done.9), channel_id=1, source_target_pairs={{0,1},{1,0},{2,3},{3,2},{4,5},{5,4},{6,7},{7,6},{8,9},{9,8},{10,11... | collective-permute-start | bytes 1572872 | tf_op jit(solution)/shard_map/ppermute | solution.py:27
  65.0 2.4 %collective-permute-start.3 = (bf16[1,128,2048]{2,1,0:T(8,128)(2,1)S(1)}, bf16[1,128,2048]{2,1,0:T(8,128)(2,1)S(1)}, u32[]{:S(2)}, u32[]{:S(2)}) collective-permute-start(bf16[1,128,2048]{2,1,0:T(8,128)(2,1)S(1)} %copy-done.10), channel_id=1, source_target_pairs={{0,1},{1,0},{2,3},{3,2},{4,5},{5,4},{6,7},{7,6},{8,9},{9,8},{10,11... | collective-permute-start | bytes 1572872 | tf_op jit(solution)/shard_map/ppermute | solution.py:27
  67.4 27.5 %all_to_all.32.arrived = bf16[64,16,128]{2,1,0:T(8,128)(2,1)S(1)} all-to-all(bf16[64,16,128]{2,1,0:T(8,128)(2,1)} %get-tuple-element.49), channel_id=1, replica_groups=mesh['ep'=64,'tp'=16] {'ep'}, dimensions={0} | all-to-all | bytes 524288 | tf_op jit(solution)/shard_map/all_to_all | solution.py:21
  94.9 0.0 collective-permute-done.1.refs_3_
  94.9 0.0 collective-permute-done.2.refs_4_
  94.9 0.0 collective-permute-done.3.refs_5_
  94.9 0.0 copy-start.13
  94.9 4.2 %collective-permute-start.4 = (bf16[64,16,128]{2,1,0:T(8,128)(2,1)S(1)}, bf16[64,16,128]{2,1,0:T(8,128)(2,1)S(1)}, u32[]{:S(2)}, u32[]{:S(2)}) collective-permute-start(bf16[64,16,128]{2,1,0:T(8,128)(2,1)S(1)} %all_to_all.32.arrived), channel_id=1, source_target_pairs={{0,1},{1,0},{2,3},{3,2},{4,5},{5,4},{6,7},{7,6},{8,9},{9,8},{10,11... | collective-permute-start | bytes 786440 | tf_op jit(solution)/shard_map/ppermute | solution.py:27
  99.2 1.1 collective-permute-done.4.other
  100.3 3.5 %shard_map.250 = bf16[64,16,128]{2,1,0:T(8,128)(2,1)} custom-call(s32[1]{0:T(128)} %bitcast.index, bf16[64,16,128]{2,1,0:T(8,128)(2,1)S(1)} %all_to_all.32.arrived, bf16[64,16,128]{2,1,0:T(8,128)(2,1)S(1)} %collective-permute-done.4.other, bf16[2048]{0:T(1024)(128)(2,1)S(1)} %copy-done.3, bf16[1,2048,128]{2,1,0:T(8,128)(2,1)} %refs_0_.1, ...), custom_call_target="tpu_custom_call" | custom-call | tf_op jit(solution)/shard_map/pallas_call | solution.py:54
  103.8 4.6 %all-to-all-start.4 = ((bf16[64,16,128]{2,1,0:T(8,128)(2,1)}), bf16[64,16,128]{2,1,0:T(8,128)(2,1)S(1)}, u32[]{:S(2)}, u32[]{:S(2)}) async-start(bf16[64,16,128]{2,1,0:T(8,128)(2,1)} %shard_map.250), calls=%async_computation.4 | async-start | bytes 524288 | tf_op jit(solution)/shard_map/all_to_all | solution.py:21
  108.4 2.3 %collective-permute-start.5 = (bf16[128,128]{1,0:T(8,128)(2,1)S(1)}, bf16[128,128]{1,0:T(8,128)(2,1)S(1)}, u32[]{:S(2)}, u32[]{:S(2)}) collective-permute-start(bf16[128,128]{1,0:T(8,128)(2,1)S(1)} %get-tuple-element.59.middle), channel_id=1, source_target_pairs={{0,1},{1,0},{2,3},{3,2},{4,5},{5,4},{6,7},{7,6},{8,9},{9,8},{10,11... | collective-permute-start | bytes 98312 | tf_op jit(solution)/shard_map/ppermute | solution.py:27
  110.7 0.8 collective-permute-done.5.other
  111.5 2.7 %shard_map.251 = (f32[128,128]{1,0:T(8,128)S(1)}, f32[128,128]{1,0:T(8,128)}) custom-call(s32[1]{0:T(128)} %bitcast.index, bf16[128,128]{1,0:T(8,128)(2,1)S(1)} %get-tuple-element.59.middle, bf16[128,128]{1,0:T(8,128)(2,1)S(1)} %collective-permute-done.5.other, bf16[2048]{0:T(1024)(128)(2,1)} %gain.11, bf16[64,2048]{1,0:T(8,128)(2,1)} %bitcast.15, ...), custom_call_target="tpu_custom_call" | custom-call | tf_op jit(solution)/shard_map/pallas_call | solution.py:54
  114.3 2.2 %collective-permute-start.6 = (f32[128,128]{1,0:T(8,128)}, f32[128,128]{1,0:T(8,128)S(1)}, u32[]{:S(2)}, u32[]{:S(2)}) collective-permute-start(f32[128,128]{1,0:T(8,128)} %get-tuple-element.61), channel_id=1, source_target_pairs={{0,1},{1,0},{2,3},{3,2},{4,5},{5,4},{6,7},{7,6},{8,9},{9,8},{10,11... | collective-permute-start | bytes 196616 | tf_op jit(solution)/shard_map/ppermute | solution.py:27
  116.5 1.1 collective-permute-done.6
  117.6 4.2 %all-to-all-done.4.returned = bf16[64,16,128]{2,1,0:T(8,128)(2,1)S(1)} async-done(((bf16[64,16,128]{2,1,0:T(8,128)(2,1)}), bf16[64,16,128]{2,1,0:T(8,128)(2,1)S(1)}, u32[]{:S(2)}, u32[]{:S(2)}) %all-to-all-start.4) | async-done | bytes 262176 | tf_op jit(solution)/shard_map/all_to_all | solution.py:21
  121.8 0.2 shard_map.252
  122.1 9.3 %all_to_all.33.tiles = bf16[8,16,128]{2,1,0:T(8,128)(2,1)S(1)} all-to-all(bf16[8,16,128]{2,1,0:T(8,128)(2,1)S(1)} %shard_map.252), channel_id=1, replica_groups={{0,2,4,6,8,10,12,14},{1,3,5,7,9,11,13,15},{16,18,20,22,24,26,28,30},{17..., dimensions={0} | all-to-all | bytes 65536 | tf_op jit(solution)/shard_map/all_to_all | solution.py:21
  131.4 0.6 shard_map.253
  (14 shorter events, 0.0 us)
Async XLA Ops:
  2.2 25.2 %all-to-all-start = ((f32[16,8,128]{2,1,0:T(8,128)}), f32[16,8,128]{2,1,0:T(8,128)S(1)}, u32[]{:S(2)}, u32[]{:S(2)}) async-start(f32[16,8,128]{2,1,0:T(8,128)} %get-tuple-element.35), calls=%async_computation | async-start | bytes 131072 | tf_op jit(solution)/shard_map/all_to_all | solution.py:21
  20.8 6.6 %copy-start.6 = (f32[1,16]{1,0:T(1,128)S(1)}, f32[1,16]{1,0:T(1,128)}, u32[]{:S(2)}) copy-start(f32[1,16]{1,0:T(1,128)} %get-tuple-element.65.sin) | copy-start | bytes 196
  20.8 6.6 %copy-start.7 = (f32[1,16]{1,0:T(1,128)S(1)}, f32[1,16]{1,0:T(1,128)}, u32[]{:S(2)}) copy-start(f32[1,16]{1,0:T(1,128)} %get-tuple-element.66.cos) | copy-start | bytes 196
  23.9 20.4 %copy-start = (bf16[64,2048]{1,0:T(8,128)(2,1)S(1)}, bf16[64,2048]{1,0:T(8,128)(2,1)}, u32[]{:S(2)}) copy-start(bf16[64,2048]{1,0:T(8,128)(2,1)} %w_output.3) | copy-start | bytes 786436
  24.0 20.4 %copy-start.2 = (bf16[512,64]{0,1:T(8,128)(2,1)S(1)}, bf16[512,64]{0,1:T(8,128)(2,1)}, u32[]{:S(2)}) copy-start(bf16[512,64]{0,1:T(8,128)(2,1)} %param.37) | copy-start | bytes 196612
  24.0 20.4 %copy-start.5 = (bf16[64]{0:T(256)(128)(2,1)S(1)}, bf16[64]{0:T(256)(128)(2,1)}, u32[]{:S(2)}) copy-start(bf16[64]{0:T(256)(128)(2,1)} %gain.9) | copy-start | bytes 388
  27.4 32.2 %copy-start.1 = (bf16[16,2048]{1,0:T(8,128)(2,1)S(1)}, bf16[16,2048]{1,0:T(8,128)(2,1)}, u32[]{:S(2)}) copy-start(bf16[16,2048]{1,0:T(8,128)(2,1)} %hidden.3) | copy-start | bytes 196612
  27.4 32.2 %copy-start.4 = (s32[16,4]{0,1:T(4,128)S(1)}, s32[16,4]{0,1:T(4,128)}, u32[]{:S(2)}) copy-start(s32[16,4]{0,1:T(4,128)} %param.41) | copy-start | bytes 772
  27.4 33.3 %copy-start.8 = (bf16[1,2048,128]{2,1,0:T(8,128)(2,1)S(1)}, bf16[1,2048,128]{2,1,0:T(8,128)(2,1)}, u32[]{:S(2)}) copy-start(bf16[1,2048,128]{2,1,0:T(8,128)(2,1)} %refs_0_.1) | copy-start | bytes 1572868
  27.4 35.6 %copy-start.9 = (bf16[1,2048,128]{2,1,0:T(8,128)(2,1)S(1)}, bf16[1,2048,128]{2,1,0:T(8,128)(2,1)}, u32[]{:S(2)}) copy-start(bf16[1,2048,128]{2,1,0:T(8,128)(2,1)} %refs_1_.1) | copy-start | bytes 1572868
  27.4 37.6 %copy-start.10 = (bf16[1,128,2048]{2,1,0:T(8,128)(2,1)S(1)}, bf16[1,128,2048]{2,1,0:T(8,128)(2,1)}, u32[]{:S(2)}) copy-start(bf16[1,128,2048]{2,1,0:T(8,128)(2,1)} %refs_2_.1) | copy-start | bytes 1572868
  29.3 71.0 %copy-start.3 = (bf16[2048]{0:T(1024)(128)(2,1)S(1)}, bf16[2048]{0:T(1024)(128)(2,1)}, u32[]{:S(2)}) copy-start(bf16[2048]{0:T(1024)(128)(2,1)} %gain.11) | copy-start | bytes 12292
  30.6 13.8 %collective-permute-start = (bf16[80,1536]{1,0:T(8,128)(2,1)S(1)}, bf16[80,1536]{1,0:T(8,128)(2,1)S(1)}, u32[]{:S(2)}, u32[]{:S(2)}) collective-permute-start(bf16[80,1536]{1,0:T(8,128)(2,1)S(1)} %get-tuple-element.43), channel_id=1, source_target_pairs={{0,1},{1,0},{2,3},{3,2},{4,5},{5,4},{6,7},{7,6},{8,9},{9,8},{10,11... | collective-permute-start | bytes 737288 | tf_op jit(solution)/shard_map/ppermute | solution.py:27
  60.7 34.2 %collective-permute-start.1 = (bf16[1,2048,128]{2,1,0:T(8,128)(2,1)S(1)}, bf16[1,2048,128]{2,1,0:T(8,128)(2,1)S(1)}, u32[]{:S(2)}, u32[]{:S(2)}) collective-permute-start(bf16[1,2048,128]{2,1,0:T(8,128)(2,1)S(1)} %copy-done.8), channel_id=1, source_target_pairs={{0,1},{1,0},{2,3},{3,2},{4,5},{5,4},{6,7},{7,6},{8,9},{9,8},{10,11... | collective-permute-start | bytes 1572872 | tf_op jit(solution)/shard_map/ppermute | solution.py:27
  63.0 31.8 %collective-permute-start.2 = (bf16[1,2048,128]{2,1,0:T(8,128)(2,1)S(1)}, bf16[1,2048,128]{2,1,0:T(8,128)(2,1)S(1)}, u32[]{:S(2)}, u32[]{:S(2)}) collective-permute-start(bf16[1,2048,128]{2,1,0:T(8,128)(2,1)S(1)} %copy-done.9), channel_id=1, source_target_pairs={{0,1},{1,0},{2,3},{3,2},{4,5},{5,4},{6,7},{7,6},{8,9},{9,8},{10,11... | collective-permute-start | bytes 1572872 | tf_op jit(solution)/shard_map/ppermute | solution.py:27
  65.0 29.9 %collective-permute-start.3 = (bf16[1,128,2048]{2,1,0:T(8,128)(2,1)S(1)}, bf16[1,128,2048]{2,1,0:T(8,128)(2,1)S(1)}, u32[]{:S(2)}, u32[]{:S(2)}) collective-permute-start(bf16[1,128,2048]{2,1,0:T(8,128)(2,1)S(1)} %copy-done.10), channel_id=1, source_target_pairs={{0,1},{1,0},{2,3},{3,2},{4,5},{5,4},{6,7},{7,6},{8,9},{9,8},{10,11... | collective-permute-start | bytes 1572872 | tf_op jit(solution)/shard_map/ppermute | solution.py:27
  94.9 5.4 %copy-start.11 = (bf16[1,2048,128]{2,1,0:T(8,128)(2,1)}, bf16[1,2048,128]{2,1,0:T(8,128)(2,1)S(1)}, u32[]{:S(2)}) copy-start(bf16[1,2048,128]{2,1,0:T(8,128)(2,1)S(1)} %collective-permute-done.1.refs_3_) | copy-start | bytes 1572868
  94.9 5.4 %copy-start.12 = (bf16[1,2048,128]{2,1,0:T(8,128)(2,1)}, bf16[1,2048,128]{2,1,0:T(8,128)(2,1)S(1)}, u32[]{:S(2)}) copy-start(bf16[1,2048,128]{2,1,0:T(8,128)(2,1)S(1)} %collective-permute-done.2.refs_4_) | copy-start | bytes 1572868
  94.9 5.4 %copy-start.13 = (bf16[1,128,2048]{2,1,0:T(8,128)(2,1)}, bf16[1,128,2048]{2,1,0:T(8,128)(2,1)S(1)}, u32[]{:S(2)}) copy-start(bf16[1,128,2048]{2,1,0:T(8,128)(2,1)S(1)} %collective-permute-done.3.refs_5_) | copy-start | bytes 1572868
  94.9 5.4 %collective-permute-start.4 = (bf16[64,16,128]{2,1,0:T(8,128)(2,1)S(1)}, bf16[64,16,128]{2,1,0:T(8,128)(2,1)S(1)}, u32[]{:S(2)}, u32[]{:S(2)}) collective-permute-start(bf16[64,16,128]{2,1,0:T(8,128)(2,1)S(1)} %all_to_all.32.arrived), channel_id=1, source_target_pairs={{0,1},{1,0},{2,3},{3,2},{4,5},{5,4},{6,7},{7,6},{8,9},{9,8},{10,11... | collective-permute-start | bytes 786440 | tf_op jit(solution)/shard_map/ppermute | solution.py:27
  103.8 18.1 %all-to-all-start.4 = ((bf16[64,16,128]{2,1,0:T(8,128)(2,1)}), bf16[64,16,128]{2,1,0:T(8,128)(2,1)S(1)}, u32[]{:S(2)}, u32[]{:S(2)}) async-start(bf16[64,16,128]{2,1,0:T(8,128)(2,1)} %shard_map.250), calls=%async_computation.4 | async-start | bytes 524288 | tf_op jit(solution)/shard_map/all_to_all | solution.py:21
  108.4 3.1 %collective-permute-start.5 = (bf16[128,128]{1,0:T(8,128)(2,1)S(1)}, bf16[128,128]{1,0:T(8,128)(2,1)S(1)}, u32[]{:S(2)}, u32[]{:S(2)}) collective-permute-start(bf16[128,128]{1,0:T(8,128)(2,1)S(1)} %get-tuple-element.59.middle), channel_id=1, source_target_pairs={{0,1},{1,0},{2,3},{3,2},{4,5},{5,4},{6,7},{7,6},{8,9},{9,8},{10,11... | collective-permute-start | bytes 98312 | tf_op jit(solution)/shard_map/ppermute | solution.py:27
  114.3 3.3 %collective-permute-start.6 = (f32[128,128]{1,0:T(8,128)}, f32[128,128]{1,0:T(8,128)S(1)}, u32[]{:S(2)}, u32[]{:S(2)}) collective-permute-start(f32[128,128]{1,0:T(8,128)} %get-tuple-element.61), channel_id=1, source_target_pairs={{0,1},{1,0},{2,3},{3,2},{4,5},{5,4},{6,7},{7,6},{8,9},{9,8},{10,11... | collective-permute-start | bytes 196616 | tf_op jit(solution)/shard_map/ppermute | solution.py:27

commit v6 on v4

--- a/solution.py
+++ b/solution.py
@@ -273,17 +273,30 @@
         other_out[at, :] = jnp.where(core == 0, high, low)
 
 
-def expert_body(
-    index, arrived, other, gain, *refs,
-):
-    weights, (out, wide, wide_other, rows_in, gains, *held, sems) = refs[:6], refs[6:]
-    copies = [
-        pltpu.make_async_copy(weight.at[0], place, sems.at[k])
-        for k, (weight, place) in enumerate(zip(weights, held))
+def pack_body(index, w_gate, w_up, w_down, packed, down, sems):
+    core = index[0] % 2
+    depth, width = w_gate.shape[1:]
+    pairs = [
+        (w.at[0], packed.at[pl.ds(0, depth), pl.ds(k * width, width)])
+        for k, w in enumerate((w_gate, w_up))
     ]
+    for place, base, parity in ((packed, depth, 1 - core), (down, 0, core)):
+        for m in range(8):
+            block = pl.ds(base + m // 2 * width, width), pl.ds(m % 2 * LANES, LANES)
+            pairs.append((w_down.at[0, :, tile_at(2 * m + parity)], place.at[block]))
+    copies = [pltpu.make_async_copy(*pair, sems.at[k]) for k, pair in enumerate(pairs)]
     for copy in copies:
         copy.start()
+    for copy in copies:
+        copy.wait()
+
+
+def expert_body(
+    index, arrived, other, gain, packed, down, away, out, wide, wide_other, rows_in, gains
+):
     core = index[0] % 2
+    depth = packed.shape[0] - down.shape[0]
+    width = down.shape[0] // 4
     peers, rows, _ = arrived.shape
     slots = peers * rows // 8
     gains[...] = row(gain)
@@ -305,17 +318,16 @@
             rows_in[:, tile_at(number)] = normed.astype(BF16)
     x = rows_in[...]
     acts = []
-    for gate, up in ((0, 1), (3, 4)):
-        copies[gate].wait()
-        pre = dot32(x, held[gate][...])
-        copies[up].wait()
-        acts.append((pre / (1.0 + jnp.exp(-pre)) * dot32(x, held[up][...])).astype(BF16))
-    copies[2].wait()
-    copies[5].wait()
-    for m in range(8):
-        at = tile_at(2 * m + core)
-        part = dot32(acts[0], held[2][:, at]) + dot32(acts[1], held[5][:, at])
-        wide[pl.ds(m, slots, stride=8), :] = part
+    for place in (packed, away):
+        both = dot32(x, place[:depth, :])
+        pre = both[:, :width]
+        acts.append((pre / (1.0 + jnp.exp(-pre)) * both[:, width:]).astype(BF16))
+    for q in range(4):
+        at = slice(q * width, (q + 1) * width)
+        part = dot32(acts[0], down[at, :])
+        part = part + dot32(acts[1], away[depth + q * width : depth + (q + 1) * width, :])
+        for k in range(2):
+            wide[pl.ds(2 * q + k, slots, stride=8), :] = part[:, k * LANES : (k + 1) * LANES]
     for p in range(peers):
         out[p] = wide[p * rows : (p + 1) * rows, :].astype(BF16)
 
@@ -449,11 +461,19 @@
         smem=(0,),
         leave=(0,),
     )
-    own_weights = (w_expert_gate, w_expert_up, w_expert_down)
-    payload, *weights = together(payload, *own_weights)
+    payload, later = together(payload, index)
     shares = exchange(payload, "tp", same_core)
-    weights = [core_swap(w) for w in weights]
-    shares, *weights = together(shares, *weights)
+    width = w_expert_gate.shape[2]
+    packed, down = call(
+        pack_body,
+        (shape((MODEL_WIDTH + 4 * width, 2 * width), BF16), shape((4 * width, 2 * width), BF16)),
+        (later, w_expert_gate, w_expert_up, w_expert_down),
+        smem=(0,),
+        raw=(1, 2, 3),
+        scratch=(pltpu.SemaphoreType.DMA((2 + 2 * chips,)),),
+    )
+    away = core_swap(packed)
+    shares, packed, down, away = together(shares, packed, down, away)
 
     middle, payload = call(
         middle_body,
@@ -475,19 +495,17 @@
             arrived,
             core_swap(arrived),
             ffn_gain,
-            *own_weights,
-            *weights,
+            packed,
+            down,
+            away,
         ),
         smem=(0,),
-        raw=range(4, 10),
         leave=(0,),
         scratch=(
             wide,
             wide,
             pltpu.VMEM((slots, MODEL_WIDTH), BF16),
             pltpu.VMEM((1, MODEL_WIDTH), F32),
-            *(pltpu.VMEM(w.shape[1:], BF16) for w in own_weights * 2),
-            pltpu.SemaphoreType.DMA((6,)),
         ),
     )
     payload, later, other = together(payload, later, other)

time: 136 us -> 130 us (0.956)
  starting transfers between devices: 54.2 us -> 50 us
    ppermute x7 -> x5, starting transfers between devices: 18.3 us -> 14 us  [core_swap(): lax.ppermute(x, 'tp', [(i, i ^ 1) for i in range(lax.axis_size('tp'))])]
    pallas_call x10 -> x11, Pallas kernels: 17.9 us -> 17.6 us  [call(): pl.pallas_call(body, out_shape=outs, in_specs=[kinds.get(i, vmem) for i i...]
    ppermute x7 -> x5, waiting for transfers between devices: 3.08 us -> 3.07 us  [core_swap(): lax.ppermute(x, 'tp', [(i, i ^ 1) for i in range(lax.axis_size('tp'))])]
  transfers between devices with their start and end apart: 10 -> 8, of which waited for: 6 -> 6; matrix products, arithmetic and copies ran while one was open for 0% -> 1% of each run, Pallas kernels for 4% -> 5%
where the time goes in v6:
time: 130 us; the launch traced here: 128 us
  starting transfers between devices  50 us (38%)
  blocking collectives  35.6 us (27%)
  waiting for transfers between devices  23.2 us (18%)
  Pallas kernels  17.6 us (14%)
    all_to_all x3, starting transfers between devices, exchange(): lax.all_to_all(x, axis, split_axis=0, concat_axis=0, axis_index_groups=gr...  36 us
    all_to_all x3, blocking collectives, exchange(): lax.all_to_all(x, axis, split_axis=0, concat_axis=0, axis_index_groups=gr...  35.6 us
    all_to_all x3, waiting for transfers between devices, exchange(): lax.all_to_all(x, axis, split_axis=0, concat_axis=0, axis_index_groups=gr...  20.1 us
    pallas_call x11, Pallas kernels, call(): pl.pallas_call(body, out_shape=outs, in_specs=[kinds.get(i, vmem) for i i...  17.6 us
    ppermute x5, starting transfers between devices, core_swap(): lax.ppermute(x, 'tp', [(i, i ^ 1) for i in range(lax.axis_size('tp'))])  14 us
    ppermute x5, waiting for transfers between devices, core_swap(): lax.ppermute(x, 'tp', [(i, i ^ 1) for i in range(lax.axis_size('tp'))])  3.07 us
  transfers between devices with their start and end apart: 8, of which 6 were waited for; matrix products, arithmetic and copies ran while one was open for 1% of the time, Pallas kernels for 5%

profile of v6, /device:TPU:1, one launch (start us, length us, event | category | flops | bytes accessed | tf_op | source)
XLA Modules:
  0.0 128.0 jit_solution(17184211730884257205)
XLA Ops:
  0.0 2.2 %shard_map.244 = (f32[16,8,128]{2,1,0:T(8,128)}, bf16[16,2048]{1,0:T(8,128)(2,1)S(1)}) custom-call(bf16[16,2048]{1,0:T(8,128)(2,1)} %hidden.3, bf16[2048]{0:T(1024)(128)(2,1)} %gain.6, bf16[64,2048]{1,0:T(8,128)(2,1)} %bitcast.14, bf16[32,2048]{1,0:T(8,128)(2,1)} %bitcast.17, bf16[64,512]{1,0:T(8,128)(2,1)} %key_up.1), custom_call_target="tpu_custom_call" | custom-call | tf_op jit(solution)/shard_map/pallas_call | solution.py:54
  2.2 17.4 %all-to-all-start = ((f32[16,8,128]{2,1,0:T(8,128)}), f32[16,8,128]{2,1,0:T(8,128)S(1)}, u32[]{:S(2)}, u32[]{:S(2)}) async-start(f32[16,8,128]{2,1,0:T(8,128)} %get-tuple-element.39), calls=%async_computation | async-start | bytes 131072 | tf_op jit(solution)/shard_map/all_to_all | solution.py:21
  20.2 0.7 fusion
  20.9 0.0 copy-start.6
  20.9 0.0 copy-start.7
  20.9 3.1 %shard_map.245 = (f32[1,640]{1,0:T(1,128)S(1)}, bf16[1632,512]{1,0:T(8,128)(2,1)S(1)}) custom-call(s32[1]{0:T(128)} %bitcast.index, bf16[16,2048]{1,0:T(8,128)(2,1)S(1)} %get-tuple-element.40.normed, bf16[2048,512]{1,0:T(8,128)(2,1)} %w_latent.1, bf16[32,2048]{1,0:T(8,128)(2,1)} %bitcast.18, bf16[512]{0:T(512)(128)(2,1)} %gain.7, ...), custom_call_target="tpu_custom_call" | custom-call | tf_op jit(solution)/shard_map/pallas_call | solution.py:54
  24.0 0.0 copy-start
  24.0 0.0 copy-start.2
  24.0 0.0 copy-start.5
  24.0 3.3 %all-to-all-done.queries = f32[16,8,128]{2,1,0:T(8,128)S(1)} async-done(((f32[16,8,128]{2,1,0:T(8,128)}), f32[16,8,128]{2,1,0:T(8,128)S(1)}, u32[]{:S(2)}, u32[]{:S(2)}) %all-to-all-start) | async-done | bytes 65568 | tf_op jit(solution)/shard_map/all_to_all | solution.py:21
  27.4 0.0 copy-done.6
  27.4 0.0 copy-done.7
  27.4 1.8 %shard_map.246 = f32[16,8,128]{2,1,0:T(8,128)} custom-call(s32[1]{0:T(128)S(6)} %copy.27.lengths, f32[16,8,128]{2,1,0:T(8,128)S(1)} %all-to-all-done.queries, bf16[1632,512]{1,0:T(8,128)(2,1)S(1)} %get-tuple-element.43.caches, f32[1,640]{1,0:T(1,128)S(1)} %get-tuple-element.44.token, f32[1,16]{1,0:T(1,128)S(1)} %copy-done.7, f32[1,16]{1,0:T(1,128)S(1)} %copy-done.6), custom_call_target="tpu_custom_call" | custom-call | tf_op jit(solution)/shard_map/pallas_call | solution.py:54
  29.2 1.3 %shard_map.247 = (bf16[80,1536]{1,0:T(8,128)(2,1)S(1)}, bf16[48,128]{1,0:T(8,128)(2,1)S(1)}) custom-call(s32[1]{0:T(128)} %bitcast.index, s32[4,16]{1,0:T(4,128)} %bitcast.12, f32[4,16]{1,0:T(4,128)} %bitcast.19, bf16[64,512]{1,0:T(8,128)(2,1)} %bitcast.10, bf16[64]{0:T(256)(128)(2,1)} %gain.9, bf16[64,2048]{1,0:T(8,128)(2,1)} %w_output.3), custom_call_target="tpu_custom_call" | custom-call | tf_op jit(solution)/shard_map/pallas_call | solution.py:54
  30.6 0.0 copy-start.1
  30.6 0.0 copy-start.4
  30.6 2.2 %collective-permute-start = (bf16[80,1536]{1,0:T(8,128)(2,1)S(1)}, bf16[80,1536]{1,0:T(8,128)(2,1)S(1)}, u32[]{:S(2)}, u32[]{:S(2)}) collective-permute-start(bf16[80,1536]{1,0:T(8,128)(2,1)S(1)} %get-tuple-element.47), channel_id=1, source_target_pairs={{0,1},{1,0},{2,3},{3,2},{4,5},{5,4},{6,7},{7,6},{8,9},{9,8},{10,11... | collective-permute-start | bytes 737288 | tf_op jit(solution)/shard_map/ppermute | solution.py:27
  32.8 11.7 %all_to_all.30.attended = f32[16,8,128]{2,1,0:T(8,128)S(1)} all-to-all(f32[16,8,128]{2,1,0:T(8,128)} %shard_map.246), channel_id=1, replica_groups=mesh['ep'=64,'tp'=16] {'tp'}, dimensions={0} | all-to-all | bytes 131072 | tf_op jit(solution)/shard_map/all_to_all | solution.py:21
  44.5 0.0 collective-permute-done.pack
  44.5 0.0 copy-done
  44.5 0.0 copy-done.2
  44.5 0.0 copy-done.5
  44.5 1.1 shard_map.248
  45.6 0.0 copy-start.8
  45.6 1.5 %shard_map.249 = (bf16[2560,256]{1,0:T(8,128)(2,1)S(1)}, bf16[512,256]{1,0:T(8,128)(2,1)S(1)}) custom-call(s32[1]{0:T(128)} %bitcast.index, bf16[1,2048,128]{2,1,0:T(8,128)(2,1)} %w_gate.1, bf16[1,2048,128]{2,1,0:T(8,128)(2,1)} %w_up.1, bf16[1,128,2048]{2,1,0:T(8,128)(2,1)} %w_down.1), custom_call_target="tpu_custom_call" | custom-call | tf_op jit(solution)/shard_map/pallas_call | solution.py:54
  47.2 2.0 %collective-permute-start.1 = (bf16[2560,256]{1,0:T(8,128)(2,1)S(1)}, bf16[2560,256]{1,0:T(8,128)(2,1)S(1)}, u32[]{:S(2)}, u32[]{:S(2)}) collective-permute-start(bf16[2560,256]{1,0:T(8,128)(2,1)S(1)} %get-tuple-element.61.packed), channel_id=1, source_target_pairs={{0,1},{1,0},{2,3},{3,2},{4,5},{5,4},{6,7},{7,6},{8,9},{9,8},{10,11... | collective-permute-start | bytes 3932168 | tf_op jit(solution)/shard_map/ppermute | solution.py:27
  49.2 0.0 copy-done.8
  49.2 14.7 %all_to_all.31.shares = bf16[8,128,128]{2,1,0:T(8,128)(2,1)S(1)} all-to-all(bf16[8,128,128]{2,1,0:T(8,128)(2,1)S(1)} %copy-done.8), channel_id=1, replica_groups={{0,2,4,6,8,10,12,14},{1,3,5,7,9,11,13,15},{16,18,20,22,24,26,28,30},{17..., dimensions={0} | all-to-all | bytes 524288 | tf_op jit(solution)/shard_map/all_to_all | solution.py:21
  63.9 0.0 collective-permute-done.1.away
  63.9 0.0 copy-done.1
  63.9 0.0 copy-done.4
  63.9 1.1 shard_map.250
  65.0 13.9 %all-to-all-start.3 = ((bf16[64,16,128]{2,1,0:T(8,128)(2,1)}), bf16[64,16,128]{2,1,0:T(8,128)(2,1)S(1)}, u32[]{:S(2)}, u32[]{:S(2)}) async-start(bf16[64,16,128]{2,1,0:T(8,128)(2,1)} %get-tuple-element.58), calls=%async_computation.3 | async-start | bytes 524288 | tf_op jit(solution)/shard_map/all_to_all | solution.py:21
  79.0 2.7 %collective-permute-start.2 = (bf16[128,128]{1,0:T(8,128)(2,1)S(1)}, bf16[128,128]{1,0:T(8,128)(2,1)S(1)}, u32[]{:S(2)}, u32[]{:S(2)}) collective-permute-start(bf16[128,128]{1,0:T(8,128)(2,1)S(1)} %get-tuple-element.66.middle), channel_id=1, source_target_pairs={{0,1},{1,0},{2,3},{3,2},{4,5},{5,4},{6,7},{7,6},{8,9},{9,8},{10,11... | collective-permute-start | bytes 98312 | tf_op jit(solution)/shard_map/ppermute | solution.py:27
  81.7 0.8 collective-permute-done.2.other
  82.5 9.4 %all-to-all-done.3.arrived = bf16[64,16,128]{2,1,0:T(8,128)(2,1)S(1)} async-done(((bf16[64,16,128]{2,1,0:T(8,128)(2,1)}), bf16[64,16,128]{2,1,0:T(8,128)(2,1)S(1)}, u32[]{:S(2)}, u32[]{:S(2)}) %all-to-all-start.3) | async-done | bytes 262176 | tf_op jit(solution)/shard_map/all_to_all | solution.py:21
  91.9 4.8 %collective-permute-start.3 = (bf16[64,16,128]{2,1,0:T(8,128)(2,1)S(1)}, bf16[64,16,128]{2,1,0:T(8,128)(2,1)S(1)}, u32[]{:S(2)}, u32[]{:S(2)}) collective-permute-start(bf16[64,16,128]{2,1,0:T(8,128)(2,1)S(1)} %all-to-all-done.3.arrived), channel_id=1, source_target_pairs={{0,1},{1,0},{2,3},{3,2},{4,5},{5,4},{6,7},{7,6},{8,9},{9,8},{10,11... | collective-permute-start | bytes 786440 | tf_op jit(solution)/shard_map/ppermute | solution.py:27
  96.8 1.1 collective-permute-done.3.other
  97.9 0.0 copy-done.3
  97.9 1.9 %shard_map.251 = bf16[64,16,128]{2,1,0:T(8,128)(2,1)} custom-call(s32[1]{0:T(128)} %bitcast.index, bf16[64,16,128]{2,1,0:T(8,128)(2,1)S(1)} %all-to-all-done.3.arrived, bf16[64,16,128]{2,1,0:T(8,128)(2,1)S(1)} %collective-permute-done.3.other, bf16[2048]{0:T(1024)(128)(2,1)S(1)} %copy-done.3, bf16[2560,256]{1,0:T(8,128)(2,1)S(1)} %get-tuple-element.61.packed, ...), custom_call_target="tpu_custom_call" | custom-call | tf_op jit(solution)/shard_map/pallas_call | solution.py:54
  99.8 4.6 %all-to-all-start.4 = ((bf16[64,16,128]{2,1,0:T(8,128)(2,1)}), bf16[64,16,128]{2,1,0:T(8,128)(2,1)S(1)}, u32[]{:S(2)}, u32[]{:S(2)}) async-start(bf16[64,16,128]{2,1,0:T(8,128)(2,1)} %shard_map.251), calls=%async_computation.4 | async-start | bytes 524288 | tf_op jit(solution)/shard_map/all_to_all | solution.py:21
  104.4 2.7 %shard_map.252 = (f32[128,128]{1,0:T(8,128)S(1)}, f32[128,128]{1,0:T(8,128)}) custom-call(s32[1]{0:T(128)} %bitcast.index, bf16[128,128]{1,0:T(8,128)(2,1)S(1)} %get-tuple-element.66.middle, bf16[128,128]{1,0:T(8,128)(2,1)S(1)} %collective-permute-done.2.other, bf16[2048]{0:T(1024)(128)(2,1)} %gain.11, bf16[64,2048]{1,0:T(8,128)(2,1)} %bitcast.15, ...), custom_call_target="tpu_custom_call" | custom-call | tf_op jit(solution)/shard_map/pallas_call | solution.py:54
  107.1 2.3 %collective-permute-start.4 = (f32[128,128]{1,0:T(8,128)}, f32[128,128]{1,0:T(8,128)S(1)}, u32[]{:S(2)}, u32[]{:S(2)}) collective-permute-start(f32[128,128]{1,0:T(8,128)} %get-tuple-element.69), channel_id=1, source_target_pairs={{0,1},{1,0},{2,3},{3,2},{4,5},{5,4},{6,7},{7,6},{8,9},{9,8},{10,11... | collective-permute-start | bytes 196616 | tf_op jit(solution)/shard_map/ppermute | solution.py:27
  109.4 1.1 collective-permute-done.4
  110.5 7.4 %all-to-all-done.4.returned = bf16[64,16,128]{2,1,0:T(8,128)(2,1)S(1)} async-done(((bf16[64,16,128]{2,1,0:T(8,128)(2,1)}), bf16[64,16,128]{2,1,0:T(8,128)(2,1)S(1)}, u32[]{:S(2)}, u32[]{:S(2)}) %all-to-all-start.4) | async-done | bytes 262176 | tf_op jit(solution)/shard_map/all_to_all | solution.py:21
  117.9 0.2 shard_map.253
  118.1 9.2 %all_to_all.32.tiles = bf16[8,16,128]{2,1,0:T(8,128)(2,1)S(1)} all-to-all(bf16[8,16,128]{2,1,0:T(8,128)(2,1)S(1)} %shard_map.253), channel_id=1, replica_groups={{0,2,4,6,8,10,12,14},{1,3,5,7,9,11,13,15},{16,18,20,22,24,26,28,30},{17..., dimensions={0} | all-to-all | bytes 65536 | tf_op jit(solution)/shard_map/all_to_all | solution.py:21
  127.4 0.6 shard_map.254
  (2 shorter events, 0.0 us)
Async XLA Ops:
  2.2 25.2 %all-to-all-start = ((f32[16,8,128]{2,1,0:T(8,128)}), f32[16,8,128]{2,1,0:T(8,128)S(1)}, u32[]{:S(2)}, u32[]{:S(2)}) async-start(f32[16,8,128]{2,1,0:T(8,128)} %get-tuple-element.39), calls=%async_computation | async-start | bytes 131072 | tf_op jit(solution)/shard_map/all_to_all | solution.py:21
  20.9 6.5 %copy-start.6 = (f32[1,16]{1,0:T(1,128)S(1)}, f32[1,16]{1,0:T(1,128)}, u32[]{:S(2)}) copy-start(f32[1,16]{1,0:T(1,128)} %get-tuple-element.73.sin) | copy-start | bytes 196
  20.9 6.5 %copy-start.7 = (f32[1,16]{1,0:T(1,128)S(1)}, f32[1,16]{1,0:T(1,128)}, u32[]{:S(2)}) copy-start(f32[1,16]{1,0:T(1,128)} %get-tuple-element.74.cos) | copy-start | bytes 196
  24.0 20.5 %copy-start = (bf16[64,2048]{1,0:T(8,128)(2,1)S(1)}, bf16[64,2048]{1,0:T(8,128)(2,1)}, u32[]{:S(2)}) copy-start(bf16[64,2048]{1,0:T(8,128)(2,1)} %w_output.3) | copy-start | bytes 786436
  24.0 20.5 %copy-start.2 = (bf16[512,64]{0,1:T(8,128)(2,1)S(1)}, bf16[512,64]{0,1:T(8,128)(2,1)}, u32[]{:S(2)}) copy-start(bf16[512,64]{0,1:T(8,128)(2,1)} %param.37) | copy-start | bytes 196612
  24.0 20.5 %copy-start.5 = (bf16[64]{0:T(256)(128)(2,1)S(1)}, bf16[64]{0:T(256)(128)(2,1)}, u32[]{:S(2)}) copy-start(bf16[64]{0:T(256)(128)(2,1)} %gain.9) | copy-start | bytes 388
  30.6 33.4 %copy-start.1 = (bf16[16,2048]{1,0:T(8,128)(2,1)S(1)}, bf16[16,2048]{1,0:T(8,128)(2,1)}, u32[]{:S(2)}) copy-start(bf16[16,2048]{1,0:T(8,128)(2,1)} %hidden.3) | copy-start | bytes 196612
  30.6 33.3 %copy-start.4 = (s32[16,4]{0,1:T(4,128)S(1)}, s32[16,4]{0,1:T(4,128)}, u32[]{:S(2)}) copy-start(s32[16,4]{0,1:T(4,128)} %param.41) | copy-start | bytes 772
  30.6 13.9 %collective-permute-start = (bf16[80,1536]{1,0:T(8,128)(2,1)S(1)}, bf16[80,1536]{1,0:T(8,128)(2,1)S(1)}, u32[]{:S(2)}, u32[]{:S(2)}) collective-permute-start(bf16[80,1536]{1,0:T(8,128)(2,1)S(1)} %get-tuple-element.47), channel_id=1, source_target_pairs={{0,1},{1,0},{2,3},{3,2},{4,5},{5,4},{6,7},{7,6},{8,9},{9,8},{10,11... | collective-permute-start | bytes 737288 | tf_op jit(solution)/shard_map/ppermute | solution.py:27
  45.6 3.6 %copy-start.8 = (bf16[8,128,128]{2,1,0:T(8,128)(2,1)S(1)}, bf16[8,128,128]{2,1,0:T(8,128)(2,1)}, u32[]{:S(2)}) copy-start(bf16[8,128,128]{2,1,0:T(8,128)(2,1)} %shard_map.248) | copy-start | bytes 786436
  45.6 52.2 %copy-start.3 = (bf16[2048]{0:T(1024)(128)(2,1)S(1)}, bf16[2048]{0:T(1024)(128)(2,1)}, u32[]{:S(2)}) copy-start(bf16[2048]{0:T(1024)(128)(2,1)} %gain.11) | copy-start | bytes 12292
  47.2 16.8 %collective-permute-start.1 = (bf16[2560,256]{1,0:T(8,128)(2,1)S(1)}, bf16[2560,256]{1,0:T(8,128)(2,1)S(1)}, u32[]{:S(2)}, u32[]{:S(2)}) collective-permute-start(bf16[2560,256]{1,0:T(8,128)(2,1)S(1)} %get-tuple-element.61.packed), channel_id=1, source_target_pairs={{0,1},{1,0},{2,3},{3,2},{4,5},{5,4},{6,7},{7,6},{8,9},{9,8},{10,11... | collective-permute-start | bytes 3932168 | tf_op jit(solution)/shard_map/ppermute | solution.py:27
  65.0 26.9 %all-to-all-start.3 = ((bf16[64,16,128]{2,1,0:T(8,128)(2,1)}), bf16[64,16,128]{2,1,0:T(8,128)(2,1)S(1)}, u32[]{:S(2)}, u32[]{:S(2)}) async-start(bf16[64,16,128]{2,1,0:T(8,128)(2,1)} %get-tuple-element.58), calls=%async_computation.3 | async-start | bytes 524288 | tf_op jit(solution)/shard_map/all_to_all | solution.py:21
  79.0 3.6 %collective-permute-start.2 = (bf16[128,128]{1,0:T(8,128)(2,1)S(1)}, bf16[128,128]{1,0:T(8,128)(2,1)S(1)}, u32[]{:S(2)}, u32[]{:S(2)}) collective-permute-start(bf16[128,128]{1,0:T(8,128)(2,1)S(1)} %get-tuple-element.66.middle), channel_id=1, source_target_pairs={{0,1},{1,0},{2,3},{3,2},{4,5},{5,4},{6,7},{7,6},{8,9},{9,8},{10,11... | collective-permute-start | bytes 98312 | tf_op jit(solution)/shard_map/ppermute | solution.py:27
  91.9 6.0 %collective-permute-start.3 = (bf16[64,16,128]{2,1,0:T(8,128)(2,1)S(1)}, bf16[64,16,128]{2,1,0:T(8,128)(2,1)S(1)}, u32[]{:S(2)}, u32[]{:S(2)}) collective-permute-start(bf16[64,16,128]{2,1,0:T(8,128)(2,1)S(1)} %all-to-all-done.3.arrived), channel_id=1, source_target_pairs={{0,1},{1,0},{2,3},{3,2},{4,5},{5,4},{6,7},{7,6},{8,9},{9,8},{10,11... | collective-permute-start | bytes 786440 | tf_op jit(solution)/shard_map/ppermute | solution.py:27
  99.8 18.1 %all-to-all-start.4 = ((bf16[64,16,128]{2,1,0:T(8,128)(2,1)}), bf16[64,16,128]{2,1,0:T(8,128)(2,1)S(1)}, u32[]{:S(2)}, u32[]{:S(2)}) async-start(bf16[64,16,128]{2,1,0:T(8,128)(2,1)} %shard_map.251), calls=%async_computation.4 | async-start | bytes 524288 | tf_op jit(solution)/shard_map/all_to_all | solution.py:21
  107.1 3.4 %collective-permute-start.4 = (f32[128,128]{1,0:T(8,128)}, f32[128,128]{1,0:T(8,128)S(1)}, u32[]{:S(2)}, u32[]{:S(2)}) collective-permute-start(f32[128,128]{1,0:T(8,128)} %get-tuple-element.69), channel_id=1, source_target_pairs={{0,1},{1,0},{2,3},{3,2},{4,5},{5,4},{6,7},{7,6},{8,9},{9,8},{10,11... | collective-permute-start | bytes 196616 | tf_op jit(solution)/shard_map/ppermute | solution.py:27

commit v7 on v6

--- a/solution.py
+++ b/solution.py
@@ -73,11 +73,23 @@
     return gain[...].astype(F32).reshape(1, -1)
 
 
-def query_body(hidden, gain, w_nope, w_rope, key_up, out, normed_out):
+def query_body(*refs):
+    sources, (out, normed_out, *held, sems) = refs[:5], refs[5:]
+    copies = [
+        pltpu.make_async_copy(source, place, sems.at[k])
+        for k, (source, place) in enumerate(zip(sources, held))
+    ]
+    for copy in copies:
+        copy.start()
+    hidden, gain, w_nope, w_rope, key_up = held
+    copies[0].wait()
+    copies[1].wait()
     values = hidden[...].astype(F32)
     factor = lax.rsqrt(jnp.mean(values * values, axis=-1, keepdims=True) + EPS)
     normed = (values * factor * row(gain)).astype(BF16)
     normed_out[...] = normed
+    for copy in copies[2:]:
+        copy.wait()
     nope = dot_t(normed, w_nope[...]).astype(BF16)
     rope = dot_t(normed, w_rope[...]).astype(BF16).astype(F32)
     latent = dot32(nope, key_up[...]).astype(BF16).astype(F32)
@@ -396,12 +408,17 @@
     large = shape((ep, slots * chips // ep, LANES), BF16)
     wide = pltpu.VMEM((slots * chips, LANES), F32)
 
+    sources = (hidden, attn_gain, w_query_nope.T, w_query_rope.T, key_up_weight)
     payload, normed = call(
         query_body,
         (small, shape(hidden.shape, BF16)),
-        (hidden, attn_gain, w_query_nope.T, w_query_rope.T, key_up_weight),
-        hbm=range(5),
+        sources,
+        raw=range(5),
         leave=(0,),
+        scratch=(
+            *(pltpu.VMEM(x.shape, BF16) for x in sources),
+            pltpu.SemaphoreType.DMA((len(sources),)),
+        ),
     )
     queries = exchange(payload, "tp")
 
@@ -459,34 +476,30 @@
         shape((chips,) + half, BF16),
         (index, attended, value_up_weight.T, head_gain, w_output, pack),
         smem=(0,),
-        leave=(0,),
-    )
-    payload, later = together(payload, index)
+    )
     shares = exchange(payload, "tp", same_core)
+
+    middle, payload = call(
+        middle_body,
+        (shape(half, BF16), large),
+        (index, shares, hidden, expert_ids.T),
+        smem=(0,),
+        scratch=(wide,),
+        leave=(1,),
+    )
+    payload, later, when = together(payload, middle, index)
+    arrived = exchange(payload, "ep")
     width = w_expert_gate.shape[2]
     packed, down = call(
         pack_body,
         (shape((MODEL_WIDTH + 4 * width, 2 * width), BF16), shape((4 * width, 2 * width), BF16)),
-        (later, w_expert_gate, w_expert_up, w_expert_down),
+        (when, w_expert_gate, w_expert_up, w_expert_down),
         smem=(0,),
         raw=(1, 2, 3),
         scratch=(pltpu.SemaphoreType.DMA((2 + 2 * chips,)),),
     )
     away = core_swap(packed)
-    shares, packed, down, away = together(shares, packed, down, away)
-
-    middle, payload = call(
-        middle_body,
-        (shape(half, BF16), large),
-        (index, shares, hidden, expert_ids.T),
-        smem=(0,),
-        scratch=(wide,),
-        leave=(1,),
-    )
-    payload, later = together(payload, middle)
-    arrived = exchange(payload, "ep")
-    other = core_swap(later)
-    arrived, other = together(arrived, other)
+    arrived, packed, down, away = together(arrived, packed, down, away)
     payload = call(
         expert_body,
         large,
@@ -508,15 +521,16 @@
             pltpu.VMEM((1, MODEL_WIDTH), F32),
         ),
     )
-    payload, later, other = together(payload, later, other)
+    payload, later = together(payload, later)
     returned = exchange(payload, "ep")
+    other_half = core_swap(later)
     side, away = call(
         side_body,
         (shape(half, F32), shape(half, F32)),
         (
             index,
             later,
-            other,
+            other_half,
             ffn_gain,
             w_shared_gate.T,
             w_shared_up.T,

time: 130 us -> 129 us (level)
  blocking collectives: 35.6 us -> 63 us
  starting transfers between devices: 50 us -> 35.2 us
  waiting for transfers between devices: 23.2 us -> 10.7 us
    all_to_all x3 -> x4, blocking collectives: 35.6 us -> 63 us  [exchange(): lax.all_to_all(x, axis, split_axis=0, concat_axis=0, axis_index_groups=gr...]
    all_to_all x3 -> x2, starting transfers between devices: 36 us -> 22 us  [exchange(): lax.all_to_all(x, axis, split_axis=0, concat_axis=0, axis_index_groups=gr...]
    all_to_all x3 -> x2, waiting for transfers between devices: 20.1 us -> 7.6 us  [exchange(): lax.all_to_all(x, axis, split_axis=0, concat_axis=0, axis_index_groups=gr...]
  transfers between devices with their start and end apart: 8 -> 7, of which waited for: 6 -> 5; matrix products, arithmetic and copies ran while one was open for 1% -> 1% of each run, Pallas kernels for 5% -> 5%
where the time goes in v7:
time: 129 us; the launch traced here: 127 us
  blocking collectives  63 us (49%)
  starting transfers between devices  35.2 us (27%)
  Pallas kernels  16.8 us (13%)
  waiting for transfers between devices  10.7 us (8%)
    all_to_all x4, blocking collectives, exchange(): lax.all_to_all(x, axis, split_axis=0, concat_axis=0, axis_index_groups=gr...  63 us
    all_to_all x2, starting transfers between devices, exchange(): lax.all_to_all(x, axis, split_axis=0, concat_axis=0, axis_index_groups=gr...  22 us
    pallas_call x11, Pallas kernels, call(): pl.pallas_call(body, out_shape=outs, in_specs=[kinds.get(i, vmem) for i i...  16.8 us
    ppermute x5, starting transfers between devices, core_swap(): lax.ppermute(x, 'tp', [(i, i ^ 1) for i in range(lax.axis_size('tp'))])  13.2 us
    all_to_all x2, waiting for transfers between devices, exchange(): lax.all_to_all(x, axis, split_axis=0, concat_axis=0, axis_index_groups=gr...  7.6 us
    ppermute x5, waiting for transfers between devices, core_swap(): lax.ppermute(x, 'tp', [(i, i ^ 1) for i in range(lax.axis_size('tp'))])  3.08 us
  transfers between devices with their start and end apart: 7, of which 5 were waited for; matrix products, arithmetic and copies ran while one was open for 1% of the time, Pallas kernels for 5%

profile of v7, /device:TPU:1, one launch (start us, length us, event | category | flops | bytes accessed | tf_op | source)
XLA Modules:
  0.0 127.3 jit_solution(18032368354776348787)
XLA Ops:
  0.0 2.1 %shard_map.244 = (f32[16,8,128]{2,1,0:T(8,128)}, bf16[16,2048]{1,0:T(8,128)(2,1)S(1)}) custom-call(bf16[16,2048]{1,0:T(8,128)(2,1)} %hidden.1, bf16[2048]{0:T(1024)(128)(2,1)} %refs_1_.1, bf16[64,2048]{1,0:T(8,128)(2,1)} %bitcast.14, bf16[32,2048]{1,0:T(8,128)(2,1)} %bitcast.17, bf16[64,512]{1,0:T(8,128)(2,1)} %refs_4_.1), custom_call_target="tpu_custom_call" | custom-call | tf_op jit(solution)/shard_map/pallas_call | solution.py:54
  2.1 17.4 %all-to-all-start = ((f32[16,8,128]{2,1,0:T(8,128)}), f32[16,8,128]{2,1,0:T(8,128)S(1)}, u32[]{:S(2)}, u32[]{:S(2)}) async-start(f32[16,8,128]{2,1,0:T(8,128)} %get-tuple-element.35), calls=%async_computation | async-start | bytes 131072 | tf_op jit(solution)/shard_map/all_to_all | solution.py:21
  20.1 0.7 fusion
  20.8 0.0 copy-start.6
  20.8 0.0 copy-start.7
  20.8 3.1 %shard_map.245 = (f32[1,640]{1,0:T(1,128)S(1)}, bf16[1632,512]{1,0:T(8,128)(2,1)S(1)}) custom-call(s32[1]{0:T(128)} %bitcast.index, bf16[16,2048]{1,0:T(8,128)(2,1)S(1)} %get-tuple-element.36.normed, bf16[2048,512]{1,0:T(8,128)(2,1)} %w_latent.1, bf16[32,2048]{1,0:T(8,128)(2,1)} %bitcast.18, bf16[512]{0:T(512)(128)(2,1)} %gain.5, ...), custom_call_target="tpu_custom_call" | custom-call | tf_op jit(solution)/shard_map/pallas_call | solution.py:54
  23.9 0.0 copy-start
  23.9 0.0 copy-start.2
  24.0 0.0 copy-start.5
  24.0 3.3 %all-to-all-done.queries = f32[16,8,128]{2,1,0:T(8,128)S(1)} async-done(((f32[16,8,128]{2,1,0:T(8,128)}), f32[16,8,128]{2,1,0:T(8,128)S(1)}, u32[]{:S(2)}, u32[]{:S(2)}) %all-to-all-start) | async-done | bytes 65568 | tf_op jit(solution)/shard_map/all_to_all | solution.py:21
  27.3 0.0 copy-done.6
  27.3 0.0 copy-done.7
  27.3 0.0 copy-start.1
  27.3 0.0 copy-start.4
  27.3 1.8 %shard_map.246 = f32[16,8,128]{2,1,0:T(8,128)} custom-call(s32[1]{0:T(128)S(6)} %copy.27.lengths, f32[16,8,128]{2,1,0:T(8,128)S(1)} %all-to-all-done.queries, bf16[1632,512]{1,0:T(8,128)(2,1)S(1)} %get-tuple-element.39.caches, f32[1,640]{1,0:T(1,128)S(1)} %get-tuple-element.40.token, f32[1,16]{1,0:T(1,128)S(1)} %copy-done.7, f32[1,16]{1,0:T(1,128)S(1)} %copy-done.6), custom_call_target="tpu_custom_call" | custom-call | tf_op jit(solution)/shard_map/pallas_call | solution.py:54
  29.2 1.3 %shard_map.247 = (bf16[80,1536]{1,0:T(8,128)(2,1)S(1)}, bf16[48,128]{1,0:T(8,128)(2,1)S(1)}) custom-call(s32[1]{0:T(128)} %bitcast.index, s32[4,16]{1,0:T(4,128)} %bitcast.12, f32[4,16]{1,0:T(4,128)} %bitcast.19, bf16[64,512]{1,0:T(8,128)(2,1)} %bitcast.10, bf16[64]{0:T(256)(128)(2,1)} %gain.7, bf16[64,2048]{1,0:T(8,128)(2,1)} %w_output.3), custom_call_target="tpu_custom_call" | custom-call | tf_op jit(solution)/shard_map/pallas_call | solution.py:54
  30.5 2.1 %collective-permute-start = (bf16[80,1536]{1,0:T(8,128)(2,1)S(1)}, bf16[80,1536]{1,0:T(8,128)(2,1)S(1)}, u32[]{:S(2)}, u32[]{:S(2)}) collective-permute-start(bf16[80,1536]{1,0:T(8,128)(2,1)S(1)} %get-tuple-element.43), channel_id=1, source_target_pairs={{0,1},{1,0},{2,3},{3,2},{4,5},{5,4},{6,7},{7,6},{8,9},{9,8},{10,11... | collective-permute-start | bytes 737288 | tf_op jit(solution)/shard_map/ppermute | solution.py:27
  32.6 11.7 %all_to_all.30.attended = f32[16,8,128]{2,1,0:T(8,128)S(1)} all-to-all(f32[16,8,128]{2,1,0:T(8,128)} %shard_map.246), channel_id=1, replica_groups=mesh['ep'=64,'tp'=16] {'tp'}, dimensions={0} | all-to-all | bytes 131072 | tf_op jit(solution)/shard_map/all_to_all | solution.py:21
  44.3 0.0 collective-permute-done.pack
  44.3 0.0 copy-done
  44.3 0.0 copy-done.2
  44.3 0.0 copy-done.5
  44.3 0.4 shard_map.248
  44.7 0.0 copy-start.3
  44.8 14.8 %all_to_all.31.shares = bf16[8,128,128]{2,1,0:T(8,128)(2,1)S(1)} all-to-all(bf16[8,128,128]{2,1,0:T(8,128)(2,1)S(1)} %shard_map.248), channel_id=1, replica_groups={{0,2,4,6,8,10,12,14},{1,3,5,7,9,11,13,15},{16,18,20,22,24,26,28,30},{17..., dimensions={0} | all-to-all | bytes 524288 | tf_op jit(solution)/shard_map/all_to_all | solution.py:21
  59.5 0.0 copy-done.1
  59.5 0.0 copy-done.4
  59.5 1.1 shard_map.249
  60.6 0.0 copy-start.8
  60.6 1.5 %shard_map.250 = (bf16[2560,256]{1,0:T(8,128)(2,1)S(1)}, bf16[512,256]{1,0:T(8,128)(2,1)S(1)}) custom-call(s32[1]{0:T(128)} %bitcast.index, bf16[1,2048,128]{2,1,0:T(8,128)(2,1)} %w_gate.1, bf16[1,2048,128]{2,1,0:T(8,128)(2,1)} %w_up.1, bf16[1,128,2048]{2,1,0:T(8,128)(2,1)} %w_down.1), custom_call_target="tpu_custom_call" | custom-call | tf_op jit(solution)/shard_map/pallas_call | solution.py:54
  62.2 2.4 %collective-permute-start.1 = (bf16[2560,256]{1,0:T(8,128)(2,1)S(1)}, bf16[2560,256]{1,0:T(8,128)(2,1)S(1)}, u32[]{:S(2)}, u32[]{:S(2)}) collective-permute-start(bf16[2560,256]{1,0:T(8,128)(2,1)S(1)} %get-tuple-element.54.packed), channel_id=1, source_target_pairs={{0,1},{1,0},{2,3},{3,2},{4,5},{5,4},{6,7},{7,6},{8,9},{9,8},{10,11... | collective-permute-start | bytes 3932168 | tf_op jit(solution)/shard_map/ppermute | solution.py:27
  64.5 0.0 copy-done.8
  64.5 27.3 %all_to_all.32.arrived = bf16[64,16,128]{2,1,0:T(8,128)(2,1)S(1)} all-to-all(bf16[64,16,128]{2,1,0:T(8,128)(2,1)S(1)} %copy-done.8), channel_id=1, replica_groups=mesh['ep'=64,'tp'=16] {'ep'}, dimensions={0} | all-to-all | bytes 524288 | tf_op jit(solution)/shard_map/all_to_all | solution.py:21
  91.8 0.0 collective-permute-done.1.away
  91.8 4.3 %collective-permute-start.2 = (bf16[64,16,128]{2,1,0:T(8,128)(2,1)S(1)}, bf16[64,16,128]{2,1,0:T(8,128)(2,1)S(1)}, u32[]{:S(2)}, u32[]{:S(2)}) collective-permute-start(bf16[64,16,128]{2,1,0:T(8,128)(2,1)S(1)} %all_to_all.32.arrived), channel_id=1, source_target_pairs={{0,1},{1,0},{2,3},{3,2},{4,5},{5,4},{6,7},{7,6},{8,9},{9,8},{10,11... | collective-permute-start | bytes 786440 | tf_op jit(solution)/shard_map/ppermute | solution.py:27
  96.1 1.1 collective-permute-done.2.other
  97.2 0.0 copy-done.3
  97.2 1.8 %shard_map.251 = bf16[64,16,128]{2,1,0:T(8,128)(2,1)} custom-call(s32[1]{0:T(128)} %bitcast.index, bf16[64,16,128]{2,1,0:T(8,128)(2,1)S(1)} %all_to_all.32.arrived, bf16[64,16,128]{2,1,0:T(8,128)(2,1)S(1)} %collective-permute-done.2.other, bf16[2048]{0:T(1024)(128)(2,1)S(1)} %copy-done.3, bf16[2560,256]{1,0:T(8,128)(2,1)S(1)} %get-tuple-element.54.packed, ...), custom_call_target="tpu_custom_call" | custom-call | tf_op jit(solution)/shard_map/pallas_call | solution.py:54
  99.0 4.6 %all-to-all-start.4 = ((bf16[64,16,128]{2,1,0:T(8,128)(2,1)}), bf16[64,16,128]{2,1,0:T(8,128)(2,1)S(1)}, u32[]{:S(2)}, u32[]{:S(2)}) async-start(bf16[64,16,128]{2,1,0:T(8,128)(2,1)} %shard_map.251), calls=%async_computation.4 | async-start | bytes 524288 | tf_op jit(solution)/shard_map/all_to_all | solution.py:21
  103.6 2.3 %collective-permute-start.3 = (bf16[128,128]{1,0:T(8,128)(2,1)S(1)}, bf16[128,128]{1,0:T(8,128)(2,1)S(1)}, u32[]{:S(2)}, u32[]{:S(2)}) collective-permute-start(bf16[128,128]{1,0:T(8,128)(2,1)S(1)} %get-tuple-element.59.middle), channel_id=1, source_target_pairs={{0,1},{1,0},{2,3},{3,2},{4,5},{5,4},{6,7},{7,6},{8,9},{9,8},{10,11... | collective-permute-start | bytes 98312 | tf_op jit(solution)/shard_map/ppermute | solution.py:27
  105.9 0.8 collective-permute-done.3.other
  106.8 2.7 %shard_map.252 = (f32[128,128]{1,0:T(8,128)S(1)}, f32[128,128]{1,0:T(8,128)}) custom-call(s32[1]{0:T(128)} %bitcast.index, bf16[128,128]{1,0:T(8,128)(2,1)S(1)} %get-tuple-element.59.middle, bf16[128,128]{1,0:T(8,128)(2,1)S(1)} %collective-permute-done.3.other, bf16[2048]{0:T(1024)(128)(2,1)} %gain.9, bf16[64,2048]{1,0:T(8,128)(2,1)} %bitcast.15, ...), custom_call_target="tpu_custom_call" | custom-call | tf_op jit(solution)/shard_map/pallas_call | solution.py:54
  109.5 2.2 %collective-permute-start.4 = (f32[128,128]{1,0:T(8,128)}, f32[128,128]{1,0:T(8,128)S(1)}, u32[]{:S(2)}, u32[]{:S(2)}) collective-permute-start(f32[128,128]{1,0:T(8,128)} %get-tuple-element.61), channel_id=1, source_target_pairs={{0,1},{1,0},{2,3},{3,2},{4,5},{5,4},{6,7},{7,6},{8,9},{9,8},{10,11... | collective-permute-start | bytes 196616 | tf_op jit(solution)/shard_map/ppermute | solution.py:27
  111.7 1.1 collective-permute-done.4
  112.8 4.3 %all-to-all-done.4.returned = bf16[64,16,128]{2,1,0:T(8,128)(2,1)S(1)} async-done(((bf16[64,16,128]{2,1,0:T(8,128)(2,1)}), bf16[64,16,128]{2,1,0:T(8,128)(2,1)S(1)}, u32[]{:S(2)}, u32[]{:S(2)}) %all-to-all-start.4) | async-done | bytes 262176 | tf_op jit(solution)/shard_map/all_to_all | solution.py:21
  117.1 0.2 shard_map.253
  117.4 9.3 %all_to_all.33.tiles = bf16[8,16,128]{2,1,0:T(8,128)(2,1)S(1)} all-to-all(bf16[8,16,128]{2,1,0:T(8,128)(2,1)S(1)} %shard_map.253), channel_id=1, replica_groups={{0,2,4,6,8,10,12,14},{1,3,5,7,9,11,13,15},{16,18,20,22,24,26,28,30},{17..., dimensions={0} | all-to-all | bytes 65536 | tf_op jit(solution)/shard_map/all_to_all | solution.py:21
  126.6 0.6 shard_map.254
  (1 shorter events, 0.0 us)
Async XLA Ops:
  2.1 25.2 %all-to-all-start = ((f32[16,8,128]{2,1,0:T(8,128)}), f32[16,8,128]{2,1,0:T(8,128)S(1)}, u32[]{:S(2)}, u32[]{:S(2)}) async-start(f32[16,8,128]{2,1,0:T(8,128)} %get-tuple-element.35), calls=%async_computation | async-start | bytes 131072 | tf_op jit(solution)/shard_map/all_to_all | solution.py:21
  20.8 6.5 %copy-start.6 = (f32[1,16]{1,0:T(1,128)S(1)}, f32[1,16]{1,0:T(1,128)}, u32[]{:S(2)}) copy-start(f32[1,16]{1,0:T(1,128)} %get-tuple-element.65.sin) | copy-start | bytes 196
  20.8 6.5 %copy-start.7 = (f32[1,16]{1,0:T(1,128)S(1)}, f32[1,16]{1,0:T(1,128)}, u32[]{:S(2)}) copy-start(f32[1,16]{1,0:T(1,128)} %get-tuple-element.66.cos) | copy-start | bytes 196
  23.9 20.4 %copy-start = (bf16[64,2048]{1,0:T(8,128)(2,1)S(1)}, bf16[64,2048]{1,0:T(8,128)(2,1)}, u32[]{:S(2)}) copy-start(bf16[64,2048]{1,0:T(8,128)(2,1)} %w_output.3) | copy-start | bytes 786436
  23.9 20.4 %copy-start.2 = (bf16[512,64]{0,1:T(8,128)(2,1)S(1)}, bf16[512,64]{0,1:T(8,128)(2,1)}, u32[]{:S(2)}) copy-start(bf16[512,64]{0,1:T(8,128)(2,1)} %param.37) | copy-start | bytes 196612
  24.0 20.4 %copy-start.5 = (bf16[64]{0:T(256)(128)(2,1)S(1)}, bf16[64]{0:T(256)(128)(2,1)}, u32[]{:S(2)}) copy-start(bf16[64]{0:T(256)(128)(2,1)} %gain.7) | copy-start | bytes 388
  27.3 32.2 %copy-start.1 = (bf16[16,2048]{1,0:T(8,128)(2,1)S(1)}, bf16[16,2048]{1,0:T(8,128)(2,1)}, u32[]{:S(2)}) copy-start(bf16[16,2048]{1,0:T(8,128)(2,1)} %hidden.1) | copy-start | bytes 196612
  27.3 32.2 %copy-start.4 = (s32[16,4]{0,1:T(4,128)S(1)}, s32[16,4]{0,1:T(4,128)}, u32[]{:S(2)}) copy-start(s32[16,4]{0,1:T(4,128)} %param.41) | copy-start | bytes 772
  30.5 13.8 %collective-permute-start = (bf16[80,1536]{1,0:T(8,128)(2,1)S(1)}, bf16[80,1536]{1,0:T(8,128)(2,1)S(1)}, u32[]{:S(2)}, u32[]{:S(2)}) collective-permute-start(bf16[80,1536]{1,0:T(8,128)(2,1)S(1)} %get-tuple-element.43), channel_id=1, source_target_pairs={{0,1},{1,0},{2,3},{3,2},{4,5},{5,4},{6,7},{7,6},{8,9},{9,8},{10,11... | collective-permute-start | bytes 737288 | tf_op jit(solution)/shard_map/ppermute | solution.py:27
  44.7 52.5 %copy-start.3 = (bf16[2048]{0:T(1024)(128)(2,1)S(1)}, bf16[2048]{0:T(1024)(128)(2,1)}, u32[]{:S(2)}) copy-start(bf16[2048]{0:T(1024)(128)(2,1)} %gain.9) | copy-start | bytes 12292
  60.6 3.9 %copy-start.8 = (bf16[64,16,128]{2,1,0:T(8,128)(2,1)S(1)}, bf16[64,16,128]{2,1,0:T(8,128)(2,1)}, u32[]{:S(2)}) copy-start(bf16[64,16,128]{2,1,0:T(8,128)(2,1)} %get-tuple-element.49) | copy-start | bytes 786436
  62.2 29.6 %collective-permute-start.1 = (bf16[2560,256]{1,0:T(8,128)(2,1)S(1)}, bf16[2560,256]{1,0:T(8,128)(2,1)S(1)}, u32[]{:S(2)}, u32[]{:S(2)}) collective-permute-start(bf16[2560,256]{1,0:T(8,128)(2,1)S(1)} %get-tuple-element.54.packed), channel_id=1, source_target_pairs={{0,1},{1,0},{2,3},{3,2},{4,5},{5,4},{6,7},{7,6},{8,9},{9,8},{10,11... | collective-permute-start | bytes 3932168 | tf_op jit(solution)/shard_map/ppermute | solution.py:27
  91.8 5.4 %collective-permute-start.2 = (bf16[64,16,128]{2,1,0:T(8,128)(2,1)S(1)}, bf16[64,16,128]{2,1,0:T(8,128)(2,1)S(1)}, u32[]{:S(2)}, u32[]{:S(2)}) collective-permute-start(bf16[64,16,128]{2,1,0:T(8,128)(2,1)S(1)} %all_to_all.32.arrived), channel_id=1, source_target_pairs={{0,1},{1,0},{2,3},{3,2},{4,5},{5,4},{6,7},{7,6},{8,9},{9,8},{10,11... | collective-permute-start | bytes 786440 | tf_op jit(solution)/shard_map/ppermute | solution.py:27
  99.0 18.1 %all-to-all-start.4 = ((bf16[64,16,128]{2,1,0:T(8,128)(2,1)}), bf16[64,16,128]{2,1,0:T(8,128)(2,1)S(1)}, u32[]{:S(2)}, u32[]{:S(2)}) async-start(bf16[64,16,128]{2,1,0:T(8,128)(2,1)} %shard_map.251), calls=%async_computation.4 | async-start | bytes 524288 | tf_op jit(solution)/shard_map/all_to_all | solution.py:21
  103.6 3.1 %collective-permute-start.3 = (bf16[128,128]{1,0:T(8,128)(2,1)S(1)}, bf16[128,128]{1,0:T(8,128)(2,1)S(1)}, u32[]{:S(2)}, u32[]{:S(2)}) collective-permute-start(bf16[128,128]{1,0:T(8,128)(2,1)S(1)} %get-tuple-element.59.middle), channel_id=1, source_target_pairs={{0,1},{1,0},{2,3},{3,2},{4,5},{5,4},{6,7},{7,6},{8,9},{9,8},{10,11... | collective-permute-start | bytes 98312 | tf_op jit(solution)/shard_map/ppermute | solution.py:27
  109.5 3.3 %collective-permute-start.4 = (f32[128,128]{1,0:T(8,128)}, f32[128,128]{1,0:T(8,128)S(1)}, u32[]{:S(2)}, u32[]{:S(2)}) collective-permute-start(f32[128,128]{1,0:T(8,128)} %get-tuple-element.61), channel_id=1, source_target_pairs={{0,1},{1,0},{2,3},{3,2},{4,5},{5,4},{6,7},{7,6},{8,9},{9,8},{10,11... | collective-permute-start | bytes 196616 | tf_op jit(solution)/shard_map/ppermute | solution.py:27

commit v8 on v7

--- a/solution.py
+++ b/solution.py
@@ -74,7 +74,7 @@
 
 
 def query_body(*refs):
-    sources, (out, normed_out, *held, sems) = refs[:5], refs[5:]
+    sources, (result, normed_out, *held, out, sems) = refs[:5], refs[5:]
     copies = [
         pltpu.make_async_copy(source, place, sems.at[k])
         for k, (source, place) in enumerate(zip(sources, held))
@@ -99,6 +99,7 @@
     out[:, 4, :] = jnp.concatenate([rope, jnp.zeros((rows, LANES - ROPE), F32)], axis=1)
     for s in range(5, 8):
         out[:, s, :] = jnp.zeros((rows, LANES), F32)
+    result[...] = out[...].astype(BF16)
 
 
 def rotated(values, cos, sin):
@@ -131,7 +132,8 @@
         copy.wait()
 
 
-def attention_body(lengths, queries, caches, token, cos, sin, out):
+def attention_body(lengths, arrived, caches, token, cos, sin, result, queries, out):
+    queries[...] = arrived[...].astype(F32)
     new_latent = token[:, :LATENT_UNITS]
     new_key = token[:, LATENT_UNITS : LATENT_UNITS + ROPE]
     parts = [queries[:, s, :] for s in range(LATENT_UNITS // LANES)]
@@ -167,6 +169,7 @@
         tile = slice(s * LANES, (s + 1) * LANES)
         out[:, s, :] = first[:, tile]
         out[:, count + s, :] = second[:, tile]
+    result[...] = out[...].astype(BF16)
 
 
 def tile_at(number):
@@ -218,7 +221,8 @@
     return (head * factor * gains).astype(BF16)
 
 
-def head_body(index, attended, value_up, gain, w_output, pack, out):
+def head_body(index, arrived, value_up, gain, w_output, pack, out, attended):
+    attended[...] = arrived[...].astype(F32)
     core = index[0] % 2
     count = LATENT_UNITS // LANES
     first = jnp.concatenate([attended[:, s, :] for s in range(count)], axis=1)
@@ -403,7 +407,8 @@
     places = latent_cache.shape[1]
     chips = tp // 2
     same_core = [list(range(core, tp, 2)) for core in range(2)]
-    small = shape((tp, 8, LANES), F32)
+    small = shape((tp, 8, LANES), BF16)
+    spread = pltpu.VMEM((tp, 8, LANES), F32)
     half = (chips * tokens, LANES)
     large = shape((ep, slots * chips // ep, LANES), BF16)
     wide = pltpu.VMEM((slots * chips, LANES), F32)
@@ -417,6 +422,7 @@
         leave=(0,),
         scratch=(
             *(pltpu.VMEM(x.shape, BF16) for x in sources),
+            spread,
             pltpu.SemaphoreType.DMA((len(sources),)),
         ),
     )
@@ -455,6 +461,7 @@
         (lengths, queries, cache, token, cos, sin),
         smem=(0,),
         leave=(0,),
+        scratch=(spread, spread),
     )
     payload, later = together(payload, index)
     attended = exchange(payload, "tp")
@@ -476,6 +483,7 @@
         shape((chips,) + half, BF16),
         (index, attended, value_up_weight.T, head_gain, w_output, pack),
         smem=(0,),
+        scratch=(spread,),
     )
     shares = exchange(payload, "tp", same_core)
 

time: 129 us -> 129 us (level)
  no operation moved by 1% of the time
where the time goes in v8:
time: 129 us; the launch traced here: 127 us
  blocking collectives  62.8 us (49%)
  starting transfers between devices  35.4 us (27%)
  Pallas kernels  16.8 us (13%)
  waiting for transfers between devices  10.4 us (8%)
    all_to_all x4, blocking collectives, exchange(): lax.all_to_all(x, axis, split_axis=0, concat_axis=0, axis_index_groups=gr...  62.8 us
    all_to_all x2, starting transfers between devices, exchange(): lax.all_to_all(x, axis, split_axis=0, concat_axis=0, axis_index_groups=gr...  22 us
    pallas_call x11, Pallas kernels, call(): pl.pallas_call(body, out_shape=outs, in_specs=[kinds.get(i, vmem) for i i...  16.8 us
    ppermute x5, starting transfers between devices, core_swap(): lax.ppermute(x, 'tp', [(i, i ^ 1) for i in range(lax.axis_size('tp'))])  13.4 us
    all_to_all x2, waiting for transfers between devices, exchange(): lax.all_to_all(x, axis, split_axis=0, concat_axis=0, axis_index_groups=gr...  7.28 us
    ppermute x5, waiting for transfers between devices, core_swap(): lax.ppermute(x, 'tp', [(i, i ^ 1) for i in range(lax.axis_size('tp'))])  3.08 us
  transfers between devices with their start and end apart: 7, of which 5 were waited for; matrix products, arithmetic and copies ran while one was open for 1% of the time, Pallas kernels for 5%

profile of v8, /device:TPU:1, one launch (start us, length us, event | category | flops | bytes accessed | tf_op | source)
XLA Modules:
  0.0 126.8 jit_solution(17109499468855066584)
XLA Ops:
  0.0 2.1 %shard_map.244 = (bf16[16,8,128]{2,1,0:T(8,128)(2,1)}, bf16[16,2048]{1,0:T(8,128)(2,1)S(1)}) custom-call(bf16[16,2048]{1,0:T(8,128)(2,1)} %hidden.1, bf16[2048]{0:T(1024)(128)(2,1)} %refs_1_.1, bf16[64,2048]{1,0:T(8,128)(2,1)} %bitcast.14, bf16[32,2048]{1,0:T(8,128)(2,1)} %bitcast.17, bf16[64,512]{1,0:T(8,128)(2,1)} %refs_4_.1), custom_call_target="tpu_custom_call" | custom-call | tf_op jit(solution)/shard_map/pallas_call | solution.py:54
  2.1 17.4 %all-to-all-start = ((bf16[16,8,128]{2,1,0:T(8,128)(2,1)}), bf16[16,8,128]{2,1,0:T(8,128)(2,1)S(1)}, u32[]{:S(2)}, u32[]{:S(2)}) async-start(bf16[16,8,128]{2,1,0:T(8,128)(2,1)} %get-tuple-element.35), calls=%async_computation | async-start | bytes 65536 | tf_op jit(solution)/shard_map/all_to_all | solution.py:21
  20.1 0.6 fusion
  20.8 0.0 copy-start.6
  20.8 0.0 copy-start.7
  20.8 3.1 %shard_map.245 = (f32[1,640]{1,0:T(1,128)S(1)}, bf16[1632,512]{1,0:T(8,128)(2,1)S(1)}) custom-call(s32[1]{0:T(128)} %bitcast.index, bf16[16,2048]{1,0:T(8,128)(2,1)S(1)} %get-tuple-element.36.normed, bf16[2048,512]{1,0:T(8,128)(2,1)} %w_latent.1, bf16[32,2048]{1,0:T(8,128)(2,1)} %bitcast.18, bf16[512]{0:T(512)(128)(2,1)} %gain.5, ...), custom_call_target="tpu_custom_call" | custom-call | tf_op jit(solution)/shard_map/pallas_call | solution.py:54
  23.9 0.0 copy-start
  23.9 0.0 copy-start.2
  23.9 0.0 copy-start.5
  23.9 3.0 %all-to-all-done.arrived = bf16[16,8,128]{2,1,0:T(8,128)(2,1)S(1)} async-done(((bf16[16,8,128]{2,1,0:T(8,128)(2,1)}), bf16[16,8,128]{2,1,0:T(8,128)(2,1)S(1)}, u32[]{:S(2)}, u32[]{:S(2)}) %all-to-all-start) | async-done | bytes 32800 | tf_op jit(solution)/shard_map/all_to_all | solution.py:21
  27.0 0.0 copy-done.6
  27.0 0.0 copy-done.7
  27.0 0.0 copy-start.1
  27.0 0.0 copy-start.4
  27.0 1.9 %shard_map.246 = bf16[16,8,128]{2,1,0:T(8,128)(2,1)} custom-call(s32[1]{0:T(128)S(6)} %copy.27.lengths, bf16[16,8,128]{2,1,0:T(8,128)(2,1)S(1)} %all-to-all-done.arrived, bf16[1632,512]{1,0:T(8,128)(2,1)S(1)} %get-tuple-element.39.caches, f32[1,640]{1,0:T(1,128)S(1)} %get-tuple-element.40.token, f32[1,16]{1,0:T(1,128)S(1)} %copy-done.7, f32[1,16]{1,0:T(1,128)S(1)} %copy-done.6), custom_call_target="tpu_custom_call" | custom-call | tf_op jit(solution)/shard_map/pallas_call | solution.py:54
  28.8 1.3 %shard_map.247 = (bf16[80,1536]{1,0:T(8,128)(2,1)S(1)}, bf16[48,128]{1,0:T(8,128)(2,1)S(1)}) custom-call(s32[1]{0:T(128)} %bitcast.index, s32[4,16]{1,0:T(4,128)} %bitcast.12, f32[4,16]{1,0:T(4,128)} %bitcast.19, bf16[64,512]{1,0:T(8,128)(2,1)} %bitcast.10, bf16[64]{0:T(256)(128)(2,1)} %gain.7, bf16[64,2048]{1,0:T(8,128)(2,1)} %w_output.3), custom_call_target="tpu_custom_call" | custom-call | tf_op jit(solution)/shard_map/pallas_call | solution.py:54
  30.2 2.3 %collective-permute-start = (bf16[80,1536]{1,0:T(8,128)(2,1)S(1)}, bf16[80,1536]{1,0:T(8,128)(2,1)S(1)}, u32[]{:S(2)}, u32[]{:S(2)}) collective-permute-start(bf16[80,1536]{1,0:T(8,128)(2,1)S(1)} %get-tuple-element.43), channel_id=1, source_target_pairs={{0,1},{1,0},{2,3},{3,2},{4,5},{5,4},{6,7},{7,6},{8,9},{9,8},{10,11... | collective-permute-start | bytes 737288 | tf_op jit(solution)/shard_map/ppermute | solution.py:27
  32.5 11.4 %all_to_all.30.arrived = bf16[16,8,128]{2,1,0:T(8,128)(2,1)S(1)} all-to-all(bf16[16,8,128]{2,1,0:T(8,128)(2,1)} %shard_map.246), channel_id=1, replica_groups=mesh['ep'=64,'tp'=16] {'tp'}, dimensions={0} | all-to-all | bytes 65536 | tf_op jit(solution)/shard_map/all_to_all | solution.py:21
  43.9 0.0 collective-permute-done.pack
  43.9 0.0 copy-done
  43.9 0.0 copy-done.2
  43.9 0.0 copy-done.5
  43.9 0.4 shard_map.248
  44.4 0.0 copy-start.3
  44.4 14.7 %all_to_all.31.shares = bf16[8,128,128]{2,1,0:T(8,128)(2,1)S(1)} all-to-all(bf16[8,128,128]{2,1,0:T(8,128)(2,1)S(1)} %shard_map.248), channel_id=1, replica_groups={{0,2,4,6,8,10,12,14},{1,3,5,7,9,11,13,15},{16,18,20,22,24,26,28,30},{17..., dimensions={0} | all-to-all | bytes 524288 | tf_op jit(solution)/shard_map/all_to_all | solution.py:21
  59.1 0.0 copy-done.1
  59.1 0.0 copy-done.4
  59.1 1.1 shard_map.249
  60.2 0.0 copy-start.8
  60.2 1.5 %shard_map.250 = (bf16[2560,256]{1,0:T(8,128)(2,1)S(1)}, bf16[512,256]{1,0:T(8,128)(2,1)S(1)}) custom-call(s32[1]{0:T(128)} %bitcast.index, bf16[1,2048,128]{2,1,0:T(8,128)(2,1)} %w_gate.1, bf16[1,2048,128]{2,1,0:T(8,128)(2,1)} %w_up.1, bf16[1,128,2048]{2,1,0:T(8,128)(2,1)} %w_down.1), custom_call_target="tpu_custom_call" | custom-call | tf_op jit(solution)/shard_map/pallas_call | solution.py:54
  61.7 2.4 %collective-permute-start.1 = (bf16[2560,256]{1,0:T(8,128)(2,1)S(1)}, bf16[2560,256]{1,0:T(8,128)(2,1)S(1)}, u32[]{:S(2)}, u32[]{:S(2)}) collective-permute-start(bf16[2560,256]{1,0:T(8,128)(2,1)S(1)} %get-tuple-element.54.packed), channel_id=1, source_target_pairs={{0,1},{1,0},{2,3},{3,2},{4,5},{5,4},{6,7},{7,6},{8,9},{9,8},{10,11... | collective-permute-start | bytes 3932168 | tf_op jit(solution)/shard_map/ppermute | solution.py:27
  64.1 0.0 copy-done.8
  64.2 27.4 %all_to_all.32.arrived = bf16[64,16,128]{2,1,0:T(8,128)(2,1)S(1)} all-to-all(bf16[64,16,128]{2,1,0:T(8,128)(2,1)S(1)} %copy-done.8), channel_id=1, replica_groups=mesh['ep'=64,'tp'=16] {'ep'}, dimensions={0} | all-to-all | bytes 524288 | tf_op jit(solution)/shard_map/all_to_all | solution.py:21
  91.5 0.0 collective-permute-done.1.away
  91.5 4.1 %collective-permute-start.2 = (bf16[64,16,128]{2,1,0:T(8,128)(2,1)S(1)}, bf16[64,16,128]{2,1,0:T(8,128)(2,1)S(1)}, u32[]{:S(2)}, u32[]{:S(2)}) collective-permute-start(bf16[64,16,128]{2,1,0:T(8,128)(2,1)S(1)} %all_to_all.32.arrived), channel_id=1, source_target_pairs={{0,1},{1,0},{2,3},{3,2},{4,5},{5,4},{6,7},{7,6},{8,9},{9,8},{10,11... | collective-permute-start | bytes 786440 | tf_op jit(solution)/shard_map/ppermute | solution.py:27
  95.7 1.1 collective-permute-done.2.other
  96.8 0.0 copy-done.3
  96.8 1.8 %shard_map.251 = bf16[64,16,128]{2,1,0:T(8,128)(2,1)} custom-call(s32[1]{0:T(128)} %bitcast.index, bf16[64,16,128]{2,1,0:T(8,128)(2,1)S(1)} %all_to_all.32.arrived, bf16[64,16,128]{2,1,0:T(8,128)(2,1)S(1)} %collective-permute-done.2.other, bf16[2048]{0:T(1024)(128)(2,1)S(1)} %copy-done.3, bf16[2560,256]{1,0:T(8,128)(2,1)S(1)} %get-tuple-element.54.packed, ...), custom_call_target="tpu_custom_call" | custom-call | tf_op jit(solution)/shard_map/pallas_call | solution.py:54
  98.6 4.6 %all-to-all-start.4 = ((bf16[64,16,128]{2,1,0:T(8,128)(2,1)}), bf16[64,16,128]{2,1,0:T(8,128)(2,1)S(1)}, u32[]{:S(2)}, u32[]{:S(2)}) async-start(bf16[64,16,128]{2,1,0:T(8,128)(2,1)} %shard_map.251), calls=%async_computation.4 | async-start | bytes 524288 | tf_op jit(solution)/shard_map/all_to_all | solution.py:21
  103.2 2.3 %collective-permute-start.3 = (bf16[128,128]{1,0:T(8,128)(2,1)S(1)}, bf16[128,128]{1,0:T(8,128)(2,1)S(1)}, u32[]{:S(2)}, u32[]{:S(2)}) collective-permute-start(bf16[128,128]{1,0:T(8,128)(2,1)S(1)} %get-tuple-element.59.middle), channel_id=1, source_target_pairs={{0,1},{1,0},{2,3},{3,2},{4,5},{5,4},{6,7},{7,6},{8,9},{9,8},{10,11... | collective-permute-start | bytes 98312 | tf_op jit(solution)/shard_map/ppermute | solution.py:27
  105.5 0.8 collective-permute-done.3.other
  106.4 2.7 %shard_map.252 = (f32[128,128]{1,0:T(8,128)S(1)}, f32[128,128]{1,0:T(8,128)}) custom-call(s32[1]{0:T(128)} %bitcast.index, bf16[128,128]{1,0:T(8,128)(2,1)S(1)} %get-tuple-element.59.middle, bf16[128,128]{1,0:T(8,128)(2,1)S(1)} %collective-permute-done.3.other, bf16[2048]{0:T(1024)(128)(2,1)} %gain.9, bf16[64,2048]{1,0:T(8,128)(2,1)} %bitcast.15, ...), custom_call_target="tpu_custom_call" | custom-call | tf_op jit(solution)/shard_map/pallas_call | solution.py:54
  109.1 2.2 %collective-permute-start.4 = (f32[128,128]{1,0:T(8,128)}, f32[128,128]{1,0:T(8,128)S(1)}, u32[]{:S(2)}, u32[]{:S(2)}) collective-permute-start(f32[128,128]{1,0:T(8,128)} %get-tuple-element.61), channel_id=1, source_target_pairs={{0,1},{1,0},{2,3},{3,2},{4,5},{5,4},{6,7},{7,6},{8,9},{9,8},{10,11... | collective-permute-start | bytes 196616 | tf_op jit(solution)/shard_map/ppermute | solution.py:27
  111.3 1.1 collective-permute-done.4
  112.4 4.3 %all-to-all-done.4.returned = bf16[64,16,128]{2,1,0:T(8,128)(2,1)S(1)} async-done(((bf16[64,16,128]{2,1,0:T(8,128)(2,1)}), bf16[64,16,128]{2,1,0:T(8,128)(2,1)S(1)}, u32[]{:S(2)}, u32[]{:S(2)}) %all-to-all-start.4) | async-done | bytes 262176 | tf_op jit(solution)/shard_map/all_to_all | solution.py:21
  116.7 0.2 shard_map.253
  117.0 9.3 %all_to_all.33.tiles = bf16[8,16,128]{2,1,0:T(8,128)(2,1)S(1)} all-to-all(bf16[8,16,128]{2,1,0:T(8,128)(2,1)S(1)} %shard_map.253), channel_id=1, replica_groups={{0,2,4,6,8,10,12,14},{1,3,5,7,9,11,13,15},{16,18,20,22,24,26,28,30},{17..., dimensions={0} | all-to-all | bytes 65536 | tf_op jit(solution)/shard_map/all_to_all | solution.py:21
  126.2 0.6 shard_map.254
  (1 shorter events, 0.0 us)
Async XLA Ops:
  2.1 24.9 %all-to-all-start = ((bf16[16,8,128]{2,1,0:T(8,128)(2,1)}), bf16[16,8,128]{2,1,0:T(8,128)(2,1)S(1)}, u32[]{:S(2)}, u32[]{:S(2)}) async-start(bf16[16,8,128]{2,1,0:T(8,128)(2,1)} %get-tuple-element.35), calls=%async_computation | async-start | bytes 65536 | tf_op jit(solution)/shard_map/all_to_all | solution.py:21
  20.8 6.2 %copy-start.6 = (f32[1,16]{1,0:T(1,128)S(1)}, f32[1,16]{1,0:T(1,128)}, u32[]{:S(2)}) copy-start(f32[1,16]{1,0:T(1,128)} %get-tuple-element.65.sin) | copy-start | bytes 196
  20.8 6.2 %copy-start.7 = (f32[1,16]{1,0:T(1,128)S(1)}, f32[1,16]{1,0:T(1,128)}, u32[]{:S(2)}) copy-start(f32[1,16]{1,0:T(1,128)} %get-tuple-element.66.cos) | copy-start | bytes 196
  23.9 20.0 %copy-start = (bf16[64,2048]{1,0:T(8,128)(2,1)S(1)}, bf16[64,2048]{1,0:T(8,128)(2,1)}, u32[]{:S(2)}) copy-start(bf16[64,2048]{1,0:T(8,128)(2,1)} %w_output.3) | copy-start | bytes 786436
  23.9 20.0 %copy-start.2 = (bf16[512,64]{0,1:T(8,128)(2,1)S(1)}, bf16[512,64]{0,1:T(8,128)(2,1)}, u32[]{:S(2)}) copy-start(bf16[512,64]{0,1:T(8,128)(2,1)} %param.37) | copy-start | bytes 196612
  23.9 20.0 %copy-start.5 = (bf16[64]{0:T(256)(128)(2,1)S(1)}, bf16[64]{0:T(256)(128)(2,1)}, u32[]{:S(2)}) copy-start(bf16[64]{0:T(256)(128)(2,1)} %gain.7) | copy-start | bytes 388
  27.0 32.1 %copy-start.1 = (bf16[16,2048]{1,0:T(8,128)(2,1)S(1)}, bf16[16,2048]{1,0:T(8,128)(2,1)}, u32[]{:S(2)}) copy-start(bf16[16,2048]{1,0:T(8,128)(2,1)} %hidden.1) | copy-start | bytes 196612
  27.0 32.1 %copy-start.4 = (s32[16,4]{0,1:T(4,128)S(1)}, s32[16,4]{0,1:T(4,128)}, u32[]{:S(2)}) copy-start(s32[16,4]{0,1:T(4,128)} %param.41) | copy-start | bytes 772
  30.2 13.8 %collective-permute-start = (bf16[80,1536]{1,0:T(8,128)(2,1)S(1)}, bf16[80,1536]{1,0:T(8,128)(2,1)S(1)}, u32[]{:S(2)}, u32[]{:S(2)}) collective-permute-start(bf16[80,1536]{1,0:T(8,128)(2,1)S(1)} %get-tuple-element.43), channel_id=1, source_target_pairs={{0,1},{1,0},{2,3},{3,2},{4,5},{5,4},{6,7},{7,6},{8,9},{9,8},{10,11... | collective-permute-start | bytes 737288 | tf_op jit(solution)/shard_map/ppermute | solution.py:27
  44.4 52.4 %copy-start.3 = (bf16[2048]{0:T(1024)(128)(2,1)S(1)}, bf16[2048]{0:T(1024)(128)(2,1)}, u32[]{:S(2)}) copy-start(bf16[2048]{0:T(1024)(128)(2,1)} %gain.9) | copy-start | bytes 12292
  60.2 4.0 %copy-start.8 = (bf16[64,16,128]{2,1,0:T(8,128)(2,1)S(1)}, bf16[64,16,128]{2,1,0:T(8,128)(2,1)}, u32[]{:S(2)}) copy-start(bf16[64,16,128]{2,1,0:T(8,128)(2,1)} %get-tuple-element.49) | copy-start | bytes 786436
  61.7 29.8 %collective-permute-start.1 = (bf16[2560,256]{1,0:T(8,128)(2,1)S(1)}, bf16[2560,256]{1,0:T(8,128)(2,1)S(1)}, u32[]{:S(2)}, u32[]{:S(2)}) collective-permute-start(bf16[2560,256]{1,0:T(8,128)(2,1)S(1)} %get-tuple-element.54.packed), channel_id=1, source_target_pairs={{0,1},{1,0},{2,3},{3,2},{4,5},{5,4},{6,7},{7,6},{8,9},{9,8},{10,11... | collective-permute-start | bytes 3932168 | tf_op jit(solution)/shard_map/ppermute | solution.py:27
  91.5 5.3 %collective-permute-start.2 = (bf16[64,16,128]{2,1,0:T(8,128)(2,1)S(1)}, bf16[64,16,128]{2,1,0:T(8,128)(2,1)S(1)}, u32[]{:S(2)}, u32[]{:S(2)}) collective-permute-start(bf16[64,16,128]{2,1,0:T(8,128)(2,1)S(1)} %all_to_all.32.arrived), channel_id=1, source_target_pairs={{0,1},{1,0},{2,3},{3,2},{4,5},{5,4},{6,7},{7,6},{8,9},{9,8},{10,11... | collective-permute-start | bytes 786440 | tf_op jit(solution)/shard_map/ppermute | solution.py:27
  98.6 18.1 %all-to-all-start.4 = ((bf16[64,16,128]{2,1,0:T(8,128)(2,1)}), bf16[64,16,128]{2,1,0:T(8,128)(2,1)S(1)}, u32[]{:S(2)}, u32[]{:S(2)}) async-start(bf16[64,16,128]{2,1,0:T(8,128)(2,1)} %shard_map.251), calls=%async_computation.4 | async-start | bytes 524288 | tf_op jit(solution)/shard_map/all_to_all | solution.py:21
  103.2 3.1 %collective-permute-start.3 = (bf16[128,128]{1,0:T(8,128)(2,1)S(1)}, bf16[128,128]{1,0:T(8,128)(2,1)S(1)}, u32[]{:S(2)}, u32[]{:S(2)}) collective-permute-start(bf16[128,128]{1,0:T(8,128)(2,1)S(1)} %get-tuple-element.59.middle), channel_id=1, source_target_pairs={{0,1},{1,0},{2,3},{3,2},{4,5},{5,4},{6,7},{7,6},{8,9},{9,8},{10,11... | collective-permute-start | bytes 98312 | tf_op jit(solution)/shard_map/ppermute | solution.py:27
  109.1 3.3 %collective-permute-start.4 = (f32[128,128]{1,0:T(8,128)}, f32[128,128]{1,0:T(8,128)S(1)}, u32[]{:S(2)}, u32[]{:S(2)}) collective-permute-start(f32[128,128]{1,0:T(8,128)} %get-tuple-element.61), channel_id=1, source_target_pairs={{0,1},{1,0},{2,3},{3,2},{4,5},{5,4},{6,7},{7,6},{8,9},{9,8},{10,11... | collective-permute-start | bytes 196616 | tf_op jit(solution)/shard_map/ppermute | solution.py:27

commit v9 on v8

--- a/solution.py
+++ b/solution.py
@@ -261,10 +261,15 @@
         out[p] = wide[p * rows : (p + 1) * rows, :].astype(BF16)
 
 
-def side_body(
-    index, middle, other, gain, w_gate, w_up, w_shared_down, w_dense_up, w_dense_down, gate,
-    own_out, other_out,
-):
+def side_body(index, middle, other, *refs):
+    sources, (own_out, other_out, *held, sems) = refs[:7], refs[7:]
+    copies = [
+        pltpu.make_async_copy(source, place, sems.at[k])
+        for k, (source, place) in enumerate(zip(sources, held))
+    ]
+    for copy in copies:
+        copy.start()
+    gain, gate, w_gate, w_up, w_dense_up, w_shared_down, w_dense_down = held
     core = index[0] % 2
     tokens = middle.shape[0] // 8
     tiles = []
@@ -274,7 +279,10 @@
         tiles.append(jnp.where(core == j % 2, mine, theirs))
     values = jnp.concatenate(tiles, axis=1)
     factor = lax.rsqrt(jnp.mean(values * values, axis=-1, keepdims=True) + EPS)
+    copies[0].wait()
     x = (values * factor * row(gain)).astype(BF16)
+    for copy in copies[1:]:
+        copy.wait()
     pre = dot_t(x, w_gate[...])
     shared = (pre / (1.0 + jnp.exp(-pre)) * dot_t(x, w_up[...])).astype(BF16)
     dense = jax.nn.gelu(dot32(x, w_dense_up[...])).astype(BF16)
@@ -532,6 +540,15 @@
     payload, later = together(payload, later)
     returned = exchange(payload, "ep")
     other_half = core_swap(later)
+    side_weights = (
+        ffn_gain,
+        dense_gate,
+        w_shared_gate.T,
+        w_shared_up.T,
+        w_dense_up,
+        w_shared_down,
+        w_dense_down,
+    )
     side, away = call(
         side_body,
         (shape(half, F32), shape(half, F32)),
@@ -539,17 +556,15 @@
             index,
             later,
             other_half,
-            ffn_gain,
-            w_shared_gate.T,
-            w_shared_up.T,
-            w_shared_down,
-            w_dense_up,
-            w_dense_down,
-            dense_gate,
-        ),
-        smem=(0,),
-        hbm=range(3, 10),
+            *side_weights,
+        ),
+        smem=(0,),
+        raw=range(3, 10),
         leave=(1,),
+        scratch=(
+            *(pltpu.VMEM(w.shape, BF16) for w in side_weights),
+            pltpu.SemaphoreType.DMA((len(side_weights),)),
+        ),
     )
     away = core_swap(away)
     returned, side = together(returned, side + away)

time: 129 us -> 129 us (level)
  no operation moved by 1% of the time
where the time goes in v9:
time: 129 us; the launch traced here: 127 us
  blocking collectives  62.8 us (49%)
  starting transfers between devices  35.4 us (27%)
  Pallas kernels  16.8 us (13%)
  waiting for transfers between devices  10.4 us (8%)
    all_to_all x4, blocking collectives, exchange(): lax.all_to_all(x, axis, split_axis=0, concat_axis=0, axis_index_groups=gr...  62.8 us
    all_to_all x2, starting transfers between devices, exchange(): lax.all_to_all(x, axis, split_axis=0, concat_axis=0, axis_index_groups=gr...  22 us
    pallas_call x11, Pallas kernels, call(): pl.pallas_call(body, out_shape=outs, in_specs=[kinds.get(i, vmem) for i i...  16.8 us
    ppermute x5, starting transfers between devices, core_swap(): lax.ppermute(x, 'tp', [(i, i ^ 1) for i in range(lax.axis_size('tp'))])  13.4 us
    all_to_all x2, waiting for transfers between devices, exchange(): lax.all_to_all(x, axis, split_axis=0, concat_axis=0, axis_index_groups=gr...  7.28 us
    ppermute x5, waiting for transfers between devices, core_swap(): lax.ppermute(x, 'tp', [(i, i ^ 1) for i in range(lax.axis_size('tp'))])  3.08 us
  transfers between devices with their start and end apart: 7, of which 5 were waited for; matrix products, arithmetic and copies ran while one was open for 1% of the time, Pallas kernels for 5%

profile of v9, /device:TPU:1, one launch (start us, length us, event | category | flops | bytes accessed | tf_op | source)
XLA Modules:
  0.0 126.8 jit_solution(5187892539765264506)
XLA Ops:
  0.0 2.1 %shard_map.244 = (bf16[16,8,128]{2,1,0:T(8,128)(2,1)}, bf16[16,2048]{1,0:T(8,128)(2,1)S(1)}) custom-call(bf16[16,2048]{1,0:T(8,128)(2,1)} %hidden.1, bf16[2048]{0:T(1024)(128)(2,1)} %refs_1_.2, bf16[64,2048]{1,0:T(8,128)(2,1)} %bitcast.14, bf16[32,2048]{1,0:T(8,128)(2,1)} %bitcast.17, bf16[64,512]{1,0:T(8,128)(2,1)} %refs_4_.2), custom_call_target="tpu_custom_call" | custom-call | tf_op jit(solution)/shard_map/pallas_call | solution.py:54
  2.1 17.4 %all-to-all-start = ((bf16[16,8,128]{2,1,0:T(8,128)(2,1)}), bf16[16,8,128]{2,1,0:T(8,128)(2,1)S(1)}, u32[]{:S(2)}, u32[]{:S(2)}) async-start(bf16[16,8,128]{2,1,0:T(8,128)(2,1)} %get-tuple-element.35), calls=%async_computation | async-start | bytes 65536 | tf_op jit(solution)/shard_map/all_to_all | solution.py:21
  20.1 0.6 fusion
  20.8 0.0 copy-start.6
  20.8 0.0 copy-start.7
  20.8 3.1 %shard_map.245 = (f32[1,640]{1,0:T(1,128)S(1)}, bf16[1632,512]{1,0:T(8,128)(2,1)S(1)}) custom-call(s32[1]{0:T(128)} %bitcast.index, bf16[16,2048]{1,0:T(8,128)(2,1)S(1)} %get-tuple-element.36.normed, bf16[2048,512]{1,0:T(8,128)(2,1)} %w_latent.1, bf16[32,2048]{1,0:T(8,128)(2,1)} %bitcast.18, bf16[512]{0:T(512)(128)(2,1)} %gain.4, ...), custom_call_target="tpu_custom_call" | custom-call | tf_op jit(solution)/shard_map/pallas_call | solution.py:54
  23.9 0.0 copy-start
  23.9 0.0 copy-start.2
  23.9 0.0 copy-start.5
  23.9 3.0 %all-to-all-done.arrived = bf16[16,8,128]{2,1,0:T(8,128)(2,1)S(1)} async-done(((bf16[16,8,128]{2,1,0:T(8,128)(2,1)}), bf16[16,8,128]{2,1,0:T(8,128)(2,1)S(1)}, u32[]{:S(2)}, u32[]{:S(2)}) %all-to-all-start) | async-done | bytes 32800 | tf_op jit(solution)/shard_map/all_to_all | solution.py:21
  27.0 0.0 copy-done.6
  27.0 0.0 copy-done.7
  27.0 0.0 copy-start.1
  27.0 0.0 copy-start.4
  27.0 1.9 %shard_map.246 = bf16[16,8,128]{2,1,0:T(8,128)(2,1)} custom-call(s32[1]{0:T(128)S(6)} %copy.27.lengths, bf16[16,8,128]{2,1,0:T(8,128)(2,1)S(1)} %all-to-all-done.arrived, bf16[1632,512]{1,0:T(8,128)(2,1)S(1)} %get-tuple-element.39.caches, f32[1,640]{1,0:T(1,128)S(1)} %get-tuple-element.40.token, f32[1,16]{1,0:T(1,128)S(1)} %copy-done.7, f32[1,16]{1,0:T(1,128)S(1)} %copy-done.6), custom_call_target="tpu_custom_call" | custom-call | tf_op jit(solution)/shard_map/pallas_call | solution.py:54
  28.8 1.3 %shard_map.247 = (bf16[80,1536]{1,0:T(8,128)(2,1)S(1)}, bf16[48,128]{1,0:T(8,128)(2,1)S(1)}) custom-call(s32[1]{0:T(128)} %bitcast.index, s32[4,16]{1,0:T(4,128)} %bitcast.12, f32[4,16]{1,0:T(4,128)} %bitcast.19, bf16[64,512]{1,0:T(8,128)(2,1)} %bitcast.10, bf16[64]{0:T(256)(128)(2,1)} %gain.6, bf16[64,2048]{1,0:T(8,128)(2,1)} %w_output.3), custom_call_target="tpu_custom_call" | custom-call | tf_op jit(solution)/shard_map/pallas_call | solution.py:54
  30.2 2.3 %collective-permute-start = (bf16[80,1536]{1,0:T(8,128)(2,1)S(1)}, bf16[80,1536]{1,0:T(8,128)(2,1)S(1)}, u32[]{:S(2)}, u32[]{:S(2)}) collective-permute-start(bf16[80,1536]{1,0:T(8,128)(2,1)S(1)} %get-tuple-element.43), channel_id=1, source_target_pairs={{0,1},{1,0},{2,3},{3,2},{4,5},{5,4},{6,7},{7,6},{8,9},{9,8},{10,11... | collective-permute-start | bytes 737288 | tf_op jit(solution)/shard_map/ppermute | solution.py:27
  32.5 11.4 %all_to_all.30.arrived = bf16[16,8,128]{2,1,0:T(8,128)(2,1)S(1)} all-to-all(bf16[16,8,128]{2,1,0:T(8,128)(2,1)} %shard_map.246), channel_id=1, replica_groups=mesh['ep'=64,'tp'=16] {'tp'}, dimensions={0} | all-to-all | bytes 65536 | tf_op jit(solution)/shard_map/all_to_all | solution.py:21
  43.9 0.0 collective-permute-done.pack
  43.9 0.0 copy-done
  43.9 0.0 copy-done.2
  43.9 0.0 copy-done.5
  43.9 0.4 shard_map.248
  44.4 0.0 copy-start.3
  44.4 14.7 %all_to_all.31.shares = bf16[8,128,128]{2,1,0:T(8,128)(2,1)S(1)} all-to-all(bf16[8,128,128]{2,1,0:T(8,128)(2,1)S(1)} %shard_map.248), channel_id=1, replica_groups={{0,2,4,6,8,10,12,14},{1,3,5,7,9,11,13,15},{16,18,20,22,24,26,28,30},{17..., dimensions={0} | all-to-all | bytes 524288 | tf_op jit(solution)/shard_map/all_to_all | solution.py:21
  59.1 0.0 copy-done.1
  59.1 0.0 copy-done.4
  59.1 1.1 shard_map.249
  60.2 0.0 copy-start.8
  60.2 1.5 %shard_map.250 = (bf16[2560,256]{1,0:T(8,128)(2,1)S(1)}, bf16[512,256]{1,0:T(8,128)(2,1)S(1)}) custom-call(s32[1]{0:T(128)} %bitcast.index, bf16[1,2048,128]{2,1,0:T(8,128)(2,1)} %w_gate.1, bf16[1,2048,128]{2,1,0:T(8,128)(2,1)} %w_up.1, bf16[1,128,2048]{2,1,0:T(8,128)(2,1)} %w_down.1), custom_call_target="tpu_custom_call" | custom-call | tf_op jit(solution)/shard_map/pallas_call | solution.py:54
  61.7 2.4 %collective-permute-start.1 = (bf16[2560,256]{1,0:T(8,128)(2,1)S(1)}, bf16[2560,256]{1,0:T(8,128)(2,1)S(1)}, u32[]{:S(2)}, u32[]{:S(2)}) collective-permute-start(bf16[2560,256]{1,0:T(8,128)(2,1)S(1)} %get-tuple-element.54.packed), channel_id=1, source_target_pairs={{0,1},{1,0},{2,3},{3,2},{4,5},{5,4},{6,7},{7,6},{8,9},{9,8},{10,11... | collective-permute-start | bytes 3932168 | tf_op jit(solution)/shard_map/ppermute | solution.py:27
  64.1 0.0 copy-done.8
  64.2 27.4 %all_to_all.32.arrived = bf16[64,16,128]{2,1,0:T(8,128)(2,1)S(1)} all-to-all(bf16[64,16,128]{2,1,0:T(8,128)(2,1)S(1)} %copy-done.8), channel_id=1, replica_groups=mesh['ep'=64,'tp'=16] {'ep'}, dimensions={0} | all-to-all | bytes 524288 | tf_op jit(solution)/shard_map/all_to_all | solution.py:21
  91.5 0.0 collective-permute-done.1.away
  91.5 4.1 %collective-permute-start.2 = (bf16[64,16,128]{2,1,0:T(8,128)(2,1)S(1)}, bf16[64,16,128]{2,1,0:T(8,128)(2,1)S(1)}, u32[]{:S(2)}, u32[]{:S(2)}) collective-permute-start(bf16[64,16,128]{2,1,0:T(8,128)(2,1)S(1)} %all_to_all.32.arrived), channel_id=1, source_target_pairs={{0,1},{1,0},{2,3},{3,2},{4,5},{5,4},{6,7},{7,6},{8,9},{9,8},{10,11... | collective-permute-start | bytes 786440 | tf_op jit(solution)/shard_map/ppermute | solution.py:27
  95.7 1.1 collective-permute-done.2.other
  96.8 0.0 copy-done.3
  96.8 1.8 %shard_map.251 = bf16[64,16,128]{2,1,0:T(8,128)(2,1)} custom-call(s32[1]{0:T(128)} %bitcast.index, bf16[64,16,128]{2,1,0:T(8,128)(2,1)S(1)} %all_to_all.32.arrived, bf16[64,16,128]{2,1,0:T(8,128)(2,1)S(1)} %collective-permute-done.2.other, bf16[2048]{0:T(1024)(128)(2,1)S(1)} %copy-done.3, bf16[2560,256]{1,0:T(8,128)(2,1)S(1)} %get-tuple-element.54.packed, ...), custom_call_target="tpu_custom_call" | custom-call | tf_op jit(solution)/shard_map/pallas_call | solution.py:54
  98.6 4.6 %all-to-all-start.4 = ((bf16[64,16,128]{2,1,0:T(8,128)(2,1)}), bf16[64,16,128]{2,1,0:T(8,128)(2,1)S(1)}, u32[]{:S(2)}, u32[]{:S(2)}) async-start(bf16[64,16,128]{2,1,0:T(8,128)(2,1)} %shard_map.251), calls=%async_computation.4 | async-start | bytes 524288 | tf_op jit(solution)/shard_map/all_to_all | solution.py:21
  103.2 2.3 %collective-permute-start.3 = (bf16[128,128]{1,0:T(8,128)(2,1)S(1)}, bf16[128,128]{1,0:T(8,128)(2,1)S(1)}, u32[]{:S(2)}, u32[]{:S(2)}) collective-permute-start(bf16[128,128]{1,0:T(8,128)(2,1)S(1)} %get-tuple-element.59.middle), channel_id=1, source_target_pairs={{0,1},{1,0},{2,3},{3,2},{4,5},{5,4},{6,7},{7,6},{8,9},{9,8},{10,11... | collective-permute-start | bytes 98312 | tf_op jit(solution)/shard_map/ppermute | solution.py:27
  105.5 0.8 collective-permute-done.3.other
  106.4 2.7 %shard_map.252 = (f32[128,128]{1,0:T(8,128)S(1)}, f32[128,128]{1,0:T(8,128)}) custom-call(s32[1]{0:T(128)} %bitcast.index, bf16[128,128]{1,0:T(8,128)(2,1)S(1)} %get-tuple-element.59.middle, bf16[128,128]{1,0:T(8,128)(2,1)S(1)} %collective-permute-done.3.other, bf16[2048]{0:T(1024)(128)(2,1)} %refs_0_.3, bf16[2048]{0:T(1024)(128)(2,1)} %refs_1_.3, ...), custom_call_target="tpu_custom_call" | custom-call | tf_op jit(solution)/shard_map/pallas_call | solution.py:54
  109.1 2.3 %collective-permute-start.4 = (f32[128,128]{1,0:T(8,128)}, f32[128,128]{1,0:T(8,128)S(1)}, u32[]{:S(2)}, u32[]{:S(2)}) collective-permute-start(f32[128,128]{1,0:T(8,128)} %get-tuple-element.61), channel_id=1, source_target_pairs={{0,1},{1,0},{2,3},{3,2},{4,5},{5,4},{6,7},{7,6},{8,9},{9,8},{10,11... | collective-permute-start | bytes 196616 | tf_op jit(solution)/shard_map/ppermute | solution.py:27
  111.3 1.1 collective-permute-done.4
  112.4 4.3 %all-to-all-done.4.returned = bf16[64,16,128]{2,1,0:T(8,128)(2,1)S(1)} async-done(((bf16[64,16,128]{2,1,0:T(8,128)(2,1)}), bf16[64,16,128]{2,1,0:T(8,128)(2,1)S(1)}, u32[]{:S(2)}, u32[]{:S(2)}) %all-to-all-start.4) | async-done | bytes 262176 | tf_op jit(solution)/shard_map/all_to_all | solution.py:21
  116.7 0.2 shard_map.253
  117.0 9.3 %all_to_all.33.tiles = bf16[8,16,128]{2,1,0:T(8,128)(2,1)S(1)} all-to-all(bf16[8,16,128]{2,1,0:T(8,128)(2,1)S(1)} %shard_map.253), channel_id=1, replica_groups={{0,2,4,6,8,10,12,14},{1,3,5,7,9,11,13,15},{16,18,20,22,24,26,28,30},{17..., dimensions={0} | all-to-all | bytes 65536 | tf_op jit(solution)/shard_map/all_to_all | solution.py:21
  126.2 0.6 shard_map.254
  (1 shorter events, 0.0 us)
Async XLA Ops:
  2.1 24.9 %all-to-all-start = ((bf16[16,8,128]{2,1,0:T(8,128)(2,1)}), bf16[16,8,128]{2,1,0:T(8,128)(2,1)S(1)}, u32[]{:S(2)}, u32[]{:S(2)}) async-start(bf16[16,8,128]{2,1,0:T(8,128)(2,1)} %get-tuple-element.35), calls=%async_computation | async-start | bytes 65536 | tf_op jit(solution)/shard_map/all_to_all | solution.py:21
  20.8 6.2 %copy-start.6 = (f32[1,16]{1,0:T(1,128)S(1)}, f32[1,16]{1,0:T(1,128)}, u32[]{:S(2)}) copy-start(f32[1,16]{1,0:T(1,128)} %get-tuple-element.65.sin) | copy-start | bytes 196
  20.8 6.2 %copy-start.7 = (f32[1,16]{1,0:T(1,128)S(1)}, f32[1,16]{1,0:T(1,128)}, u32[]{:S(2)}) copy-start(f32[1,16]{1,0:T(1,128)} %get-tuple-element.66.cos) | copy-start | bytes 196
  23.9 20.0 %copy-start = (bf16[64,2048]{1,0:T(8,128)(2,1)S(1)}, bf16[64,2048]{1,0:T(8,128)(2,1)}, u32[]{:S(2)}) copy-start(bf16[64,2048]{1,0:T(8,128)(2,1)} %w_output.3) | copy-start | bytes 786436
  23.9 20.0 %copy-start.2 = (bf16[512,64]{0,1:T(8,128)(2,1)S(1)}, bf16[512,64]{0,1:T(8,128)(2,1)}, u32[]{:S(2)}) copy-start(bf16[512,64]{0,1:T(8,128)(2,1)} %param.37) | copy-start | bytes 196612
  23.9 20.0 %copy-start.5 = (bf16[64]{0:T(256)(128)(2,1)S(1)}, bf16[64]{0:T(256)(128)(2,1)}, u32[]{:S(2)}) copy-start(bf16[64]{0:T(256)(128)(2,1)} %gain.6) | copy-start | bytes 388
  27.0 32.1 %copy-start.1 = (bf16[16,2048]{1,0:T(8,128)(2,1)S(1)}, bf16[16,2048]{1,0:T(8,128)(2,1)}, u32[]{:S(2)}) copy-start(bf16[16,2048]{1,0:T(8,128)(2,1)} %hidden.1) | copy-start | bytes 196612
  27.0 32.1 %copy-start.4 = (s32[16,4]{0,1:T(4,128)S(1)}, s32[16,4]{0,1:T(4,128)}, u32[]{:S(2)}) copy-start(s32[16,4]{0,1:T(4,128)} %param.41) | copy-start | bytes 772
  30.2 13.8 %collective-permute-start = (bf16[80,1536]{1,0:T(8,128)(2,1)S(1)}, bf16[80,1536]{1,0:T(8,128)(2,1)S(1)}, u32[]{:S(2)}, u32[]{:S(2)}) collective-permute-start(bf16[80,1536]{1,0:T(8,128)(2,1)S(1)} %get-tuple-element.43), channel_id=1, source_target_pairs={{0,1},{1,0},{2,3},{3,2},{4,5},{5,4},{6,7},{7,6},{8,9},{9,8},{10,11... | collective-permute-start | bytes 737288 | tf_op jit(solution)/shard_map/ppermute | solution.py:27
  44.4 52.4 %copy-start.3 = (bf16[2048]{0:T(1024)(128)(2,1)S(1)}, bf16[2048]{0:T(1024)(128)(2,1)}, u32[]{:S(2)}) copy-start(bf16[2048]{0:T(1024)(128)(2,1)} %refs_0_.3) | copy-start | bytes 12292
  60.2 4.0 %copy-start.8 = (bf16[64,16,128]{2,1,0:T(8,128)(2,1)S(1)}, bf16[64,16,128]{2,1,0:T(8,128)(2,1)}, u32[]{:S(2)}) copy-start(bf16[64,16,128]{2,1,0:T(8,128)(2,1)} %get-tuple-element.49) | copy-start | bytes 786436
  61.7 29.8 %collective-permute-start.1 = (bf16[2560,256]{1,0:T(8,128)(2,1)S(1)}, bf16[2560,256]{1,0:T(8,128)(2,1)S(1)}, u32[]{:S(2)}, u32[]{:S(2)}) collective-permute-start(bf16[2560,256]{1,0:T(8,128)(2,1)S(1)} %get-tuple-element.54.packed), channel_id=1, source_target_pairs={{0,1},{1,0},{2,3},{3,2},{4,5},{5,4},{6,7},{7,6},{8,9},{9,8},{10,11... | collective-permute-start | bytes 3932168 | tf_op jit(solution)/shard_map/ppermute | solution.py:27
  91.5 5.3 %collective-permute-start.2 = (bf16[64,16,128]{2,1,0:T(8,128)(2,1)S(1)}, bf16[64,16,128]{2,1,0:T(8,128)(2,1)S(1)}, u32[]{:S(2)}, u32[]{:S(2)}) collective-permute-start(bf16[64,16,128]{2,1,0:T(8,128)(2,1)S(1)} %all_to_all.32.arrived), channel_id=1, source_target_pairs={{0,1},{1,0},{2,3},{3,2},{4,5},{5,4},{6,7},{7,6},{8,9},{9,8},{10,11... | collective-permute-start | bytes 786440 | tf_op jit(solution)/shard_map/ppermute | solution.py:27
  98.6 18.1 %all-to-all-start.4 = ((bf16[64,16,128]{2,1,0:T(8,128)(2,1)}), bf16[64,16,128]{2,1,0:T(8,128)(2,1)S(1)}, u32[]{:S(2)}, u32[]{:S(2)}) async-start(bf16[64,16,128]{2,1,0:T(8,128)(2,1)} %shard_map.251), calls=%async_computation.4 | async-start | bytes 524288 | tf_op jit(solution)/shard_map/all_to_all | solution.py:21
  103.2 3.1 %collective-permute-start.3 = (bf16[128,128]{1,0:T(8,128)(2,1)S(1)}, bf16[128,128]{1,0:T(8,128)(2,1)S(1)}, u32[]{:S(2)}, u32[]{:S(2)}) collective-permute-start(bf16[128,128]{1,0:T(8,128)(2,1)S(1)} %get-tuple-element.59.middle), channel_id=1, source_target_pairs={{0,1},{1,0},{2,3},{3,2},{4,5},{5,4},{6,7},{7,6},{8,9},{9,8},{10,11... | collective-permute-start | bytes 98312 | tf_op jit(solution)/shard_map/ppermute | solution.py:27
  109.1 3.4 %collective-permute-start.4 = (f32[128,128]{1,0:T(8,128)}, f32[128,128]{1,0:T(8,128)S(1)}, u32[]{:S(2)}, u32[]{:S(2)}) collective-permute-start(f32[128,128]{1,0:T(8,128)} %get-tuple-element.61), channel_id=1, source_target_pairs={{0,1},{1,0},{2,3},{3,2},{4,5},{5,4},{6,7},{7,6},{8,9},{9,8},{10,11... | collective-permute-start | bytes 196616 | tf_op jit(solution)/shard_map/ppermute | solution.py:27
